TPU v7x, 1024 devices: a whole 4x4x32 slice. The times are simulated.
1024 devices in a mesh: kv: 128 (over z, y), tp: 8 (over x, core).
Axes of the slice: x: 4, y: 4, z: 32, core: 2. Of those that a mesh axis runs over, the one named last changes fastest.
Arguments:
- tokens: bfloat16 [32768, 2048], P('kv'), may hold values from -6 to 6
- query_weight: bfloat16 [2048, 2048], P(None, 'tp'), may hold values from -0.125 to 0.125
- key_weight: bfloat16 [2048, 512], P(None, 'tp'), may hold values from -0.125 to 0.125
- value_weight: bfloat16 [2048, 512], P(None, 'tp'), may hold values from -0.125 to 0.125
- gate_weight: bfloat16 [2048, 64], replicated, may hold values from -0.125 to 0.125
- query_gain: float32 [64], replicated
- key_gain: float32 [64], replicated
- out_weight: bfloat16 [2048, 2048], P('tp'), may hold values from -0.125 to 0.125
- shared_block: int32 [128], P('kv'), may hold values from 0 to 3, as said below
- chosen_device: int32 [512, 15], P('kv'), may hold values from 0 to 127, as said below
Outputs:
- mixed_out: bfloat16 [32768, 2048], P(('kv', 'tp'))
- log_weight: float32 [2, 32768, 32], P(None, 'kv', 'tp')
Inputs may be any that keep to these rules, and one draw needn't show every extreme that they name: `shared_block`: entry d names one of the 64-position blocks of device d's 256 positions. `chosen_device`: row b names 15 different devices, never the device that holds query block b.
All inputs are finite; a program needn't handle non-finite values.
Results may differ from a plain program's by a relative error of at most 0.019.
The roundings to bfloat16 on the way count: a program that leaves them out, or rounds other values in their place, can miss the bound.
Values may be sent and summed in bfloat16 or wider, within the bound.
No kernel may reach another device: no remote copies, remote signals or barrier semaphores. Data moves between devices by JAX's collectives and lax.ppermute only.
A program may use at most 32 MiB of HBM per device.

v0:
```python
import jax
import jax.numpy as jnp
from jax import lax
from jax.sharding import Mesh
from jax.sharding import PartitionSpec as P

SEL = 64
CMP = 32
KV = ("kv_0", "kv_1")
KV_TP = ("kv_0", "kv_1", "tp")


norm_eps = 1e-06
rope_base = 500000.0
big_negative = -1e30


def in_order(pieces, dim):
    lengths = list(pieces.shape[1:])
    lengths[dim] *= pieces.shape[0]
    return jnp.moveaxis(pieces, 0, dim).reshape(lengths)


def gather_in_order(array, axes, sequence):
    pieces = array[None]
    for k in sequence:
        pieces = lax.all_gather(pieces, axes[k], axis=0, tiled=True)
    carried = [lax.axis_size(axes[k]) for k in reversed(sequence)]
    pieces = pieces.reshape(*carried, *array.shape)
    turned = sorted(range(len(sequence)), key=lambda place: sequence[len(sequence) - 1 - place])
    return pieces.transpose(*turned, *range(len(sequence), pieces.ndim)).reshape(-1, *array.shape)


def whole_of(array, axes, sequence, dim):
    return in_order(gather_in_order(array, axes, sequence), dim)


def split_up(array, dim, length):
    lengths = array.shape
    pieces = array.reshape(*lengths[:dim], length, lengths[dim] // length, *lengths[dim + 1 :])
    return jnp.moveaxis(pieces, dim, 0)


def sent_and_summed(array, axis, dim):
    pieces = split_up(array, dim, lax.axis_size(axis))
    arrived = lax.all_to_all(pieces, axis, split_axis=0, concat_axis=0, tiled=True)
    return arrived.astype(jnp.float32).sum(axis=0)


def rounded(values_in):
    return lax.optimization_barrier(values_in.astype(jnp.bfloat16))


def unit_norm(values_in, gain_vec):
    upcast = values_in.astype(jnp.float32)
    return (
        upcast * lax.rsqrt(jnp.mean(upcast * upcast, axis=-1, keepdims=True) + norm_eps) * gain_vec
    )


def rotate(values_in, places):
    half_size = values_in.shape[-1] // 2
    inverse = jnp.power(
        rope_base, -jnp.arange(half_size, dtype=jnp.float32) * 2.0 / values_in.shape[-1]
    )
    angles = places.astype(jnp.float32)[:, None] * inverse[None, :]
    cos_vals = jnp.cos(angles)[:, None, :]
    sin_vals = jnp.sin(angles)[:, None, :]
    upcast = values_in.astype(jnp.float32)
    front_half = upcast[..., :half_size]
    back_half = upcast[..., half_size:]
    return jnp.concatenate(
        [
            front_half * cos_vals - back_half * sin_vals,
            back_half * cos_vals + front_half * sin_vals,
        ],
        axis=-1,
    )


def shards(
    tokens,
    query_weight,
    key_weight,
    value_weight,
    gate_weight,
    query_gain,
    key_gain,
    out_weight,
    shared_block,
    chosen_device,
):
    tok_rows = tokens.shape[0]
    head_size = query_gain.shape[0]
    head_count = query_weight.shape[1] // head_size
    groups = key_weight.shape[1] // head_size
    per_group = head_count // groups
    group_width = groups * head_size
    block_len = SEL
    local_blocks = tok_rows // block_len
    device = lax.axis_index(KV)
    tp_index = lax.axis_index("tp")
    score_scale = head_size ** (-0.5)
    places = device * tok_rows + jnp.arange(tok_rows, dtype=jnp.int32)
    queries = rounded(jnp.dot(tokens, query_weight, preferred_element_type=jnp.float32)).reshape(
        tok_rows, head_count, head_size
    )
    keys_raw = rounded(jnp.dot(tokens, key_weight, preferred_element_type=jnp.float32)).reshape(
        tok_rows, groups, head_size
    )
    values_raw = rounded(jnp.dot(tokens, value_weight, preferred_element_type=jnp.float32))
    q_plain = rounded(unit_norm(queries, query_gain))
    k_plain = rounded(unit_norm(keys_raw, key_gain))
    q_turned = rotate(q_plain, places).astype(jnp.bfloat16)
    k_turned = rotate(k_plain, places).astype(jnp.bfloat16).reshape(tok_rows, group_width)
    gate_cols = lax.dynamic_slice_in_dim(gate_weight, tp_index * 2 * head_count, 2 * head_count, 1)
    gate_vals = jax.nn.sigmoid(
        jnp.dot(tokens, gate_cols, preferred_element_type=jnp.float32)
    ).reshape(tok_rows, head_count, 2)
    span_count = tok_rows // CMP
    span_keys = jnp.mean(
        k_plain.astype(jnp.float32).reshape(span_count, CMP, group_width), axis=1
    ).astype(jnp.bfloat16)
    span_values = jnp.mean(
        values_raw.astype(jnp.float32).reshape(span_count, CMP, group_width), axis=1
    ).astype(jnp.bfloat16)
    summary = jnp.concatenate([span_keys, span_values], axis=1)
    first_row = shared_block[0] * block_len
    shared = jnp.concatenate(
        [
            lax.dynamic_slice_in_dim(k_turned, first_row, block_len, 0),
            lax.dynamic_slice_in_dim(values_raw, first_row, block_len, 0),
        ],
        axis=1,
    )[None]
    all_summary, all_shared = (whole_of(summary, KV, (0, 1), 0), whole_of(shared, KV, (0, 1), 0))
    total_spans = all_summary.shape[0]
    span_keys_all = all_summary[:, :group_width].reshape(total_spans, groups, head_size)
    span_values_all = all_summary[:, group_width:].reshape(total_spans, groups, head_size)
    q_grouped = q_plain.reshape(tok_rows, groups, per_group, head_size)
    scores = (
        jnp.einsum("rghd,cgd->rghc", q_grouped, span_keys_all, preferred_element_type=jnp.float32)
        * score_scale
    )
    span_ends = jnp.arange(total_spans, dtype=jnp.int32) * CMP + CMP - 1
    allowed = (span_ends[None, :] <= places[:, None])[:, None, None, :]
    has_span = (places >= CMP - 1)[:, None, None]
    peak_val = jnp.max(jnp.where(allowed, scores, big_negative), axis=-1)
    weights_raw = jnp.where(allowed, jnp.exp(scores - peak_val[..., None]), 0.0)
    divisor = jnp.where(has_span, jnp.sum(weights_raw, axis=-1), 1.0)
    span_out = (
        jnp.einsum(
            "rghc,cgd->rghd",
            weights_raw.astype(jnp.bfloat16),
            span_values_all,
            preferred_element_type=jnp.float32,
        )
        / divisor[..., None]
    )
    span_lse = jnp.where(has_span, peak_val + jnp.log(divisor), 0.0)
    q_blocks = q_turned.reshape(local_blocks, block_len, groups, per_group, head_size)
    own_keys = k_turned.reshape(local_blocks, block_len, groups, head_size)
    own_values = values_raw.reshape(local_blocks, block_len, groups, head_size)
    causal_own = jnp.arange(block_len)[None, :] <= jnp.arange(block_len)[:, None]
    named_count = chosen_device.shape[1]
    remote = all_shared[chosen_device].reshape(
        local_blocks, named_count * block_len, 2 * group_width
    )
    key_rows = jnp.concatenate(
        [own_keys, remote[..., :group_width].reshape(local_blocks, -1, groups, head_size)], axis=1
    )
    value_rows = jnp.concatenate(
        [own_values, remote[..., group_width:].reshape(local_blocks, -1, groups, head_size)], axis=1
    )
    remote_ok = jnp.repeat(chosen_device < device, block_len, axis=1)
    allowed_sel = jnp.concatenate(
        [
            jnp.broadcast_to(causal_own[None], (local_blocks, block_len, block_len)),
            jnp.broadcast_to(
                remote_ok[:, None, :], (local_blocks, block_len, named_count * block_len)
            ),
        ],
        axis=2,
    )[:, :, None, None, :]
    scores_sel = (
        jnp.einsum("jqghd,jkgd->jqghk", q_blocks, key_rows, preferred_element_type=jnp.float32)
        * score_scale
    )
    peak_sel = jnp.max(jnp.where(allowed_sel, scores_sel, big_negative), axis=-1)
    weights_sel = jnp.where(allowed_sel, jnp.exp(scores_sel - peak_sel[..., None]), 0.0)
    sum_sel = jnp.sum(weights_sel, axis=-1)
    chosen_out = (
        jnp.einsum(
            "jqghk,jkgd->jqghd",
            weights_sel.astype(jnp.bfloat16),
            value_rows,
            preferred_element_type=jnp.float32,
        )
        / sum_sel[..., None]
    )
    chosen_lse = peak_sel + jnp.log(sum_sel)
    mixed_heads = (
        gate_vals[..., 0:1] * span_out.reshape(tok_rows, head_count, head_size)
        + gate_vals[..., 1:2] * chosen_out.reshape(tok_rows, head_count, head_size)
    ).astype(jnp.bfloat16)
    mixed_heads = mixed_heads.reshape(tok_rows, head_count * head_size)
    mixed_out = sent_and_summed(
        jnp.dot(mixed_heads, out_weight, preferred_element_type=jnp.float32).astype(jnp.bfloat16),
        "tp",
        0,
    ).astype(jnp.bfloat16)
    log_weight = jnp.stack(
        [span_lse.reshape(tok_rows, head_count), chosen_lse.reshape(tok_rows, head_count)]
    )
    return (mixed_out, log_weight)


def solution(mesh):
    torus = Mesh(mesh.devices.reshape(32, 4, mesh.shape["tp"]), ("kv_0", "kv_1", "tp"))
    return jax.shard_map(
        shards,
        mesh=torus,
        in_specs=(
            P(KV, None),
            P(None, "tp"),
            P(None, "tp"),
            P(None, "tp"),
            P(),
            P(),
            P(),
            P("tp", None),
            P(KV),
            P(KV, None),
        ),
        out_specs=(P(KV_TP, None), P(None, KV, "tp")),
        check_vma=False,
    )
```

profile of v0, /device:TPU:1, one launch (start us, length us, event | category | flops | bytes accessed | tf_op | source)
XLA Modules:
  0.0 213.6 jit_solution(10321295822801554678)
XLA Ops:
  8.1 1.7 convolution_convert_fusion.3
  9.9 0.7 fusion.61
  10.6 1.7 convolution_convert_fusion.2
  12.5 0.2 fusion.60
  12.9 62.5 %all-gather.1 = bf16[2048,128]{1,0:T(8,128)(2,1)} all-gather(bf16[64,128]{1,0:T(8,128)(2,1)S(1)} %copy.84), channel_id=3, replica_groups=mesh['kv_0'=32,'kv_1'=4,'tp'=8] {'kv_0'}, dimensions={0}, use_global_device_ids=true | all-gather | bytes 540672 | tf_op jit(solution)/shard_map/all_gather | solution.py:27
  75.4 0.5 broadcast_compare_fusion.1
  75.9 0.1 reshape.479
  76.2 0.7 concatenate.56
  76.9 0.1 copy.77
  77.0 0.1 copy.78
  77.1 0.7 reshape.494
  77.8 1.1 fusion.27
  78.9 0.7 broadcast_in_dim.111
  79.7 0.7 broadcast_in_dim.112
  80.4 0.6 copy.88
  81.0 0.6 copy.90
  81.6 1.4 copy.89
  83.1 38.9 %all-gather = bf16[256,128]{1,0:T(8,128)(2,1)S(1)} all-gather(bf16[8,128]{1,0:T(8,128)(2,1)S(1)} %pad_maximum_fusion.2), channel_id=2, replica_groups=mesh['kv_0'=32,'kv_1'=4,'tp'=8] {'kv_0'}, dimensions={0}, use_global_device_ids=true | all-gather | bytes 67584 | tf_op jit(solution)/shard_map/all_gather | solution.py:27
  122.0 0.4 convolution_convert_fusion.1
  122.5 0.1 copy.82
  122.6 0.7 multiply_convert_fusion
  123.4 10.7 %all_gather.13 = bf16[128,8,128]{2,1,0:T(8,128)(2,1)S(1)} all-gather(bf16[32,8,128]{2,1,0:T(8,128)(2,1)S(1)} %bitcast.194), channel_id=1, replica_groups=mesh['kv_0'=32,'kv_1'=4,'tp'=8] {'kv_1'}, dimensions={0}, use_global_device_ids=true | all-gather | bytes 327680 | tf_op jit(solution)/shard_map/all_gather | solution.py:27
  134.2 0.2 multiply_cosine_fusion
  134.4 0.1 concatenate.60
  134.5 0.2 copy.92
  134.7 0.1 concatenate.61
  134.9 0.9 copy.93
  135.8 0.7 pad_clamp_fusion
  136.6 0.3 pad_add_fusion
  136.9 0.2 broadcast_compare_fusion
  137.1 0.8 fusion.3
  137.9 0.9 fusion.6
  138.9 1.7 fusion.28
  140.6 3.1 %copy.86 = bf16[32,4,1,64,128]{4,3,1,0,2:T(8,128)(2,1)} copy(bf16[32,4,1,64,128]{4,3,0,1,2:T(8,128)(2,1)} %bitcast.186) | data formatting | bytes 4194304 | tf_op jit(solution)/shard_map/transpose | solution.py:31
  143.7 2.3 %gather_fusion = bf16[60,64,128]{2,1,0:T(8,128)(2,1)S(1)} fusion(bf16[128,64,128]{2,1,0:T(8,128)(2,1)} %bitcast.185, s32[1024]{0:T(1024)S(1)} %pad_clamp_fusion), kind=kCustom, calls=%fused_computation | custom fusion | bytes 1966320 | tf_op jit(solution)/shard_map/gather | solution.py:166
  146.0 1.3 fusion.77
  147.4 1.5 copy.106
  148.9 1.1 copy.107
  150.0 2.3 %fusion = (f32[4,64,4]{1,2,0:T(4,128)S(1)}, f32[4,1024,64,4]{1,2,3,0:T(8,128)S(1)}) fusion(pred[4,64,1024]{2,1,0:T(8,128)(4,1)S(1)} %pad_add_fusion, bf16[4,64,4,32]{3,1,2,0:T(8,128)(2,1)} %copy.93, bf16[4,64,4,32]{3,1,2,0:T(8,128)(2,1)S(1)} %copy.92, bf16[4,960,1,64]{1,3,0,2:T(8,128)(2,1)} %bitcast.192, bf16[4,64,1,32]{1,3,0,2:T(8,128)(2,1)} %copy.90, ...), kind=kOutput, calls=%fused_computation.3 | convolution fusion | flops 139197440 | bytes 5115904 | tf_op jit(solution)/shard_map/jqghd,jkgd->jqghk/dot_general | solution.py:186
  152.3 1.2 fusion.8
  153.5 1.6 fusion.34
  155.1 0.3 copy.100
  155.4 0.3 reshape.509
  155.9 1.4 convolution_convert_fusion
  157.3 33.6 %all-to-all-start = ((bf16[8,32,2048]{2,1,0:T(8,128)(2,1)}), bf16[8,32,2048]{2,1,0:T(8,128)(2,1)S(1)}, u32[]{:S(2)}, u32[]{:S(2)}) async-start(bf16[8,32,2048]{2,1,0:T(8,128)(2,1)} %bitcast.42), calls=%async_computation | async-start | bytes 2097152 | tf_op jit(solution)/shard_map/all_to_all | solution.py:46
  191.1 0.6 pad_maximum_fusion.1
  191.7 14.2 %all-to-all-done = bf16[8,32,2048]{2,1,0:T(8,128)(2,1)S(1)} async-done(((bf16[8,32,2048]{2,1,0:T(8,128)(2,1)}), bf16[8,32,2048]{2,1,0:T(8,128)(2,1)S(1)}, u32[]{:S(2)}, u32[]{:S(2)}) %all-to-all-start) | async-done | bytes 1048608 | tf_op jit(solution)/shard_map/all_to_all | solution.py:46
  205.9 0.8 reduce_sum.74
  (64 shorter events, 1.1 us)
Async XLA Ops:
  7.2 148.7 %copy-start = (bf16[256,2048]{1,0:T(8,128)(2,1)S(1)}, bf16[256,2048]{1,0:T(8,128)(2,1)}, u32[]{:S(2)}) copy-start(bf16[256,2048]{1,0:T(8,128)(2,1)} %param.17) | copy-start | bytes 3145732
  7.2 70.6 %copy-start.1 = (bf16[256,2048]{1,0:T(8,128)(2,1)S(1)}, bf16[256,2048]{1,0:T(8,128)(2,1)}, u32[]{:S(2)}) copy-start(bf16[256,2048]{1,0:T(8,128)(2,1)} %param.10) | copy-start | bytes 3145732
  7.2 68.2 %copy-start.6 = (s32[4,15]{1,0:T(4,128)S(1)}, s32[4,15]{1,0:T(4,128)}, u32[]{:S(2)}) copy-start(s32[4,15]{1,0:T(4,128)} %param.19) | copy-start | bytes 724
  7.2 114.8 %copy-start.2 = (bf16[2048,256]{1,0:T(8,128)(2,1)S(1)}, bf16[2048,256]{1,0:T(8,128)(2,1)}, u32[]{:S(2)}) copy-start(bf16[2048,256]{1,0:T(8,128)(2,1)} %param.11) | copy-start | bytes 3145732
  7.2 133.4 %all-gather.4.cloned.1.call-start = ((), (), s32[]{:S(2)}) async-start(), calls=%async_computation.1 | async-start | bytes 2621440 | tf_op jit(solution)/shard_map/all_gather | solution.py:27
  7.3 68.9 %copy-start.9 = (f32[32]{0:T(128)}, f32[32]{0:T(128)S(1)}, u32[]{:S(2)}) copy-start(f32[32]{0:T(128)S(1)} %multiply_power_fusion) | copy-start | bytes 388
  8.1 68.0 %copy-start.7 = (f32[256]{0:T(256)}, f32[256]{0:T(256)S(1)}, u32[]{:S(2)}) copy-start(f32[256]{0:T(256)S(1)} %fusion.69) | copy-start | bytes 3076
  77.1 57.1 %copy-start.8 = (f32[256]{0:T(256)S(1)}, f32[256]{0:T(256)}, u32[]{:S(2)}) copy-start(f32[256]{0:T(256)} %copy-done.7) | copy-start | bytes 3076
  77.1 57.1 %copy-start.10 = (f32[32]{0:T(128)S(1)}, f32[32]{0:T(128)}, u32[]{:S(2)}) copy-start(f32[32]{0:T(128)} %copy-done.9) | copy-start | bytes 388
  80.4 56.1 %copy-start.5 = (pred[4,960]{1,0:T(4,128)(4,1)S(1)}, pred[4,960]{1,0:T(4,128)(4,1)}, u32[]{:S(2)}) copy-start(pred[4,960]{1,0:T(4,128)(4,1)} %broadcast_in_dim.112) | copy-start | bytes 11524
  135.7 3.1 %copy-start.11 = (pred[256]{0:T(512)(128)(4,1)}, pred[256]{0:T(512)(128)(4,1)S(1)}, u32[]{:S(2)}) copy-start(pred[256]{0:T(512)(128)(4,1)S(1)} %fusion.70) | copy-start | bytes 772
  150.0 3.5 %copy-start.4 = (bf16[4,64,1,64]{1,3,0,2:T(8,128)(2,1)S(1)}, bf16[4,64,1,64]{1,3,0,2:T(8,128)(2,1)}, u32[]{:S(2)}) copy-start(bf16[4,64,1,64]{1,3,0,2:T(8,128)(2,1)} %copy.88) | copy-start | bytes 98308
  153.5 2.3 %copy-start.3 = (f32[1,64,256,4]{2,1,3,0:T(8,128)S(1)}, f32[1,64,256,4]{2,1,3,0:T(8,128)}, u32[]{:S(2)}) copy-start(f32[1,64,256,4]{2,1,3,0:T(8,128)} %fusion.28) | copy-start | bytes 786436
  155.1 35.8 %copy-start.12 = (pred[256]{0:T(512)(128)(4,1)S(1)}, pred[256]{0:T(512)(128)(4,1)}, u32[]{:S(2)}) copy-start(pred[256]{0:T(512)(128)(4,1)} %copy-done.11) | copy-start | bytes 772
  157.3 48.6 %all-to-all-start = ((bf16[8,32,2048]{2,1,0:T(8,128)(2,1)}), bf16[8,32,2048]{2,1,0:T(8,128)(2,1)S(1)}, u32[]{:S(2)}, u32[]{:S(2)}) async-start(bf16[8,32,2048]{2,1,0:T(8,128)(2,1)} %bitcast.42), calls=%async_computation | async-start | bytes 2097152 | tf_op jit(solution)/shard_map/all_to_all | solution.py:46
Sparse Core Ops, SparseCore 0:
  75.5 54.4 all-gather.3
where the time goes:
time: 214 us
  blocking collectives  112 us (52%)
  starting transfers between devices  33.7 us (16%)
  local copies, waits for them, and re-layouts  17.8 us (8%)
  between operations  15.3 us (7%)
  waiting for transfers between devices  14.3 us (7%)
  matrix products  12.8 us (6%)
  other arithmetic  7.65 us (4%)
    all_gather x3, blocking collectives, gather_in_order(): pieces = lax.all_gather(pieces, axes[k], axis=0, tiled=True)  112 us
    all_to_all x1, starting transfers between devices, sent_and_summed(): lax.all_to_all(pieces, axis, split_axis=0, concat_axis=0, tiled=True)  33.6 us
    all_to_all x1, waiting for transfers between devices, sent_and_summed(): lax.all_to_all(pieces, axis, split_axis=0, concat_axis=0, tiled=True)  14.2 us
  transfers between devices with their start and end apart: 2, of which 1 were waited for; matrix products, arithmetic and copies ran while one was open for 7% of the time, Pallas kernels for 0%

commit v1 on v0

--- a/solution.py
+++ b/solution.py
@@ -6,8 +6,8 @@
 
 SEL = 64
 CMP = 32
-KV = ("kv_0", "kv_1")
-KV_TP = ("kv_0", "kv_1", "tp")
+KV = ("z_far", "z_near", "y")
+KV_TP = ("z_far", "z_near", "y", "tp")
 
 
 norm_eps = 1e-06
@@ -15,24 +15,10 @@
 big_negative = -1e30
 
 
-def in_order(pieces, dim):
-    lengths = list(pieces.shape[1:])
-    lengths[dim] *= pieces.shape[0]
-    return jnp.moveaxis(pieces, 0, dim).reshape(lengths)
-
-
-def gather_in_order(array, axes, sequence):
-    pieces = array[None]
-    for k in sequence:
-        pieces = lax.all_gather(pieces, axes[k], axis=0, tiled=True)
-    carried = [lax.axis_size(axes[k]) for k in reversed(sequence)]
-    pieces = pieces.reshape(*carried, *array.shape)
-    turned = sorted(range(len(sequence)), key=lambda place: sequence[len(sequence) - 1 - place])
-    return pieces.transpose(*turned, *range(len(sequence), pieces.ndim)).reshape(-1, *array.shape)
-
-
-def whole_of(array, axes, sequence, dim):
-    return in_order(gather_in_order(array, axes, sequence), dim)
+def spread(block, axis):
+    count = lax.axis_size(axis)
+    copies = lax.optimization_barrier(jnp.broadcast_to(block[None], (count, *block.shape)))
+    return lax.all_to_all(copies, axis, split_axis=0, concat_axis=0, tiled=True)
 
 
 def split_up(array, dim, length):
@@ -132,9 +118,21 @@
             lax.dynamic_slice_in_dim(values_raw, first_row, block_len, 0),
         ],
         axis=1,
-    )[None]
-    all_summary, all_shared = (whole_of(summary, KV, (0, 1), 0), whole_of(shared, KV, (0, 1), 0))
+    )
+    far_count, near_count, y_count = (lax.axis_size(axis) for axis in KV)
+    column = spread(spread(jnp.concatenate([shared, summary], axis=0), "z_far"), "z_near")
+    column = column.reshape(near_count * far_count, block_len + span_count, 2 * group_width)
+    all_summary = spread(column[:, block_len:], "y").reshape(-1, 2 * group_width)
+    all_shared = spread(column[:, :block_len], "y").reshape(-1, block_len, 2 * group_width)
     total_spans = all_summary.shape[0]
+    slot_of = jnp.arange(total_spans, dtype=jnp.int32) // span_count
+    owner = (
+        (slot_of % far_count) * near_count + slot_of // far_count % near_count
+    ) * y_count + slot_of // (far_count * near_count)
+    span_starts = owner * tok_rows + jnp.arange(total_spans, dtype=jnp.int32) % span_count * CMP
+    slots = (chosen_device % y_count * near_count + chosen_device // y_count % near_count) * (
+        far_count
+    ) + chosen_device // (y_count * near_count)
     span_keys_all = all_summary[:, :group_width].reshape(total_spans, groups, head_size)
     span_values_all = all_summary[:, group_width:].reshape(total_spans, groups, head_size)
     q_grouped = q_plain.reshape(tok_rows, groups, per_group, head_size)
@@ -142,7 +140,7 @@
         jnp.einsum("rghd,cgd->rghc", q_grouped, span_keys_all, preferred_element_type=jnp.float32)
         * score_scale
     )
-    span_ends = jnp.arange(total_spans, dtype=jnp.int32) * CMP + CMP - 1
+    span_ends = span_starts + CMP - 1
     allowed = (span_ends[None, :] <= places[:, None])[:, None, None, :]
     has_span = (places >= CMP - 1)[:, None, None]
     peak_val = jnp.max(jnp.where(allowed, scores, big_negative), axis=-1)
@@ -163,7 +161,7 @@
     own_values = values_raw.reshape(local_blocks, block_len, groups, head_size)
     causal_own = jnp.arange(block_len)[None, :] <= jnp.arange(block_len)[:, None]
     named_count = chosen_device.shape[1]
-    remote = all_shared[chosen_device].reshape(
+    remote = all_shared[slots].reshape(
         local_blocks, named_count * block_len, 2 * group_width
     )
     key_rows = jnp.concatenate(
@@ -216,7 +214,7 @@
 
 
 def solution(mesh):
-    torus = Mesh(mesh.devices.reshape(32, 4, mesh.shape["tp"]), ("kv_0", "kv_1", "tp"))
+    torus = Mesh(mesh.devices.reshape(8, 4, 4, mesh.shape["tp"]), KV_TP)
     return jax.shard_map(
         shards,
         mesh=torus,

time: 214 us -> 162 us (0.76)
  blocking collectives: 112 us -> 55.1 us
  waiting for transfers between devices: 14.3 us -> 41.8 us
  between operations: 15.3 us -> 1.8 us
  starting transfers between devices: 33.7 us -> 23 us
  matrix products: 12.8 us -> 15 us
    all_gather x3 -> x0, blocking collectives: 112 us -> none  [gather_in_order(): pieces = lax.all_gather(pieces, axes[k], axis=0, tiled=True)]
    all_to_all x0 -> x1, blocking collectives: none -> 55.1 us  [spread(): return lax.all_to_all(copies, axis, split_axis=0, concat_axis=0, tiled=True)]
    all_to_all x0 -> x3, waiting for transfers between devices: none -> 27.6 us  [spread(): return lax.all_to_all(copies, axis, split_axis=0, concat_axis=0, tiled=True)]
    all_to_all x1, starting transfers between devices: 33.6 us -> 7.96 us  [sent_and_summed(): lax.all_to_all(pieces, axis, split_axis=0, concat_axis=0, tiled=True)]
    all_to_all x0 -> x3, starting transfers between devices: none -> 15 us  [spread(): return lax.all_to_all(copies, axis, split_axis=0, concat_axis=0, tiled=True)]
    transpose x2 -> x0, local copies, waits for them, and re-layouts: 3.19 us -> none  [gather_in_order(): pieces.transpose(*turned, *range(len(sequence), pieces.ndim))]
    broadcast_in_dim x1 -> x5, local copies, waits for them, and re-layouts: 0.68 us -> 3.62 us  [the longest x4 3.54 us: spread(): jnp.broadcast_to(block[None], (count, *block.shape))]
  transfers between devices with their start and end apart: 2 -> 4, of which waited for: 1 -> 4; matrix products, arithmetic and copies ran while one was open for 7% -> 11% of each run, Pallas kernels for 0% -> 0%
where the time goes in v1:
time: 162 us
  blocking collectives  55.1 us (34%)
  waiting for transfers between devices  41.8 us (26%)
  starting transfers between devices  23 us (14%)
  local copies, waits for them, and re-layouts  17.2 us (11%)
  matrix products  15 us (9%)
  other arithmetic  7.73 us (5%)
  between operations  1.8 us (1%)
    all_to_all x1, blocking collectives, spread(): return lax.all_to_all(copies, axis, split_axis=0, concat_axis=0, tiled=True)  55.1 us
    all_to_all x3, waiting for transfers between devices, spread(): return lax.all_to_all(copies, axis, split_axis=0, concat_axis=0, tiled=True)  27.6 us
    all_to_all x3, starting transfers between devices, spread(): return lax.all_to_all(copies, axis, split_axis=0, concat_axis=0, tiled=True)  15 us
    all_to_all x1, waiting for transfers between devices, sent_and_summed(): lax.all_to_all(pieces, axis, split_axis=0, concat_axis=0, tiled=True)  14.2 us
    all_to_all x1, starting transfers between devices, sent_and_summed(): lax.all_to_all(pieces, axis, split_axis=0, concat_axis=0, tiled=True)  7.96 us
    unnamed x31, local copies, waits for them, and re-layouts  3.97 us
    broadcast_in_dim x4, local copies, waits for them, and re-layouts, spread(): jnp.broadcast_to(block[None], (count, *block.shape))  3.54 us
    concatenate x8, local copies, waits for them, and re-layouts, rotate(): jnp.concatenate([front_half * cos_vals - back_half * sin_vals, back_half...  3.39 us
  transfers between devices with their start and end apart: 4, of which 4 were waited for; matrix products, arithmetic and copies ran while one was open for 11% of the time, Pallas kernels for 0%

profile of v1, /device:TPU:1, one launch (start us, length us, event | category | flops | bytes accessed | tf_op | source)
XLA Modules:
  0.0 161.7 jit_solution(11249916639222895003)
XLA Ops:
  0.7 1.9 %convolution_convert_fusion.3 = bf16[256,64]{0,1:T(8,128)(2,1)S(1)} fusion(bf16[256,2048]{1,0:T(8,128)(2,1)} %param.10, bf16[2048,64]{0,1:T(8,128)(2,1)} %param.12), kind=kOutput, calls=%fused_computation.26 | convolution fusion | flops 67125248 | bytes 1343488 | tf_op jit(solution)/shard_map/dot_general | solution.py:94
  2.6 0.7 fusion.61
  4.1 1.7 %convolution_convert_fusion.2 = bf16[256,64]{0,1:T(8,128)(2,1)S(1)} fusion(bf16[256,2048]{1,0:T(8,128)(2,1)} %param.10, bf16[2048,64]{0,1:T(8,128)(2,1)} %param.13), kind=kOutput, calls=%fused_computation.25 | convolution fusion | flops 67125248 | bytes 1343488 | tf_op jit(solution)/shard_map/dot_general | solution.py:97
  6.2 0.1 copy.57
  6.3 0.2 fusion.60
  6.8 55.1 %all_to_all.25 = bf16[8,72,128]{2,1,0:T(8,128)(2,1)S(1)} all-to-all(bf16[8,72,128]{2,1,0:T(8,128)(2,1)S(1)} %broadcast_in_dim.124), channel_id=1, replica_groups=mesh['z_far'=8,'z_near'=4,'y'=4,'tp'=8] {'z_far'}, dimensions={0} | all-to-all | bytes 294912 | tf_op jit(solution)/shard_map/all_to_all | solution.py:21
  62.0 0.9 broadcast_in_dim.125
  62.9 7.1 %all-to-all-start.1 = ((bf16[4,8,72,128]{3,2,1,0:T(8,128)(2,1)}), bf16[4,8,72,128]{3,2,1,0:T(8,128)(2,1)S(1)}, u32[]{:S(2)}, u32[]{:S(2)}) async-start(bf16[4,8,72,128]{3,2,1,0:T(8,128)(2,1)} %broadcast_in_dim.125), calls=%async_computation.1 | async-start | bytes 1179648 | tf_op jit(solution)/shard_map/all_to_all | solution.py:21
  70.3 1.1 fusion.27
  71.7 0.6 copy.64
  72.3 0.6 copy.66
  73.0 0.6 copy.65
  73.6 1.7 %convolution_convert_fusion.1 = bf16[256,256]{1,0:T(8,128)(2,1)S(1)} fusion(bf16[256,2048]{1,0:T(8,128)(2,1)S(1)} %copy-done.1, bf16[2048,256]{1,0:T(8,128)(2,1)} %param.11), kind=kOutput, calls=%fused_computation.24 | convolution fusion | flops 268500992 | bytes 2228224 | tf_op jit(solution)/shard_map/dot_general | solution.py:91
  75.5 0.2 multiply_cosine_fusion
  75.8 0.1 concatenate.64
  75.9 0.9 copy.68
  76.8 0.1 concatenate.65
  76.9 0.9 copy.69
  77.8 0.5 fusion.100
  78.3 0.6 pad_clamp_fusion
  79.0 1.0 pad_add_fusion
  80.1 0.2 broadcast_compare_fusion
  80.3 5.1 %all-to-all-done.1 = bf16[4,8,72,128]{3,2,1,0:T(8,128)(2,1)S(1)} async-done(((bf16[4,8,72,128]{3,2,1,0:T(8,128)(2,1)}), bf16[4,8,72,128]{3,2,1,0:T(8,128)(2,1)S(1)}, u32[]{:S(2)}, u32[]{:S(2)}) %all-to-all-start.1) | async-done | bytes 589856 | tf_op jit(solution)/shard_map/all_to_all | solution.py:21
  85.4 0.8 broadcast_in_dim.126
  86.2 4.2 %all-to-all-start.2 = ((bf16[4,32,8,128]{3,2,1,0:T(8,128)(2,1)}), bf16[4,32,8,128]{3,2,1,0:T(8,128)(2,1)S(1)}, u32[]{:S(2)}, u32[]{:S(2)}) async-start(bf16[4,32,8,128]{3,2,1,0:T(8,128)(2,1)} %broadcast_in_dim.126), calls=%async_computation.2 | async-start | bytes 524288 | tf_op jit(solution)/shard_map/all_to_all | solution.py:21
  90.4 1.9 %broadcast_in_dim.132 = bf16[4,32,64,128]{3,2,1,0:T(8,128)(2,1)} broadcast(bf16[32,64,128]{2,1,0:T(8,128)(2,1)S(1)} %slice.57), dimensions={1,2,3} | broadcast | bytes 2621440 | tf_op jit(solution)/shard_map/broadcast_in_dim | solution.py:20
  92.3 3.6 %all-to-all-done.2 = bf16[4,32,8,128]{3,2,1,0:T(8,128)(2,1)S(1)} async-done(((bf16[4,32,8,128]{3,2,1,0:T(8,128)(2,1)}), bf16[4,32,8,128]{3,2,1,0:T(8,128)(2,1)S(1)}, u32[]{:S(2)}, u32[]{:S(2)}) %all-to-all-start.2) | async-done | bytes 262176 | tf_op jit(solution)/shard_map/all_to_all | solution.py:21
  95.9 0.7 copy-done.4
  96.6 3.8 %all-to-all-start.3 = ((bf16[4,32,64,128]{3,2,1,0:T(8,128)(2,1)}), bf16[4,32,64,128]{3,2,1,0:T(8,128)(2,1)S(1)}, u32[]{:S(2)}, u32[]{:S(2)}) async-start(bf16[4,32,64,128]{3,2,1,0:T(8,128)(2,1)} %broadcast_in_dim.132), calls=%async_computation.3 | async-start | bytes 4194304 | tf_op jit(solution)/shard_map/all_to_all | solution.py:21
  100.4 1.8 %fusion.3 = (f32[256,4]{0,1:T(4,128)S(1)}, f32[1024,256,4]{1,0,2:T(8,128)S(1)}) fusion(pred[256,1024]{0,1:T(8,128)(4,1)S(1)} %broadcast_compare_fusion, bf16[256,4,64]{0,2,1:T(8,128)(2,1)S(1)} %multiply_convert_fusion, bf16[1024,128]{1,0:T(8,128)(2,1)} %bitcast.179), kind=kOutput, calls=%fused_computation.8 | convolution fusion | flops 137362432 | bytes 4853760 | tf_op jit(solution)/shard_map/rghd,cgd->rghc/dot_general | solution.py:140
  102.2 0.9 fusion.6
  103.1 1.7 %fusion.28 = f32[1,64,256,4]{2,1,3,0:T(8,128)} fusion(f32[1024,256,4]{1,0,2:T(8,128)S(1)} %get-tuple-element.13, f32[256,4]{0,1:T(4,128)S(1)} %get-tuple-element.12, pred[256,1024]{0,1:T(8,128)(4,1)S(1)} %broadcast_compare_fusion, bf16[1024,128]{1,0:T(8,128)(2,1)S(1)} %bitcast.180, f32[256,4]{0,1:T(4,128)S(1)} %broadcast_select_fusion), kind=kOutput, calls=%fused_computation.32 | convolution fusion | flops 138477568 | bytes 4988928 | tf_op jit(solution)/shard_map/rghc,cgd->rghd/dot_general | solution.py:150
  104.9 18.9 %all-to-all-done.3 = bf16[4,32,64,128]{3,2,1,0:T(8,128)(2,1)S(1)} async-done(((bf16[4,32,64,128]{3,2,1,0:T(8,128)(2,1)}), bf16[4,32,64,128]{3,2,1,0:T(8,128)(2,1)S(1)}, u32[]{:S(2)}, u32[]{:S(2)}) %all-to-all-start.3) | async-done | bytes 2097184 | tf_op jit(solution)/shard_map/all_to_all | solution.py:21
  123.8 1.3 copy-done.2
  125.1 2.5 %gather_fusion = bf16[60,64,128]{2,1,0:T(8,128)(2,1)S(1)} fusion(bf16[128,64,128]{2,1,0:T(8,128)(2,1)} %bitcast.176, s32[1024]{0:T(1024)} %pad_clamp_fusion), kind=kCustom, calls=%fused_computation | custom fusion | bytes 1966320 | tf_op jit(solution)/shard_map/gather | solution.py:164
  127.6 1.3 fusion.108
  128.9 1.5 copy.82
  130.5 0.3 copy.83
  130.8 2.1 %fusion = (f32[4,64,4]{1,2,0:T(4,128)S(1)}, f32[4,1024,64,4]{1,2,3,0:T(8,128)S(1)}) fusion(pred[4,64,1024]{2,1,0:T(8,128)(4,1)S(1)} %copy-done.3, bf16[4,64,4,32]{3,1,2,0:T(8,128)(2,1)} %copy.69, bf16[4,64,4,32]{3,1,2,0:T(8,128)(2,1)} %copy.68, bf16[4,960,1,64]{1,3,0,2:T(8,128)(2,1)S(1)} %bitcast.182, bf16[4,64,1,32]{1,3,0,2:T(8,128)(2,1)S(1)} %copy-done.8, ...), kind=kOutput, calls=%fused_computation.3 | convolution fusion | flops 139197440 | bytes 5115904 | tf_op jit(solution)/shard_map/jqghd,jkgd->jqghk/dot_general | solution.py:184
  133.0 1.2 fusion.8
  134.2 1.6 fusion.34
  135.8 0.3 copy.76
  136.2 0.3 reshape.587
  136.6 1.4 convolution_convert_fusion
  138.0 8.0 %all-to-all-start.4 = ((bf16[8,32,2048]{2,1,0:T(8,128)(2,1)}), bf16[8,32,2048]{2,1,0:T(8,128)(2,1)S(1)}, u32[]{:S(2)}, u32[]{:S(2)}) async-start(bf16[8,32,2048]{2,1,0:T(8,128)(2,1)} %bitcast.36), calls=%async_computation.4 | async-start | bytes 2097152 | tf_op jit(solution)/shard_map/all_to_all | solution.py:32
  146.1 0.6 pad_maximum_fusion.1
  146.7 14.2 %all-to-all-done.4 = bf16[8,32,2048]{2,1,0:T(8,128)(2,1)S(1)} async-done(((bf16[8,32,2048]{2,1,0:T(8,128)(2,1)}), bf16[8,32,2048]{2,1,0:T(8,128)(2,1)S(1)}, u32[]{:S(2)}, u32[]{:S(2)}) %all-to-all-start.4) | async-done | bytes 1048608 | tf_op jit(solution)/shard_map/all_to_all | solution.py:32
  160.9 0.8 reduce_sum.74
  (72 shorter events, 2.0 us)
Async XLA Ops:
  0.6 135.9 %copy-start = (bf16[256,2048]{1,0:T(8,128)(2,1)S(1)}, bf16[256,2048]{1,0:T(8,128)(2,1)}, u32[]{:S(2)}) copy-start(bf16[256,2048]{1,0:T(8,128)(2,1)} %param.17) | copy-start | bytes 3145732
  0.6 69.7 %copy-start.1 = (bf16[256,2048]{1,0:T(8,128)(2,1)S(1)}, bf16[256,2048]{1,0:T(8,128)(2,1)}, u32[]{:S(2)}) copy-start(bf16[256,2048]{1,0:T(8,128)(2,1)} %param.10) | copy-start | bytes 3145732
  0.7 69.6 %copy-start.10 = (s32[4,15]{1,0:T(4,128)S(1)}, s32[4,15]{1,0:T(4,128)}, u32[]{:S(2)}) copy-start(s32[4,15]{1,0:T(4,128)} %param.19) | copy-start | bytes 724
  4.1 71.3 %copy-start.13 = (f32[64]{0:T(128)S(1)}, f32[64]{0:T(128)}, u32[]{:S(2)}) copy-start(f32[64]{0:T(128)} %param.15) | copy-start | bytes 772
  62.9 22.5 %all-to-all-start.1 = ((bf16[4,8,72,128]{3,2,1,0:T(8,128)(2,1)}), bf16[4,8,72,128]{3,2,1,0:T(8,128)(2,1)S(1)}, u32[]{:S(2)}, u32[]{:S(2)}) async-start(bf16[4,8,72,128]{3,2,1,0:T(8,128)(2,1)} %broadcast_in_dim.125), calls=%async_computation.1 | async-start | bytes 1179648 | tf_op jit(solution)/shard_map/all_to_all | solution.py:21
  86.2 9.7 %all-to-all-start.2 = ((bf16[4,32,8,128]{3,2,1,0:T(8,128)(2,1)}), bf16[4,32,8,128]{3,2,1,0:T(8,128)(2,1)S(1)}, u32[]{:S(2)}, u32[]{:S(2)}) async-start(bf16[4,32,8,128]{3,2,1,0:T(8,128)(2,1)} %broadcast_in_dim.126), calls=%async_computation.2 | async-start | bytes 524288 | tf_op jit(solution)/shard_map/all_to_all | solution.py:21
  95.9 0.7 copy-start.4
  96.6 27.2 %all-to-all-start.3 = ((bf16[4,32,64,128]{3,2,1,0:T(8,128)(2,1)}), bf16[4,32,64,128]{3,2,1,0:T(8,128)(2,1)S(1)}, u32[]{:S(2)}, u32[]{:S(2)}) async-start(bf16[4,32,64,128]{3,2,1,0:T(8,128)(2,1)} %broadcast_in_dim.132), calls=%async_computation.3 | async-start | bytes 4194304 | tf_op jit(solution)/shard_map/all_to_all | solution.py:21
  100.4 2.7 %copy-start.11 = (pred[256]{0:T(512)(128)(4,1)S(1)}, pred[256]{0:T(512)(128)(4,1)}, u32[]{:S(2)}) copy-start(pred[256]{0:T(512)(128)(4,1)} %fusion.100) | copy-start | bytes 772
  100.4 2.7 %copy-start.5 = (bf16[4,32,8,128]{3,2,1,0:T(8,128)(2,1)S(1)}, bf16[4,32,8,128]{3,2,1,0:T(8,128)(2,1)}, u32[]{:S(2)}) copy-start(bf16[4,32,8,128]{3,2,1,0:T(8,128)(2,1)} %copy-done.4) | copy-start | bytes 786436
  123.8 1.3 copy-start.2
  125.1 5.7 %copy-start.3 = (pred[4,64,1024]{2,1,0:T(8,128)(4,1)S(1)}, pred[4,64,1024]{2,1,0:T(8,128)(4,1)}, u32[]{:S(2)}) copy-start(pred[4,64,1024]{2,1,0:T(8,128)(4,1)} %pad_add_fusion) | copy-start | bytes 786436
  125.1 5.7 %copy-start.8 = (bf16[4,64,1,32]{1,3,0,2:T(8,128)(2,1)S(1)}, bf16[4,64,1,32]{1,3,0,2:T(8,128)(2,1)}, u32[]{:S(2)}) copy-start(bf16[4,64,1,32]{1,3,0,2:T(8,128)(2,1)} %copy.66) | copy-start | bytes 49156
  125.1 5.7 %copy-start.9 = (bf16[4,64,1,32]{1,3,0,2:T(8,128)(2,1)S(1)}, bf16[4,64,1,32]{1,3,0,2:T(8,128)(2,1)}, u32[]{:S(2)}) copy-start(bf16[4,64,1,32]{1,3,0,2:T(8,128)(2,1)} %copy.65) | copy-start | bytes 49156
  130.8 3.4 %copy-start.7 = (bf16[4,64,1,64]{1,3,0,2:T(8,128)(2,1)S(1)}, bf16[4,64,1,64]{1,3,0,2:T(8,128)(2,1)}, u32[]{:S(2)}) copy-start(bf16[4,64,1,64]{1,3,0,2:T(8,128)(2,1)} %copy.64) | copy-start | bytes 98308
  134.2 2.3 %copy-start.6 = (f32[1,64,256,4]{2,1,3,0:T(8,128)S(1)}, f32[1,64,256,4]{2,1,3,0:T(8,128)}, u32[]{:S(2)}) copy-start(f32[1,64,256,4]{2,1,3,0:T(8,128)} %fusion.28) | copy-start | bytes 786436
  135.8 10.2 %copy-start.12 = (pred[256]{0:T(512)(128)(4,1)S(1)}, pred[256]{0:T(512)(128)(4,1)}, u32[]{:S(2)}) copy-start(pred[256]{0:T(512)(128)(4,1)} %fusion.100) | copy-start | bytes 772
  138.0 22.9 %all-to-all-start.4 = ((bf16[8,32,2048]{2,1,0:T(8,128)(2,1)}), bf16[8,32,2048]{2,1,0:T(8,128)(2,1)S(1)}, u32[]{:S(2)}, u32[]{:S(2)}) async-start(bf16[8,32,2048]{2,1,0:T(8,128)(2,1)} %bitcast.36), calls=%async_computation.4 | async-start | bytes 2097152 | tf_op jit(solution)/shard_map/all_to_all | solution.py:32

commit v2 on v1

v2 whole, which is shorter than its diff:
```python
import jax
import jax.numpy as jnp
from jax import lax
from jax.experimental import pallas as pl
from jax.experimental.pallas import tpu as pltpu
from jax.sharding import Mesh
from jax.sharding import PartitionSpec as P

SEL = 64
CMP = 32
KV = ("z_far", "z_near", "y")
KV_TP = ("z_far", "z_near", "y", "tp")


norm_eps = 1e-06
rope_base = 500000.0
big_negative = -1e30


def spread(block, axis):
    count = lax.axis_size(axis)
    copies = lax.optimization_barrier(jnp.broadcast_to(block[None], (count, *block.shape)))
    return lax.all_to_all(copies, axis, split_axis=0, concat_axis=0, tiled=True)


def split_up(array, dim, length):
    lengths = array.shape
    pieces = array.reshape(*lengths[:dim], length, lengths[dim] // length, *lengths[dim + 1 :])
    return jnp.moveaxis(pieces, dim, 0)


def sent_and_summed(array, axis, dim):
    pieces = split_up(array, dim, lax.axis_size(axis))
    arrived = lax.all_to_all(pieces, axis, split_axis=0, concat_axis=0, tiled=True)
    return arrived.astype(jnp.float32).sum(axis=0)


def rounded(values_in):
    return lax.optimization_barrier(values_in.astype(jnp.bfloat16))


def unit_norm(values_in, gain_vec):
    upcast = values_in.astype(jnp.float32)
    return (
        upcast * lax.rsqrt(jnp.mean(upcast * upcast, axis=-1, keepdims=True) + norm_eps) * gain_vec
    )


def rotate(values_in, places):
    half_size = values_in.shape[-1] // 2
    inverse = jnp.power(
        rope_base, -jnp.arange(half_size, dtype=jnp.float32) * 2.0 / values_in.shape[-1]
    )
    angles = places.astype(jnp.float32)[:, None] * inverse[None, :]
    cos_vals = jnp.cos(angles)[:, None, :]
    sin_vals = jnp.sin(angles)[:, None, :]
    upcast = values_in.astype(jnp.float32)
    front_half = upcast[..., :half_size]
    back_half = upcast[..., half_size:]
    return jnp.concatenate(
        [
            front_half * cos_vals - back_half * sin_vals,
            back_half * cos_vals + front_half * sin_vals,
        ],
        axis=-1,
    )


def swapped(values_in):
    half_size = values_in.shape[-1] // 2
    return jnp.concatenate([values_in[:, half_size:], values_in[:, :half_size]], axis=1)


def side_by_side(rows):
    half_size = rows.shape[0] // 2
    return jnp.concatenate([rows[:half_size], rows[half_size:]], axis=1)


def dot_last(left, right):
    return lax.dot_general(
        left, right, (((1,), (1,)), ((), ())), preferred_element_type=jnp.float32
    )


def key_kernel(pick, tokens, key_weight, value_weight, gain, cosines, sines, sent, own_keys, own_values):
    copies, _, _ = sent.shape
    blocks, packed, _ = own_keys.shape
    tok_rows = tokens.shape[0]
    block_len = 2 * packed
    keys = dot_last(tokens[...], key_weight[...])
    keys = keys.astype(jnp.bfloat16).astype(jnp.float32)
    values = dot_last(tokens[...], value_weight[...]).astype(jnp.bfloat16)
    square = jnp.mean(keys * keys, axis=-1, keepdims=True)
    plain = (keys * lax.rsqrt(square + norm_eps) * gain[...]).astype(jnp.bfloat16)
    plain = plain.astype(jnp.float32)
    turned = (plain * cosines[...] + swapped(plain) * sines[...]).astype(jnp.bfloat16)
    for block in range(blocks):
        rows = slice(block * block_len, (block + 1) * block_len)
        own_keys[block] = side_by_side(turned[rows])
        own_values[block] = side_by_side(values[rows])
    both = jnp.concatenate([plain, values.astype(jnp.float32)], axis=1)
    spans = jnp.mean(both.reshape(tok_rows // CMP, CMP, both.shape[1]), axis=1).astype(jnp.bfloat16)
    shared_keys = own_keys[pick[0]]
    shared_values = own_values[pick[0]]
    for copy in range(copies):
        sent[copy, :packed] = shared_keys
        sent[copy, packed:block_len] = shared_values
        sent[copy, block_len:] = spans


def one_sided(queries, rows, upper):
    pieces = []
    lanes = lax.broadcasted_iota(jnp.int32, (rows.size, 128), 1)
    keep = (lanes >= 64) if upper else (lanes < 64)
    for pair in range(queries.shape[1] // 128):
        both = queries[rows, pair * 128 : (pair + 1) * 128].astype(jnp.float32)
        turned = swapped(both)
        for piece in (turned, both) if upper else (both, turned):
            pieces.append(jnp.where(keep, piece, 0.0).astype(jnp.bfloat16))
    return jnp.concatenate(pieces, axis=0)


def score_kernel(
    starts,
    origin,
    blocked,
    span_ends,
    arrived,
    own_keys,
    q_plain,
    q_turned,
    gates,
    weights,
    mixed_spans,
    factors,
    logs,
    chosen_keys,
    spans,
):
    blocks, packed, _ = own_keys.shape
    y_count, arrived_rows, _ = arrived.shape
    block_len = 2 * packed
    heads = q_plain.shape[1] // 64
    named = starts.shape[0] // blocks
    span_rows = spans.shape[0] // y_count
    score_scale = 64 ** (-0.5)
    for place in range(y_count):
        spans[place * span_rows : (place + 1) * span_rows] = arrived[
            place, arrived_rows - span_rows :
        ]
    row_place = lax.broadcasted_iota(jnp.int32, (heads * block_len, 1), 0) % block_len

    @pl.loop(0, blocks)
    def _(block):
        rows = pl.ds(pl.multiple_of(block * block_len, block_len), block_len)
        gate_rows = gates[rows, :]
        gate_of = [
            jnp.concatenate(
                [gate_rows[:, 2 * head + b : 2 * head + b + 1] for head in range(heads)], axis=0
            )
            for b in range(2)
        ]
        scores = dot_last(one_sided(q_plain, rows, False), spans[...])
        places = origin[0] + block * block_len + row_place
        has_span = places >= CMP - 1
        scores = jnp.where(span_ends[...] <= places, scores * score_scale, big_negative)
        peak = jnp.max(scores, axis=-1, keepdims=True)
        raw = jnp.exp(scores - peak)
        total = jnp.where(has_span, jnp.sum(raw, axis=-1, keepdims=True), 1.0)
        summed = jnp.dot(raw.astype(jnp.bfloat16), spans[...], preferred_element_type=jnp.float32)
        summed = jnp.where(has_span, gate_of[0] * (summed[:, 64:] / total), 0.0)
        span_log = jnp.where(has_span, peak + jnp.log(total), 0.0)
        for pair in range(heads // 2):
            first = slice(2 * pair * block_len, (2 * pair + 1) * block_len)
            second = slice((2 * pair + 1) * block_len, (2 * pair + 2) * block_len)
            mixed_spans[rows, pair * 128 : (pair + 1) * 128] = jnp.concatenate(
                [summed[first], summed[second]], axis=1
            )
        chosen_keys[:packed] = own_keys[block]
        for number in range(named):
            start = pl.multiple_of(starts[block * named + number], packed)
            place = start // arrived_rows
            chosen_keys[(number + 1) * packed : (number + 2) * packed] = arrived[
                place, pl.ds(pl.multiple_of(start - place * arrived_rows, packed), packed)
            ]
        half_scores = []
        lanes = lax.broadcasted_iota(jnp.int32, (heads * block_len, chosen_keys.shape[0]), 1)
        for upper in (False, True):
            scores = dot_last(one_sided(q_turned, rows, upper), chosen_keys[...])
            scores = scores * score_scale + blocked[block]
            later = (lanes < packed) & (lanes + packed * upper > row_place)
            half_scores.append(jnp.where(later, big_negative, scores))
        peak = jnp.maximum(
            jnp.max(half_scores[0], axis=-1, keepdims=True),
            jnp.max(half_scores[1], axis=-1, keepdims=True),
        )
        total = 0.0
        for upper in range(2):
            raw = jnp.exp(half_scores[upper] - peak)
            total = total + jnp.sum(raw, axis=-1, keepdims=True)
            weights[block, upper] = raw.astype(jnp.bfloat16)
        factors[block] = jnp.broadcast_to(gate_of[1] / total, factors.shape[1:])
        chosen_log = peak + jnp.log(total)
        for head in range(heads):
            piece = slice(head * block_len, (head + 1) * block_len)
            logs[0, rows, head : head + 1] = span_log[piece]
            logs[1, rows, head : head + 1] = chosen_log[piece]


def mix_kernel(starts, arrived, own_values, weights, mixed_spans, factors, mixed, chosen_values):
    blocks, packed, _ = own_values.shape
    block_len = 2 * packed
    named = starts.shape[0] // blocks
    heads = factors.shape[1] // block_len

    @pl.loop(0, blocks)
    def _(block):
        rows = pl.ds(pl.multiple_of(block * block_len, block_len), block_len)
        chosen_values[:packed] = own_values[block]
        for number in range(named):
            start = pl.multiple_of(starts[block * named + number], packed)
            chosen_values[(number + 1) * packed : (number + 2) * packed] = arrived[
                pl.ds(start, packed)
            ]
        lower, upper = (
            jnp.dot(weights[block, half], chosen_values[...], preferred_element_type=jnp.float32)
            for half in range(2)
        )
        summed = (lower + swapped(upper)) * factors[block]
        for pair in range(heads // 2):
            first = summed[2 * pair * block_len : (2 * pair + 1) * block_len, :64]
            second = summed[(2 * pair + 1) * block_len : (2 * pair + 2) * block_len, :64]
            lane_range = slice(pair * 128, (pair + 1) * 128)
            mixed[rows, lane_range] = (
                mixed_spans[rows, lane_range] + jnp.concatenate([first, second], axis=1)
            ).astype(jnp.bfloat16)


def in_vmem(kernel, scalars, arrays, outputs, scratch, flops, room):
    return pl.pallas_call(
        kernel,
        out_shape=outputs,
        in_specs=[pl.BlockSpec(memory_space=pltpu.SMEM)] * len(scalars)
        + [pl.BlockSpec(memory_space=pltpu.VMEM)] * len(arrays),
        out_specs=jax.tree.map(lambda _: pl.BlockSpec(memory_space=pltpu.VMEM), outputs),
        scratch_shapes=scratch,
        cost_estimate=pl.CostEstimate(flops=flops, bytes_accessed=4 << 20, transcendentals=0),
        compiler_params=pltpu.CompilerParams(vmem_limit_bytes=room << 20),
    )(*scalars, *arrays)


def turns(places, head_size):
    half_size = head_size // 2
    inverse = jnp.power(rope_base, -jnp.arange(half_size, dtype=jnp.float32) * 2.0 / head_size)
    angles = places.astype(jnp.float32)[:, None] * inverse[None, :]
    return jnp.cos(angles), jnp.sin(angles)


def shards(
    tokens,
    query_weight,
    key_weight,
    value_weight,
    gate_weight,
    query_gain,
    key_gain,
    out_weight,
    shared_block,
    chosen_device,
):
    tok_rows = tokens.shape[0]
    head_size = query_gain.shape[0]
    head_count = query_weight.shape[1] // head_size
    block_len = SEL
    packed = block_len // 2
    local_blocks = tok_rows // block_len
    device = lax.axis_index(KV)
    tp_index = lax.axis_index("tp")
    places = device * tok_rows + jnp.arange(tok_rows, dtype=jnp.int32)
    far_count, near_count, y_count = (lax.axis_size(axis) for axis in KV)
    column_count = far_count * near_count
    span_count = tok_rows // CMP
    cos_vals, sin_vals = turns(places, head_size)

    packed_blocks = jax.ShapeDtypeStruct((local_blocks, packed, 2 * head_size), jnp.bfloat16)
    sent, own_keys, own_values = in_vmem(
        key_kernel,
        (shared_block,),
        (
            tokens,
            key_weight.T,
            value_weight.T,
            key_gain[None],
            jnp.concatenate([cos_vals, cos_vals], axis=1),
            jnp.concatenate([-sin_vals, sin_vals], axis=1),
        ),
        (
            jax.ShapeDtypeStruct(
                (far_count, block_len + span_count, 2 * head_size), jnp.bfloat16
            ),
            packed_blocks,
            packed_blocks,
        ),
        (),
        10**9,
        8,
    )
    far = lax.all_to_all(sent, "z_far", split_axis=0, concat_axis=0, tiled=True)
    column = spread(far, "z_near").reshape(column_count, block_len + span_count, 2 * head_size)
    first_part = jnp.concatenate(
        [
            column[:, :packed].reshape(-1, 2 * head_size),
            column[:, block_len:].reshape(-1, 2 * head_size),
        ],
        axis=0,
    )
    arrived_keys = spread(first_part, "y")
    arrived_values = spread(column[:, packed:block_len].reshape(-1, 2 * head_size), "y")
    arrived_values = arrived_values.reshape(-1, 2 * head_size)

    queries = rounded(jnp.dot(tokens, query_weight, preferred_element_type=jnp.float32)).reshape(
        tok_rows, head_count, head_size
    )
    q_plain = rounded(unit_norm(queries, query_gain))
    q_turned = rotate(q_plain, places).astype(jnp.bfloat16)
    gate_cols = lax.dynamic_slice_in_dim(gate_weight, tp_index * 2 * head_count, 2 * head_count, 1)
    gate_vals = jax.nn.sigmoid(jnp.dot(tokens, gate_cols, preferred_element_type=jnp.float32))

    span_index = jnp.arange(y_count * column_count * span_count, dtype=jnp.int32)
    slot_of = span_index // span_count
    owner = (
        (slot_of % far_count) * near_count + slot_of // far_count % near_count
    ) * y_count + slot_of // column_count
    span_ends = owner * tok_rows + span_index % span_count * CMP + CMP - 1
    in_column = chosen_device // y_count % near_count * far_count + chosen_device // (
        y_count * near_count
    )
    place = chosen_device % y_count
    key_starts = (place * first_part.shape[0] + in_column * packed).reshape(-1)
    value_starts = ((place * column_count + in_column) * packed).reshape(-1)
    counted = jnp.concatenate(
        [jnp.ones((local_blocks, 1), jnp.bool_), chosen_device < device], axis=1
    )
    blocked = jnp.repeat(jnp.where(counted, 0.0, big_negative), packed, axis=1)[:, None, :]
    chosen_rows = blocked.shape[2]

    weights, mixed_spans, factors, log_weight = in_vmem(
        score_kernel,
        (key_starts, (device * tok_rows)[None]),
        (
            blocked,
            span_ends[None],
            arrived_keys,
            own_keys,
            q_plain.reshape(tok_rows, head_count * head_size),
            q_turned.reshape(tok_rows, head_count * head_size),
            gate_vals,
        ),
        (
            jax.ShapeDtypeStruct(
                (local_blocks, 2, head_count * block_len, chosen_rows), jnp.bfloat16
            ),
            jax.ShapeDtypeStruct((tok_rows, head_count * head_size), jnp.float32),
            jax.ShapeDtypeStruct(
                (local_blocks, head_count * block_len, 2 * head_size), jnp.float32
            ),
            jax.ShapeDtypeStruct((2, tok_rows, head_count), jnp.float32),
        ),
        (
            pltpu.VMEM((chosen_rows, 2 * head_size), jnp.bfloat16),
            pltpu.VMEM((span_ends.shape[0], 2 * head_size), jnp.bfloat16),
        ),
        4 * 10**9,
        16,
    )
    mixed_heads = in_vmem(
        mix_kernel,
        (value_starts,),
        (arrived_values, own_values, weights, mixed_spans, factors),
        jax.ShapeDtypeStruct((tok_rows, head_count * head_size), jnp.bfloat16),
        (pltpu.VMEM((chosen_rows, 2 * head_size), jnp.bfloat16),),
        10**9,
        10,
    )
    mixed_out = sent_and_summed(
        jnp.dot(mixed_heads, out_weight, preferred_element_type=jnp.float32).astype(jnp.bfloat16),
        "tp",
        0,
    ).astype(jnp.bfloat16)
    return (mixed_out, log_weight)


def solution(mesh):
    torus = Mesh(mesh.devices.reshape(8, 4, 4, mesh.shape["tp"]), KV_TP)
    return jax.shard_map(
        shards,
        mesh=torus,
        in_specs=(
            P(KV, None),
            P(None, "tp"),
            P(None, "tp"),
            P(None, "tp"),
            P(),
            P(),
            P(),
            P("tp", None),
            P(KV),
            P(KV, None),
        ),
        out_specs=(P(KV_TP, None), P(None, KV, "tp")),
        check_vma=False,
    )
```

time: 162 us -> 161 us (level)
  matrix products: 15 us -> 4.77 us
  Pallas kernels: 0 us -> 8.39 us
  local copies, waits for them, and re-layouts: 17.2 us -> 24.5 us
  other arithmetic: 7.73 us -> 3.08 us
    unnamed x31 -> x45, local copies, waits for them, and re-layouts: 3.97 us -> 15.9 us
    dot_general x6 -> x0, matrix products: 10.8 us -> none  [the longest x1 2.15 us: shards(): jnp.einsum('jqghd,jkgd->jqghk', q_blocks, key_rows, preferred_element_typ...]
    pallas_call x0 -> x3, Pallas kernels: none -> 8.39 us  [in_vmem(): pl.pallas_call(kernel, out_shape=outputs, in_specs=[pl.BlockSpec(memory_s...]
    concatenate x10 -> x0, local copies, waits for them, and re-layouts: 3.6 us -> none  [the longest x8 3.39 us: rotate(): jnp.concatenate([front_half * cos_vals - back_half * sin_vals, back_half...]
    gather x1 -> x0, local copies, waits for them, and re-layouts: 2.49 us -> none  [shards(): all_shared[slots]]
    reduce_sum x4 -> x0, other arithmetic: 2.18 us -> none  [the longest x1 1.23 us: shards(): sum_sel = jnp.sum(weights_sel, axis=-1)]
    broadcast_in_dim x4 -> x3, local copies, waits for them, and re-layouts: 3.54 us -> 3.27 us  [spread(): jnp.broadcast_to(block[None], (count, *block.shape))]
  transfers between devices with their start and end apart: 4 -> 4, of which waited for: 4 -> 3; matrix products, arithmetic and copies ran while one was open for 11% -> 7% of each run, Pallas kernels for 0% -> 3%
where the time goes in v2:
time: 161 us; the launch traced here: 160 us
  blocking collectives  55.2 us (34%)
  waiting for transfers between devices  40.8 us (25%)
  local copies, waits for them, and re-layouts  24.5 us (15%)
  starting transfers between devices  21.7 us (13%)
  Pallas kernels  8.39 us (5%)
  matrix products  4.77 us (3%)
  other arithmetic  3.08 us (2%)
    all_to_all x1, blocking collectives, shards(): far = lax.all_to_all(sent, 'z_far', split_axis=0, concat_axis=0, tiled=True)  55.2 us
    all_to_all x3, waiting for transfers between devices, spread(): return lax.all_to_all(copies, axis, split_axis=0, concat_axis=0, tiled=True)  26.6 us
    unnamed x45, local copies, waits for them, and re-layouts  15.9 us
    all_to_all x3, starting transfers between devices, spread(): return lax.all_to_all(copies, axis, split_axis=0, concat_axis=0, tiled=True)  14.9 us
    all_to_all x1, waiting for transfers between devices, sent_and_summed(): lax.all_to_all(pieces, axis, split_axis=0, concat_axis=0, tiled=True)  14.3 us
    pallas_call x3, Pallas kernels, in_vmem(): pl.pallas_call(kernel, out_shape=outputs, in_specs=[pl.BlockSpec(memory_s...  8.39 us
    all_to_all x1, starting transfers between devices, sent_and_summed(): lax.all_to_all(pieces, axis, split_axis=0, concat_axis=0, tiled=True)  6.82 us
    broadcast_in_dim x3, local copies, waits for them, and re-layouts, spread(): jnp.broadcast_to(block[None], (count, *block.shape))  3.27 us
  transfers between devices with their start and end apart: 4, of which 3 were waited for; matrix products, arithmetic and copies ran while one was open for 7% of the time, Pallas kernels for 3%

profile of v2, /device:TPU:1, one launch (start us, length us, event | category | flops | bytes accessed | tf_op | source)
XLA Modules:
  0.0 160.1 jit_solution(15138241050760437175)
XLA Ops:
  1.4 0.5 fusion.4
  2.0 0.1 pad_maximum_fusion.1
  2.1 1.2 copy-done.3
  3.3 0.9 copy-done.14
  4.3 0.9 copy-done.15
  5.2 0.7 copy-done.16
  5.9 0.9 shard_map.113
  6.8 0.6 copy-done.12
  7.4 0.6 copy-done.17
  8.0 55.2 %all_to_all.25 = bf16[8,72,128]{2,1,0:T(8,128)(2,1)S(1)} all-to-all(bf16[8,72,128]{2,1,0:T(8,128)(2,1)S(1)} %get-tuple-element.9), channel_id=1, replica_groups=mesh['z_far'=8,'z_near'=4,'y'=4,'tp'=8] {'z_far'}, dimensions={0} | all-to-all | bytes 294912 | tf_op jit(solution)/shard_map/all_to_all | solution.py:308
  63.3 0.9 broadcast_in_dim.21
  64.2 7.2 %all-to-all-start.1 = ((bf16[4,8,72,128]{3,2,1,0:T(8,128)(2,1)}), bf16[4,8,72,128]{3,2,1,0:T(8,128)(2,1)S(1)}, u32[]{:S(2)}, u32[]{:S(2)}) async-start(bf16[4,8,72,128]{3,2,1,0:T(8,128)(2,1)} %broadcast_in_dim.21), calls=%async_computation.1 | async-start | bytes 1179648 | tf_op jit(solution)/shard_map/all_to_all | solution.py:23
  71.5 1.7 %convolution_convert_fusion.1 = bf16[256,256]{1,0:T(8,128)(2,1)S(1)} fusion(bf16[256,2048]{1,0:T(8,128)(2,1)S(1)} %copy-done.4, bf16[2048,256]{1,0:T(8,128)(2,1)} %param.11), kind=kOutput, calls=%fused_computation.1 | convolution fusion | flops 268500992 | bytes 2228224 | tf_op jit(solution)/shard_map/dot_general | solution.py:321
  73.2 0.1 copy.22
  73.3 0.1 multiply_convert_fusion
  73.5 0.6 copy-done.19
  74.1 12.7 %all-to-all-done.1 = bf16[4,8,72,128]{3,2,1,0:T(8,128)(2,1)S(1)} async-done(((bf16[4,8,72,128]{3,2,1,0:T(8,128)(2,1)}), bf16[4,8,72,128]{3,2,1,0:T(8,128)(2,1)S(1)}, u32[]{:S(2)}, u32[]{:S(2)}) %all-to-all-start.1) | async-done | bytes 589856 | tf_op jit(solution)/shard_map/all_to_all | solution.py:23
  86.9 1.3 broadcast_in_dim.53
  88.2 4.2 %all-to-all-start.3 = ((bf16[4,1280,128]{2,1,0:T(8,128)(2,1)}), bf16[4,1280,128]{2,1,0:T(8,128)(2,1)S(1)}, u32[]{:S(2)}, u32[]{:S(2)}) async-start(bf16[4,1280,128]{2,1,0:T(8,128)(2,1)} %broadcast_in_dim.53), calls=%async_computation.3 | async-start | bytes 2621440 | tf_op jit(solution)/shard_map/all_to_all | solution.py:23
  92.4 0.7 pad_maximum_fusion.3
  93.1 0.6 add_multiply_fusion
  93.7 1.1 broadcast_in_dim.25
  94.8 13.9 %all-to-all-done.3.arrived = bf16[4,1280,128]{2,1,0:T(8,128)(2,1)S(1)} async-done(((bf16[4,1280,128]{2,1,0:T(8,128)(2,1)}), bf16[4,1280,128]{2,1,0:T(8,128)(2,1)S(1)}, u32[]{:S(2)}, u32[]{:S(2)}) %all-to-all-start.3) | async-done | bytes 1310752 | tf_op jit(solution)/shard_map/all_to_all | solution.py:23
  108.7 3.5 %all-to-all-start.2 = ((bf16[4,1024,128]{2,1,0:T(8,128)(2,1)}), bf16[4,1024,128]{2,1,0:T(8,128)(2,1)S(1)}, u32[]{:S(2)}, u32[]{:S(2)}) async-start(bf16[4,1024,128]{2,1,0:T(8,128)(2,1)} %broadcast_in_dim.25), calls=%async_computation.2 | async-start | bytes 2097152 | tf_op jit(solution)/shard_map/all_to_all | solution.py:23
  112.3 1.0 copy.29.q_turned
  113.3 0.7 broadcast_in_dim.52
  114.0 0.8 broadcast_in_dim_reshape.4.blocked
  114.8 1.7 %copy.28.q_plain = bf16[256,256]{1,0:T(8,128)(2,1)} copy(bf16[256,256]{0,1:T(8,128)(2,1)} %bitcast.29) | data formatting | bytes 262144 | tf_op jit(solution)/shard_map/reshape | solution.py:355
  116.5 0.1 reshape.307.starts
  116.6 0.8 reshape.304.starts
  117.4 1.7 %fusion.3.gates = f32[256,8]{1,0:T(8,128)S(1)} fusion(bf16[256,2048]{1,0:T(8,128)(2,1)} %tokens.1, bf16[2048,64]{0,1:T(8,128)(2,1)} %param.14, s32[]{:T(128)S(6)} %select_n.104), kind=kOutput, calls=%fused_computation.6 | convolution fusion | flops 8394752 | bytes 1089540 | tf_op jit(solution)/shard_map/dot_general | solution.py:327
  119.1 0.9 copy-done.11
  120.0 0.8 copy-done.18
  120.7 5.4 %shard_map.114 = (bf16[4,2,256,512]{3,2,1,0:T(8,128)(2,1)S(1)}, f32[256,256]{1,0:T(8,128)S(1)}, f32[4,256,128]{2,1,0:T(8,128)S(1)}, f32[2,256,4]{2,1,0:T(8,128)S(1)}) custom-call(s32[60]{0:T(128)S(1)} %reshape.307.starts, s32[1]{0:T(128)} %bitcast.6.origin, f32[4,1,512]{2,1,0:T(1,128)S(1)} %broadcast_in_dim_reshape.4.blocked, ...), custom_call_target="tpu_custom_call" | custom-call | flops 4000000000 | bytes 4194304 | tf_op jit(solution)/shard_map/pallas_call | solution.py:240
  126.1 1.4 copy-done.1
  127.5 0.8 copy-done.5
  128.3 0.7 copy-done.7
  129.0 0.7 copy-done.9
  129.7 1.6 copy-done.2
  131.3 1.0 copy-done.6
  132.3 0.9 copy-done.8
  133.2 0.8 copy-done.13
  134.0 2.1 %shard_map.115 = bf16[256,256]{1,0:T(8,128)(2,1)S(1)} custom-call(s32[60]{0:T(128)S(1)} %reshape.304.starts, bf16[4096,128]{1,0:T(8,128)(2,1)S(1)} %bitcast.23, bf16[4,32,128]{2,1,0:T(8,128)(2,1)S(1)} %copy-done.13, bf16[4,2,256,512]{3,2,1,0:T(8,128)(2,1)S(1)} %copy-done.2, f32[256,256]{1,0:T(8,128)S(1)} %copy-done.8, f32[4,256,128]{2,1,0:T(8,128)S(1)} %copy-done.6), custom_call_target="tpu_custom_call" | custom-call | flops 1000000000 | bytes 4194304 | tf_op jit(solution)/shard_map/pallas_call | solution.py:240
  136.1 1.4 convolution_convert_fusion
  137.5 6.8 %all-to-all-start.4 = ((bf16[8,32,2048]{2,1,0:T(8,128)(2,1)}), bf16[8,32,2048]{2,1,0:T(8,128)(2,1)S(1)}, u32[]{:S(2)}, u32[]{:S(2)}) async-start(bf16[8,32,2048]{2,1,0:T(8,128)(2,1)} %bitcast.13), calls=%async_computation.4 | async-start | bytes 2097152 | tf_op jit(solution)/shard_map/all_to_all | solution.py:34
  144.3 0.7 copy.30
  145.1 14.3 %all-to-all-done.4 = bf16[8,32,2048]{2,1,0:T(8,128)(2,1)S(1)} async-done(((bf16[8,32,2048]{2,1,0:T(8,128)(2,1)}), bf16[8,32,2048]{2,1,0:T(8,128)(2,1)S(1)}, u32[]{:S(2)}, u32[]{:S(2)}) %all-to-all-start.4) | async-done | bytes 1048608 | tf_op jit(solution)/shard_map/all_to_all | solution.py:34
  159.3 0.8 reduce_sum.22
  (43 shorter events, 0.5 us)
Async XLA Ops:
  0.6 135.4 %copy-start = (bf16[256,2048]{1,0:T(8,128)(2,1)S(1)}, bf16[256,2048]{1,0:T(8,128)(2,1)}, u32[]{:S(2)}) copy-start(bf16[256,2048]{1,0:T(8,128)(2,1)} %param.17) | copy-start | bytes 3145732
  2.1 1.2 copy-start.3
  3.3 0.9 copy-start.14
  4.3 0.9 copy-start.15
  5.2 0.7 copy-start.16
  6.8 0.6 copy-start.12
  7.4 0.6 copy-start.17
  8.0 63.5 %copy-start.4 = (bf16[256,2048]{1,0:T(8,128)(2,1)S(1)}, bf16[256,2048]{1,0:T(8,128)(2,1)}, u32[]{:S(2)}) copy-start(bf16[256,2048]{1,0:T(8,128)(2,1)} %tokens.1) | copy-start | bytes 3145732
  64.2 9.2 %copy-start.21 = (f32[64]{0:T(128)S(1)}, f32[64]{0:T(128)}, u32[]{:S(2)}) copy-start(f32[64]{0:T(128)} %param.15) | copy-start | bytes 772
  64.2 22.6 %all-to-all-start.1 = ((bf16[4,8,72,128]{3,2,1,0:T(8,128)(2,1)}), bf16[4,8,72,128]{3,2,1,0:T(8,128)(2,1)S(1)}, u32[]{:S(2)}, u32[]{:S(2)}) async-start(bf16[4,8,72,128]{3,2,1,0:T(8,128)(2,1)} %broadcast_in_dim.21), calls=%async_computation.1 | async-start | bytes 1179648 | tf_op jit(solution)/shard_map/all_to_all | solution.py:23
  73.4 0.7 copy-start.19
  86.9 6.2 %copy-start.20 = (s32[4,15]{1,0:T(4,128)S(1)}, s32[4,15]{1,0:T(4,128)}, u32[]{:S(2)}) copy-start(s32[4,15]{1,0:T(4,128)} %param.19) | copy-start | bytes 724
  88.2 20.5 %all-to-all-start.3 = ((bf16[4,1280,128]{2,1,0:T(8,128)(2,1)}), bf16[4,1280,128]{2,1,0:T(8,128)(2,1)S(1)}, u32[]{:S(2)}, u32[]{:S(2)}) async-start(bf16[4,1280,128]{2,1,0:T(8,128)(2,1)} %broadcast_in_dim.53), calls=%async_computation.3 | async-start | bytes 2621440 | tf_op jit(solution)/shard_map/all_to_all | solution.py:23
  108.7 21.0 %all-to-all-start.2 = ((bf16[4,1024,128]{2,1,0:T(8,128)(2,1)}), bf16[4,1024,128]{2,1,0:T(8,128)(2,1)S(1)}, u32[]{:S(2)}, u32[]{:S(2)}) async-start(bf16[4,1024,128]{2,1,0:T(8,128)(2,1)} %broadcast_in_dim.25), calls=%async_computation.2 | async-start | bytes 2097152 | tf_op jit(solution)/shard_map/all_to_all | solution.py:23
  119.1 0.9 copy-start.11
  120.0 0.8 copy-start.18
  126.1 1.4 copy-start.1
  127.5 0.8 copy-start.5
  128.3 0.7 copy-start.7
  129.0 0.7 copy-start.9
  129.7 1.6 copy-start.2
  131.3 1.0 copy-start.6
  132.3 0.9 copy-start.8
  133.2 0.8 copy-start.13
  136.1 8.3 %copy-start.10 = (f32[2,256,4]{2,1,0:T(8,128)S(1)}, f32[2,256,4]{2,1,0:T(8,128)}, u32[]{:S(2)}) copy-start(f32[2,256,4]{2,1,0:T(8,128)} %copy-done.9) | copy-start | bytes 24580
  137.5 21.8 %all-to-all-start.4 = ((bf16[8,32,2048]{2,1,0:T(8,128)(2,1)}), bf16[8,32,2048]{2,1,0:T(8,128)(2,1)S(1)}, u32[]{:S(2)}, u32[]{:S(2)}) async-start(bf16[8,32,2048]{2,1,0:T(8,128)(2,1)} %bitcast.13), calls=%async_computation.4 | async-start | bytes 2097152 | tf_op jit(solution)/shard_map/all_to_all | solution.py:34

commit v3 on v2

v3 whole, which is shorter than its diff:
```python
import jax
import jax.numpy as jnp
from jax import lax
from jax.experimental import pallas as pl
from jax.experimental.pallas import tpu as pltpu
from jax.sharding import Mesh
from jax.sharding import PartitionSpec as P

SEL = 64
CMP = 32
KV = ("z", "y")
TP = ("x", "core")
KEY_ROOM = 60
QUERY_ROOM = 60
ATTENTION_ROOM = 12


norm_eps = 1e-06
rope_base = 500000.0
big_negative = -1e30


def spread(block, axis):
    count = lax.axis_size(axis)
    copies = lax.optimization_barrier(jnp.broadcast_to(block[None], (count, *block.shape)))
    return lax.all_to_all(copies, axis, split_axis=0, concat_axis=0, tiled=True)


def swapped(values_in):
    half_size = values_in.shape[-1] // 2
    return jnp.concatenate([values_in[:, half_size:], values_in[:, :half_size]], axis=1)


def side_by_side(rows):
    half_size = rows.shape[0] // 2
    return jnp.concatenate([rows[:half_size], rows[half_size:]], axis=1)


def dot_last(left, right):
    return lax.dot_general(
        left, right, (((1,), (1,)), ((), ())), preferred_element_type=jnp.float32
    )


def key_kernel(pick, tokens, key_weight, value_weight, gain, cosines, sines, sent, own):
    _, blocks, packed, _ = own.shape
    tok_rows = tokens.shape[0]
    block_len = 2 * packed
    keys = dot_last(tokens[...], key_weight[...])
    keys = keys.astype(jnp.bfloat16).astype(jnp.float32)
    values = dot_last(tokens[...], value_weight[...]).astype(jnp.bfloat16)
    square = jnp.mean(keys * keys, axis=-1, keepdims=True)
    plain = (keys * lax.rsqrt(square + norm_eps) * gain[...]).astype(jnp.bfloat16)
    plain = plain.astype(jnp.float32)
    turned = plain * cosines[:, :64] + swapped(plain) * sines[:, :64]
    turned = turned.astype(jnp.bfloat16)
    for block in range(blocks):
        rows = slice(block * block_len, (block + 1) * block_len)
        own[0, block] = side_by_side(turned[rows])
        own[1, block] = side_by_side(values[rows])
    both = jnp.concatenate([plain, values.astype(jnp.float32)], axis=1)
    spans = jnp.mean(both.reshape(tok_rows // CMP, CMP, both.shape[1]), axis=1)
    sent[:packed] = own[0, pick[0]]
    sent[packed:block_len] = own[1, pick[0]]
    sent[block_len:] = spans.astype(jnp.bfloat16)


def query_kernel(group, tokens, query_weight, gate_weight, gain, cosines, sines, ready, gates):
    tok_rows = tokens.shape[0]
    width = query_weight.shape[1]
    gate_count = gates.shape[1]
    start = pl.multiple_of(group[0] * gate_count, gate_count)
    gates[...] = jax.nn.sigmoid(
        dot_last(tokens[...], gate_weight[pl.ds(start, gate_count), :].astype(jnp.bfloat16))
    )
    lanes = lax.broadcasted_iota(jnp.int32, (tok_rows, 128), 1)
    for pair in range(width // 128):
        queries = jnp.dot(
            tokens[...],
            query_weight[:, pair * 128 : (pair + 1) * 128],
            preferred_element_type=jnp.float32,
        )
        queries = queries.astype(jnp.bfloat16).astype(jnp.float32)
        squares = queries * queries
        first = jnp.sum(jnp.where(lanes < 64, squares, 0.0), axis=-1, keepdims=True)
        second = jnp.sum(jnp.where(lanes < 64, 0.0, squares), axis=-1, keepdims=True)
        square = jnp.where(lanes < 64, first, second) * (1.0 / 64)
        plain = (queries * lax.rsqrt(square + norm_eps) * gain[...]).astype(jnp.bfloat16)
        ready[0, pair] = plain
        plain = plain.astype(jnp.float32)
        partner = jnp.where(
            lanes % 64 < 32, pltpu.roll(plain, 96, axis=1), pltpu.roll(plain, 32, axis=1)
        )
        turned = plain * cosines[...] + partner * sines[...]
        ready[1, pair] = turned.astype(jnp.bfloat16)


def one_sided(queries, upper):
    pieces = []
    lanes = lax.broadcasted_iota(jnp.int32, queries[0].shape, 1)
    keep = (lanes >= 64) if upper else (lanes < 64)
    for both in queries:
        both = both.astype(jnp.float32)
        turned = swapped(both)
        for piece in (turned, both) if upper else (both, turned):
            pieces.append(jnp.where(keep, piece, 0.0).astype(jnp.bfloat16))
    return jnp.concatenate(pieces, axis=0)


def attention_kernel(
    place_of,
    chosen,
    arrived,
    ready_far,
    gates_far,
    own_far,
    kept,
    given,
    logs,
    ready,
    gates,
    own,
    chosen_rows,
    spans,
    semaphores,
):
    device, core = place_of[0], place_of[1]
    blocks, named = chosen.shape
    _, _, packed, _ = own.shape
    y_count, z_count, sent_rows, _ = arrived.shape
    block_len = 2 * packed
    pairs = ready.shape[1]
    heads = 2 * pairs
    tok_rows = blocks * block_len
    span_rows = sent_rows - block_len
    score_scale = 64 ** (-0.5)
    loads = [
        pltpu.make_async_copy(far, near, semaphores.at[number])
        for number, (far, near) in enumerate(
            ((ready_far, ready), (gates_far, gates), (own_far, own))
        )
    ]
    for load in loads:
        load.start()
    column_rows = z_count * span_rows
    for y in range(y_count):
        column = arrived[y, :, block_len:, :].astype(jnp.float32)
        spans[y * column_rows : (y + 1) * column_rows] = column.reshape(column_rows, 128).astype(
            jnp.bfloat16
        )
    for load in loads:
        load.wait()
    row_place = lax.broadcasted_iota(jnp.int32, (heads * block_len, 1), 0) % block_len
    span_index = lax.broadcasted_iota(jnp.int32, (1, y_count * column_rows), 1)
    owner = span_index % column_rows // span_rows * y_count + span_index // column_rows
    span_ends = owner * tok_rows + span_index % span_rows * CMP + CMP - 1
    rank = lax.broadcasted_iota(jnp.int32, (1, chosen_rows.shape[1]), 1) // packed

    @pl.loop(0, blocks)
    def _(block):
        rows = pl.ds(pl.multiple_of(block * block_len, block_len), block_len)
        gate_rows = gates[rows, :]
        gate_of = [
            jnp.concatenate(
                [gate_rows[:, 2 * head + b : 2 * head + b + 1] for head in range(heads)], axis=0
            )
            for b in range(2)
        ]
        scores = dot_last(
            one_sided([ready[0, pair, rows, :] for pair in range(pairs)], False), spans[...]
        )
        places = device * tok_rows + block * block_len + row_place
        has_span = places >= CMP - 1
        scores = jnp.where(span_ends <= places, scores * score_scale, big_negative)
        peak = jnp.max(scores, axis=-1, keepdims=True)
        raw = jnp.exp(scores - peak)
        total = jnp.where(has_span, jnp.sum(raw, axis=-1, keepdims=True), 1.0)
        summed = jnp.dot(raw.astype(jnp.bfloat16), spans[...], preferred_element_type=jnp.float32)
        mixed_spans = jnp.where(has_span, gate_of[0] * (summed[:, 64:] / total), 0.0)
        span_log = jnp.where(has_span, peak + jnp.log(total), 0.0)

        blocked = jnp.zeros(rank.shape, jnp.float32)
        for part in range(2):
            chosen_rows[part, :packed] = own[part, block]
        for number in range(named):
            source = chosen[block, number]
            z, y = source // y_count, source % y_count
            for part in range(2):
                chosen_rows[part, (number + 1) * packed : (number + 2) * packed] = arrived[
                    y, z, part * packed : (part + 1) * packed, :
                ]
            bias = jnp.where(source < device, 0.0, big_negative)
            blocked = jnp.where(rank == number + 1, bias, blocked)
        half_scores = []
        lanes = lax.broadcasted_iota(jnp.int32, (heads * block_len, chosen_rows.shape[1]), 1)
        queries = [ready[1, pair, rows, :] for pair in range(pairs)]
        for upper in (False, True):
            scores = dot_last(one_sided(queries, upper), chosen_rows[0])
            scores = scores * score_scale + blocked
            later = (lanes < packed) & (lanes + packed * upper > row_place)
            half_scores.append(jnp.where(later, big_negative, scores))
        peak = jnp.maximum(
            jnp.max(half_scores[0], axis=-1, keepdims=True),
            jnp.max(half_scores[1], axis=-1, keepdims=True),
        )
        total = 0.0
        products = []
        for upper in range(2):
            raw = jnp.exp(half_scores[upper] - peak)
            total = total + jnp.sum(raw, axis=-1, keepdims=True)
            products.append(
                jnp.dot(
                    raw.astype(jnp.bfloat16), chosen_rows[1], preferred_element_type=jnp.float32
                )
            )
        summed = products[0][:, :64] + products[1][:, 64:]
        mixed = mixed_spans + gate_of[1] * (summed / total)
        chosen_log = peak + jnp.log(total)
        for pair in range(pairs):
            first = mixed[2 * pair * block_len : (2 * pair + 1) * block_len]
            second = mixed[(2 * pair + 1) * block_len : (2 * pair + 2) * block_len]
            both = jnp.concatenate([first, second], axis=1)
            lower, upper = both[:packed], both[packed:]
            lane_range = slice(pair * 128, (pair + 1) * 128)
            kept[block, :, lane_range] = jnp.where(core == 0, lower, upper).astype(jnp.bfloat16)
            given[block, :, lane_range] = jnp.where(core == 0, upper, lower).astype(jnp.bfloat16)
        for head in range(heads):
            piece = slice(head * block_len, (head + 1) * block_len)
            logs[0, rows, head : head + 1] = span_log[piece]
            logs[1, rows, head : head + 1] = chosen_log[piece]


def kernel_call(kernel, specs, operands, outputs, scratch, flops, room):
    return pl.pallas_call(
        kernel,
        out_shape=outputs,
        in_specs=[pl.BlockSpec(memory_space=space) for space in specs],
        out_specs=jax.tree.map(lambda _: pl.BlockSpec(memory_space=pltpu.VMEM), outputs),
        scratch_shapes=scratch,
        cost_estimate=pl.CostEstimate(flops=flops, bytes_accessed=4 << 20, transcendentals=0),
        compiler_params=pltpu.CompilerParams(vmem_limit_bytes=room << 20),
    )(*operands)


def turns(places, head_size):
    half_size = head_size // 2
    inverse = jnp.power(rope_base, -jnp.arange(half_size, dtype=jnp.float32) * 2.0 / head_size)
    angles = places.astype(jnp.float32)[:, None] * inverse[None, :]
    cos_vals, sin_vals = jnp.cos(angles), jnp.sin(angles)
    return (
        jnp.concatenate([cos_vals] * 4, axis=1),
        jnp.concatenate([-sin_vals, sin_vals] * 2, axis=1),
    )


def shards(
    tokens,
    query_weight,
    key_weight,
    value_weight,
    gate_weight,
    query_gain,
    key_gain,
    out_weight,
    shared_block,
    chosen_device,
):
    tok_rows = tokens.shape[0]
    head_size = query_gain.shape[0]
    width = query_weight.shape[1]
    head_count = width // head_size
    packed = SEL // 2
    local_blocks = tok_rows // SEL
    device = lax.axis_index(KV)
    z_count, y_count = (lax.axis_size(axis) for axis in KV)
    sent_rows = SEL + tok_rows // CMP
    places = device * tok_rows + jnp.arange(tok_rows, dtype=jnp.int32)
    cosines, sines = turns(places, head_size)
    bf16, f32 = jnp.bfloat16, jnp.float32
    shape = jax.ShapeDtypeStruct
    vmem, smem, anywhere = pltpu.VMEM, pltpu.SMEM, pl.ANY

    sent, own = kernel_call(
        key_kernel,
        [smem] + [vmem] * 6,
        (shared_block, tokens, key_weight.T, value_weight.T, key_gain[None], cosines, sines),
        (shape((sent_rows, 128), bf16), shape((2, local_blocks, packed, 128), bf16)),
        (),
        10**9,
        KEY_ROOM,
    )
    column = lax.all_gather(sent, "z", axis=0, tiled=True)
    arrived = spread(column, "y").reshape(y_count, z_count, sent_rows, 128)

    tokens_later, own, cosines, sines, swap_weight, _ = lax.optimization_barrier(
        (tokens, own, cosines, sines, out_weight, column)
    )
    other_weight = lax.ppermute(swap_weight, "core", [(0, 1), (1, 0)])
    ready, gates = kernel_call(
        query_kernel,
        [smem] + [vmem] * 6,
        (
            lax.axis_index(TP).reshape(1),
            tokens_later,
            query_weight,
            gate_weight.T,
            jnp.concatenate([query_gain, query_gain])[None],
            cosines,
            sines,
        ),
        (
            shape((2, width // 128, tok_rows, 128), bf16),
            shape((tok_rows, 2 * head_count), f32),
        ),
        (),
        10**9,
        QUERY_ROOM,
    )
    kept, given, log_weight = kernel_call(
        attention_kernel,
        [smem, smem, vmem, anywhere, anywhere, anywhere],
        (
            jnp.stack([device, lax.axis_index("core")]),
            chosen_device,
            arrived,
            ready,
            gates,
            own,
        ),
        (
            shape((local_blocks, packed, width), bf16),
            shape((local_blocks, packed, width), bf16),
            shape((2, tok_rows, head_count), f32),
        ),
        (
            pltpu.VMEM(ready.shape, bf16),
            pltpu.VMEM(gates.shape, f32),
            pltpu.VMEM(own.shape, bf16),
            pltpu.VMEM((2, (chosen_device.shape[1] + 1) * packed, 128), bf16),
            pltpu.VMEM((y_count * z_count * (sent_rows - SEL), 128), bf16),
            pltpu.SemaphoreType.DMA((3,)),
        ),
        4 * 10**9,
        ATTENTION_ROOM,
    )
    taken = lax.ppermute(given, "core", [(0, 1), (1, 0)])
    own_partial = jnp.dot(
        kept.reshape(-1, width), out_weight, preferred_element_type=jnp.float32
    ).astype(bf16)
    other_partial = jnp.dot(
        taken.reshape(-1, width), other_weight, preferred_element_type=jnp.float32
    ).astype(bf16)
    pair_sum = (own_partial.astype(f32) + other_partial.astype(f32)).astype(bf16)
    pair_sum = pair_sum.reshape(local_blocks, packed, -1)
    pieces = lax.all_to_all(pair_sum, "x", split_axis=0, concat_axis=0, tiled=True)
    mixed_out = pieces.astype(f32).sum(axis=0).astype(bf16)
    return (mixed_out, log_weight)


def solution(mesh):
    torus = Mesh(mesh.devices.reshape(32, 4, 4, 2), ("z", "y", "x", "core"))
    return jax.shard_map(
        shards,
        mesh=torus,
        in_specs=(
            P(KV, None),
            P(None, TP),
            P(None, TP),
            P(None, TP),
            P(),
            P(),
            P(),
            P(TP, None),
            P(KV),
            P(KV, None),
        ),
        out_specs=(P((*KV, *TP), None), P(None, KV, TP)),
        check_vma=False,
    )
```

time: 161 us -> 132 us (0.82)
  waiting for transfers between devices: 40.8 us -> 8.58 us
  local copies, waits for them, and re-layouts: 24.5 us -> 4.29 us
  starting transfers between devices: 21.7 us -> 38.7 us
  Pallas kernels: 8.39 us -> 13.2 us
  blocking collectives: 55.2 us -> 58.4 us
    all_gather x0 -> x1, blocking collectives: none -> 58.4 us  [shards(): column = lax.all_gather(sent, 'z', axis=0, tiled=True)]
    all_to_all x1 -> x0, blocking collectives: 55.2 us -> none  [shards(): far = lax.all_to_all(sent, 'z_far', split_axis=0, concat_axis=0, tiled=True)]
    ppermute x0 -> x2, starting transfers between devices: none -> 30.4 us  [the longest x1 16.8 us: shards(): other_weight = lax.ppermute(swap_weight, 'core', [(0, 1), (1, 0)])]
    all_to_all x3 -> x1, waiting for transfers between devices: 26.6 us -> 0.01 us  [spread(): return lax.all_to_all(copies, axis, split_axis=0, concat_axis=0, tiled=True)]
    unnamed x45 -> x11, local copies, waits for them, and re-layouts: 15.9 us -> 2.57 us
    all_to_all x3 -> x1, starting transfers between devices: 14.9 us -> 4.31 us  [spread(): return lax.all_to_all(copies, axis, split_axis=0, concat_axis=0, tiled=True)]
    all_to_all x1, waiting for transfers between devices: 14.3 us -> 8.57 us  [shards(): lax.all_to_all(pair_sum, 'x', split_axis=0, concat_axis=0, tiled=True)]
    pallas_call x3, Pallas kernels: 8.39 us -> 13.2 us  [kernel_call(): pl.pallas_call(kernel, out_shape=outputs, in_specs=[pl.BlockSpec(memory_s...]
  transfers between devices with their start and end apart: 4 -> 4, of which waited for: 3 -> 1; matrix products, arithmetic and copies ran while one was open for 7% -> 2% of each run, Pallas kernels for 3% -> 8%
where the time goes in v3:
time: 132 us; the launch traced here: 131 us
  blocking collectives  58.4 us (44%)
  starting transfers between devices  38.7 us (29%)
  Pallas kernels  13.2 us (10%)
  waiting for transfers between devices  8.58 us (6%)
  local copies, waits for them, and re-layouts  4.29 us (3%)
  matrix products  3.87 us (3%)
  other arithmetic  2.91 us (2%)
  between operations  1.39 us (1%)
    all_gather x1, blocking collectives, shards(): column = lax.all_gather(sent, 'z', axis=0, tiled=True)  58.4 us
    ppermute x1, starting transfers between devices, shards(): other_weight = lax.ppermute(swap_weight, 'core', [(0, 1), (1, 0)])  16.8 us
    ppermute x1, starting transfers between devices, shards(): taken = lax.ppermute(given, 'core', [(0, 1), (1, 0)])  13.6 us
    pallas_call x3, Pallas kernels, kernel_call(): pl.pallas_call(kernel, out_shape=outputs, in_specs=[pl.BlockSpec(memory_s...  13.2 us
    all_to_all x1, waiting for transfers between devices, shards(): lax.all_to_all(pair_sum, 'x', split_axis=0, concat_axis=0, tiled=True)  8.57 us
    all_to_all x1, starting transfers between devices, spread(): return lax.all_to_all(copies, axis, split_axis=0, concat_axis=0, tiled=True)  4.31 us
    all_to_all x1, starting transfers between devices, shards(): lax.all_to_all(pair_sum, 'x', split_axis=0, concat_axis=0, tiled=True)  3.96 us
  transfers between devices with their start and end apart: 4, of which 1 were waited for; matrix products, arithmetic and copies ran while one was open for 2% of the time, Pallas kernels for 8%

profile of v3, /device:TPU:1, one launch (start us, length us, event | category | flops | bytes accessed | tf_op | source)
XLA Modules:
  0.0 131.3 jit_solution(13370606280048148950)
XLA Ops:
  1.3 0.5 fusion.4
  1.9 1.0 pad_maximum_fusion
  2.8 3.0 %shard_map.113 = (bf16[72,128]{1,0:T(8,128)(2,1)}, bf16[2,4,32,128]{3,2,1,0:T(8,128)(2,1)}) custom-call(s32[1]{0:T(128)S(6)} %copy.15.pick, bf16[256,2048]{1,0:T(8,128)(2,1)} %tokens.2, bf16[64,2048]{1,0:T(8,128)(2,1)} %bitcast.20, bf16[64,2048]{1,0:T(8,128)(2,1)} %bitcast.21, f32[1,64]{1,0:T(1,128)} %bitcast.23, f32[256,128]{1,0:T(8,128)} %get-tuple-element.17.cosines, ...), custom_call_target="tpu_custom_call" | custom-call | flops 1000000000 | bytes 4194304 | tf_op jit(solution)/shard_map/pallas_call | solution.py:234
  5.8 58.4 %all_gather.3 = bf16[2304,128]{1,0:T(8,128)(2,1)S(1)} all-gather(bf16[72,128]{1,0:T(8,128)(2,1)} %get-tuple-element.14), channel_id=1, replica_groups=mesh['z'=32,'y'=4,'x'=4,'core'=2] {'z'}, dimensions={0}, use_global_device_ids=true | all-gather | bytes 608256 | tf_op jit(solution)/shard_map/all_gather | solution.py:292
  64.2 1.7 %broadcast_in_dim.7 = bf16[4,2304,128]{2,1,0:T(8,128)(2,1)} broadcast(bf16[2304,128]{1,0:T(8,128)(2,1)S(1)} %all_gather.3), dimensions={1,2} | broadcast | bytes 2949120 | tf_op jit(solution)/shard_map/broadcast_in_dim | solution.py:25
  65.9 0.0 copy-start.4
  65.9 4.3 %all-to-all-start = ((bf16[4,2304,128]{2,1,0:T(8,128)(2,1)}), bf16[4,2304,128]{2,1,0:T(8,128)(2,1)S(1)}, u32[]{:S(2)}, u32[]{:S(2)}) async-start(bf16[4,2304,128]{2,1,0:T(8,128)(2,1)} %broadcast_in_dim.7), calls=%async_computation | async-start | bytes 4718592 | tf_op jit(solution)/shard_map/all_to_all | solution.py:26
  70.2 0.0 copy-start
  70.2 0.0 copy-start.3
  70.2 16.8 %collective-permute-start.1 = (bf16[256,2048]{1,0:T(8,128)(2,1)}, bf16[256,2048]{1,0:T(8,128)(2,1)}, u32[]{:S(2)}, u32[]{:S(2)}) collective-permute-start(bf16[256,2048]{1,0:T(8,128)(2,1)} %param.17), channel_id=1, source_target_pairs={{0,1},{1,0},{2,3},{3,2},{4,5},{5,4},{6,7},{7,6},{8,9},{9,8},{10,11... | collective-permute-start | bytes 3145736 | tf_op jit(solution)/shard_map/ppermute | solution.py:298
  87.1 0.0 copy-done.4
  87.1 0.6 maximum_bitcast_fusion.gain
  87.7 3.5 %shard_map.114 = (bf16[2,2,256,128]{3,2,1,0:T(8,128)(2,1)}, f32[256,8]{1,0:T(8,128)}) custom-call(s32[1]{0:T(128)} %bitcast.6.group, bf16[256,2048]{1,0:T(8,128)(2,1)} %tokens.2, bf16[2048,256]{1,0:T(8,128)(2,1)} %query_weight.1, bf16[64,2048]{1,0:T(8,128)(2,1)} %bitcast.22, f32[1,128]{1,0:T(1,128)} %maximum_bitcast_fusion.gain, ...), custom_call_target="tpu_custom_call" | custom-call | flops 1000000000 | bytes 4194304 | tf_op jit(solution)/shard_map/pallas_call | solution.py:234
  91.2 0.1 pad_add_fusion.place_of
  91.2 0.0 all-to-all-done
  91.2 0.0 copy-done
  91.2 0.0 copy-done.3
  91.3 0.0 copy-start.1
  91.3 0.9 copy-done.1
  92.2 0.0 copy-start.2
  92.2 0.9 copy-done.2
  93.1 6.7 %shard_map.115 = (bf16[4,32,256]{2,1,0:T(8,128)(2,1)S(1)}, bf16[4,32,256]{2,1,0:T(8,128)(2,1)S(1)}, f32[2,256,4]{2,1,0:T(8,128)S(1)}) custom-call(s32[2]{0:T(128)S(1)} %pad_add_fusion.place_of, s32[4,15]{1,0:T(4,128)S(1)} %copy-done, bf16[4,32,72,128]{3,2,1,0:T(8,128)(2,1)S(1)} %bitcast.17, bf16[2,2,256,128]{3,2,1,0:T(8,128)(2,1)S(1)} %copy-done.1, ...), custom_call_target="tpu_custom_call" | custom-call | flops 4000000000 | bytes 4194304 | tf_op jit(solution)/shard_map/pallas_call | solution.py:234
  99.8 13.6 %collective-permute-start = (bf16[4,32,256]{2,1,0:T(8,128)(2,1)S(1)}, bf16[4,32,256]{2,1,0:T(8,128)(2,1)S(1)}, u32[]{:S(2)}, u32[]{:S(2)}) collective-permute-start(bf16[4,32,256]{2,1,0:T(8,128)(2,1)S(1)} %get-tuple-element.23), channel_id=1, source_target_pairs={{0,1},{1,0},{2,3},{3,2},{4,5},{5,4},{6,7},{7,6},{8,9},{9,8},{10,11... | collective-permute-start | bytes 196616 | tf_op jit(solution)/shard_map/ppermute | solution.py:346
  113.5 1.5 %fusion.3 = f32[128,2048]{1,0:T(8,128)S(1)} fusion(bf16[128,256]{1,0:T(8,128)(2,1)S(1)} %bitcast.18, bf16[256,2048]{1,0:T(8,128)(2,1)} %param.17), kind=kOutput, calls=%fused_computation.5 | convolution fusion | flops 134742016 | bytes 2162688 | tf_op jit(solution)/shard_map/dot_general | solution.py:347
  115.0 0.0 collective-permute-done.1
  115.0 0.0 collective-permute-done
  115.0 2.3 %fusion.2 = bf16[128,2048]{1,0:T(8,128)(2,1)} fusion(f32[128,2048]{1,0:T(8,128)S(1)} %fusion.3, bf16[128,256]{1,0:T(8,128)(2,1)S(1)} %bitcast.19, bf16[256,2048]{1,0:T(8,128)(2,1)} %collective-permute-done.1), kind=kOutput, calls=%fused_computation.3 | convolution fusion | flops 135266304 | bytes 2686976 | tf_op jit(solution)/shard_map/dot_general | solution.py:350
  117.4 4.0 %all-to-all-start.1 = ((bf16[4,32,2048]{2,1,0:T(8,128)(2,1)}), bf16[4,32,2048]{2,1,0:T(8,128)(2,1)S(1)}, u32[]{:S(2)}, u32[]{:S(2)}) async-start(bf16[4,32,2048]{2,1,0:T(8,128)(2,1)} %bitcast.11), calls=%async_computation.1 | async-start | bytes 1048576 | tf_op jit(solution)/shard_map/all_to_all | solution.py:355
  121.3 0.7 copy.14
  122.0 8.6 %all-to-all-done.1 = bf16[4,32,2048]{2,1,0:T(8,128)(2,1)S(1)} async-done(((bf16[4,32,2048]{2,1,0:T(8,128)(2,1)}), bf16[4,32,2048]{2,1,0:T(8,128)(2,1)S(1)}, u32[]{:S(2)}, u32[]{:S(2)}) %all-to-all-start.1) | async-done | bytes 524320 | tf_op jit(solution)/shard_map/all_to_all | solution.py:355
  130.6 0.7 reduce_sum.12
  (2 shorter events, 0.0 us)
Async XLA Ops:
  65.9 21.2 %copy-start.4 = (f32[64]{0:T(128)S(1)}, f32[64]{0:T(128)}, u32[]{:S(2)}) copy-start(f32[64]{0:T(128)} %param.15) | copy-start | bytes 772
  65.9 25.3 %all-to-all-start = ((bf16[4,2304,128]{2,1,0:T(8,128)(2,1)}), bf16[4,2304,128]{2,1,0:T(8,128)(2,1)S(1)}, u32[]{:S(2)}, u32[]{:S(2)}) async-start(bf16[4,2304,128]{2,1,0:T(8,128)(2,1)} %broadcast_in_dim.7), calls=%async_computation | async-start | bytes 4718592 | tf_op jit(solution)/shard_map/all_to_all | solution.py:26
  70.2 21.0 %copy-start = (s32[4,15]{1,0:T(4,128)S(1)}, s32[4,15]{1,0:T(4,128)}, u32[]{:S(2)}) copy-start(s32[4,15]{1,0:T(4,128)} %chosen.1) | copy-start | bytes 724
  70.2 21.0 %copy-start.3 = (bf16[2,4,32,128]{3,2,1,0:T(8,128)(2,1)S(1)}, bf16[2,4,32,128]{3,2,1,0:T(8,128)(2,1)}, u32[]{:S(2)}) copy-start(bf16[2,4,32,128]{3,2,1,0:T(8,128)(2,1)} %get-tuple-element.21.own_far) | copy-start | bytes 196612
  70.2 44.8 %collective-permute-start.1 = (bf16[256,2048]{1,0:T(8,128)(2,1)}, bf16[256,2048]{1,0:T(8,128)(2,1)}, u32[]{:S(2)}, u32[]{:S(2)}) collective-permute-start(bf16[256,2048]{1,0:T(8,128)(2,1)} %param.17), channel_id=1, source_target_pairs={{0,1},{1,0},{2,3},{3,2},{4,5},{5,4},{6,7},{7,6},{8,9},{9,8},{10,11... | collective-permute-start | bytes 3145736 | tf_op jit(solution)/shard_map/ppermute | solution.py:298
  91.3 1.0 copy-start.1
  92.2 0.9 copy-start.2
  99.8 15.2 %collective-permute-start = (bf16[4,32,256]{2,1,0:T(8,128)(2,1)S(1)}, bf16[4,32,256]{2,1,0:T(8,128)(2,1)S(1)}, u32[]{:S(2)}, u32[]{:S(2)}) collective-permute-start(bf16[4,32,256]{2,1,0:T(8,128)(2,1)S(1)} %get-tuple-element.23), channel_id=1, source_target_pairs={{0,1},{1,0},{2,3},{3,2},{4,5},{5,4},{6,7},{7,6},{8,9},{9,8},{10,11... | collective-permute-start | bytes 196616 | tf_op jit(solution)/shard_map/ppermute | solution.py:346
  117.4 13.2 %all-to-all-start.1 = ((bf16[4,32,2048]{2,1,0:T(8,128)(2,1)}), bf16[4,32,2048]{2,1,0:T(8,128)(2,1)S(1)}, u32[]{:S(2)}, u32[]{:S(2)}) async-start(bf16[4,32,2048]{2,1,0:T(8,128)(2,1)} %bitcast.11), calls=%async_computation.1 | async-start | bytes 1048576 | tf_op jit(solution)/shard_map/all_to_all | solution.py:355

commit v4 on v3

--- a/solution.py
+++ b/solution.py
@@ -1,3 +1,5 @@
+import functools
+
 import jax
 import jax.numpy as jnp
 from jax import lax
@@ -8,7 +10,7 @@
 
 SEL = 64
 CMP = 32
-KV = ("z", "y")
+KV = ("z_far", "z_near", "y")
 TP = ("x", "core")
 KEY_ROOM = 60
 QUERY_ROOM = 60
@@ -29,6 +31,10 @@
 def swapped(values_in):
     half_size = values_in.shape[-1] // 2
     return jnp.concatenate([values_in[:, half_size:], values_in[:, :half_size]], axis=1)
+
+
+def repeated(halves, signs):
+    return jnp.concatenate([sign * halves for sign in signs], axis=1)
 
 
 def side_by_side(rows):
@@ -52,7 +58,9 @@
     square = jnp.mean(keys * keys, axis=-1, keepdims=True)
     plain = (keys * lax.rsqrt(square + norm_eps) * gain[...]).astype(jnp.bfloat16)
     plain = plain.astype(jnp.float32)
-    turned = plain * cosines[:, :64] + swapped(plain) * sines[:, :64]
+    turned = plain * repeated(cosines[...], (1, 1)) + swapped(plain) * repeated(
+        sines[...], (-1, 1)
+    )
     turned = turned.astype(jnp.bfloat16)
     for block in range(blocks):
         rows = slice(block * block_len, (block + 1) * block_len)
@@ -65,15 +73,17 @@
     sent[block_len:] = spans.astype(jnp.bfloat16)
 
 
-def query_kernel(group, tokens, query_weight, gate_weight, gain, cosines, sines, ready, gates):
+def query_kernel(group, tokens, query_weight, gate_weight, gain, cosines, sines, ready):
     tok_rows = tokens.shape[0]
     width = query_weight.shape[1]
-    gate_count = gates.shape[1]
+    gate_count = 2 * (width // 64)
     start = pl.multiple_of(group[0] * gate_count, gate_count)
-    gates[...] = jax.nn.sigmoid(
+    ready[2 * (width // 128), :, :gate_count] = jax.nn.sigmoid(
         dot_last(tokens[...], gate_weight[pl.ds(start, gate_count), :].astype(jnp.bfloat16))
     )
     lanes = lax.broadcasted_iota(jnp.int32, (tok_rows, 128), 1)
+    cos_lanes = repeated(cosines[...], (1, 1, 1, 1))
+    sin_lanes = repeated(sines[...], (-1, 1, -1, 1))
     for pair in range(width // 128):
         queries = jnp.dot(
             tokens[...],
@@ -86,13 +96,13 @@
         second = jnp.sum(jnp.where(lanes < 64, 0.0, squares), axis=-1, keepdims=True)
         square = jnp.where(lanes < 64, first, second) * (1.0 / 64)
         plain = (queries * lax.rsqrt(square + norm_eps) * gain[...]).astype(jnp.bfloat16)
-        ready[0, pair] = plain
         plain = plain.astype(jnp.float32)
+        ready[pair] = plain
         partner = jnp.where(
             lanes % 64 < 32, pltpu.roll(plain, 96, axis=1), pltpu.roll(plain, 32, axis=1)
         )
-        turned = plain * cosines[...] + partner * sines[...]
-        ready[1, pair] = turned.astype(jnp.bfloat16)
+        turned = plain * cos_lanes + partner * sin_lanes
+        ready[width // 128 + pair] = turned.astype(jnp.bfloat16).astype(jnp.float32)
 
 
 def one_sided(queries, upper):
@@ -100,7 +110,6 @@
     lanes = lax.broadcasted_iota(jnp.int32, queries[0].shape, 1)
     keep = (lanes >= 64) if upper else (lanes < 64)
     for both in queries:
-        both = both.astype(jnp.float32)
         turned = swapped(both)
         for piece in (turned, both) if upper else (both, turned):
             pieces.append(jnp.where(keep, piece, 0.0).astype(jnp.bfloat16))
@@ -108,58 +117,47 @@
 
 
 def attention_kernel(
+    far_count,
     place_of,
     chosen,
     arrived,
-    ready_far,
-    gates_far,
-    own_far,
+    ready,
+    own,
     kept,
     given,
     logs,
-    ready,
-    gates,
-    own,
     chosen_rows,
     spans,
-    semaphores,
 ):
     device, core = place_of[0], place_of[1]
     blocks, named = chosen.shape
     _, _, packed, _ = own.shape
     y_count, z_count, sent_rows, _ = arrived.shape
     block_len = 2 * packed
-    pairs = ready.shape[1]
+    pairs = kept.shape[2] // 128
     heads = 2 * pairs
     tok_rows = blocks * block_len
     span_rows = sent_rows - block_len
     score_scale = 64 ** (-0.5)
-    loads = [
-        pltpu.make_async_copy(far, near, semaphores.at[number])
-        for number, (far, near) in enumerate(
-            ((ready_far, ready), (gates_far, gates), (own_far, own))
-        )
-    ]
-    for load in loads:
-        load.start()
     column_rows = z_count * span_rows
     for y in range(y_count):
         column = arrived[y, :, block_len:, :].astype(jnp.float32)
         spans[y * column_rows : (y + 1) * column_rows] = column.reshape(column_rows, 128).astype(
             jnp.bfloat16
         )
-    for load in loads:
-        load.wait()
     row_place = lax.broadcasted_iota(jnp.int32, (heads * block_len, 1), 0) % block_len
     span_index = lax.broadcasted_iota(jnp.int32, (1, y_count * column_rows), 1)
-    owner = span_index % column_rows // span_rows * y_count + span_index // column_rows
+    slot = span_index % column_rows // span_rows
+    near_count = z_count // far_count
+    owner = (slot % far_count * near_count + slot // far_count) * y_count
+    owner = owner + span_index // column_rows
     span_ends = owner * tok_rows + span_index % span_rows * CMP + CMP - 1
     rank = lax.broadcasted_iota(jnp.int32, (1, chosen_rows.shape[1]), 1) // packed
 
     @pl.loop(0, blocks)
     def _(block):
         rows = pl.ds(pl.multiple_of(block * block_len, block_len), block_len)
-        gate_rows = gates[rows, :]
+        gate_rows = ready[2 * pairs, rows, :]
         gate_of = [
             jnp.concatenate(
                 [gate_rows[:, 2 * head + b : 2 * head + b + 1] for head in range(heads)], axis=0
@@ -167,7 +165,7 @@
             for b in range(2)
         ]
         scores = dot_last(
-            one_sided([ready[0, pair, rows, :] for pair in range(pairs)], False), spans[...]
+            one_sided([ready[pair, rows, :] for pair in range(pairs)], False), spans[...]
         )
         places = device * tok_rows + block * block_len + row_place
         has_span = places >= CMP - 1
@@ -185,15 +183,16 @@
         for number in range(named):
             source = chosen[block, number]
             z, y = source // y_count, source % y_count
+            slot = z % near_count * far_count + z // near_count
             for part in range(2):
                 chosen_rows[part, (number + 1) * packed : (number + 2) * packed] = arrived[
-                    y, z, part * packed : (part + 1) * packed, :
+                    y, slot, part * packed : (part + 1) * packed, :
                 ]
             bias = jnp.where(source < device, 0.0, big_negative)
             blocked = jnp.where(rank == number + 1, bias, blocked)
         half_scores = []
         lanes = lax.broadcasted_iota(jnp.int32, (heads * block_len, chosen_rows.shape[1]), 1)
-        queries = [ready[1, pair, rows, :] for pair in range(pairs)]
+        queries = [ready[pairs + pair, rows, :] for pair in range(pairs)]
         for upper in (False, True):
             scores = dot_last(one_sided(queries, upper), chosen_rows[0])
             scores = scores * score_scale + blocked
@@ -246,11 +245,7 @@
     half_size = head_size // 2
     inverse = jnp.power(rope_base, -jnp.arange(half_size, dtype=jnp.float32) * 2.0 / head_size)
     angles = places.astype(jnp.float32)[:, None] * inverse[None, :]
-    cos_vals, sin_vals = jnp.cos(angles), jnp.sin(angles)
-    return (
-        jnp.concatenate([cos_vals] * 4, axis=1),
-        jnp.concatenate([-sin_vals, sin_vals] * 2, axis=1),
-    )
+    return jnp.cos(angles), jnp.sin(angles)
 
 
 def shards(
@@ -272,13 +267,14 @@
     packed = SEL // 2
     local_blocks = tok_rows // SEL
     device = lax.axis_index(KV)
-    z_count, y_count = (lax.axis_size(axis) for axis in KV)
+    far_count, near_count, y_count = (lax.axis_size(axis) for axis in KV)
+    z_count = far_count * near_count
     sent_rows = SEL + tok_rows // CMP
     places = device * tok_rows + jnp.arange(tok_rows, dtype=jnp.int32)
     cosines, sines = turns(places, head_size)
     bf16, f32 = jnp.bfloat16, jnp.float32
     shape = jax.ShapeDtypeStruct
-    vmem, smem, anywhere = pltpu.VMEM, pltpu.SMEM, pl.ANY
+    vmem, smem = pltpu.VMEM, pltpu.SMEM
 
     sent, own = kernel_call(
         key_kernel,
@@ -289,14 +285,15 @@
         10**9,
         KEY_ROOM,
     )
-    column = lax.all_gather(sent, "z", axis=0, tiled=True)
+    far = lax.all_gather(sent, "z_far", axis=0, tiled=True)
+    column = lax.all_gather(far, "z_near", axis=0, tiled=True)
     arrived = spread(column, "y").reshape(y_count, z_count, sent_rows, 128)
 
     tokens_later, own, cosines, sines, swap_weight, _ = lax.optimization_barrier(
         (tokens, own, cosines, sines, out_weight, column)
     )
     other_weight = lax.ppermute(swap_weight, "core", [(0, 1), (1, 0)])
-    ready, gates = kernel_call(
+    ready = kernel_call(
         query_kernel,
         [smem] + [vmem] * 6,
         (
@@ -308,23 +305,19 @@
             cosines,
             sines,
         ),
-        (
-            shape((2, width // 128, tok_rows, 128), bf16),
-            shape((tok_rows, 2 * head_count), f32),
-        ),
+        shape((2 * (width // 128) + 1, tok_rows, 128), f32),
         (),
         10**9,
         QUERY_ROOM,
     )
     kept, given, log_weight = kernel_call(
-        attention_kernel,
-        [smem, smem, vmem, anywhere, anywhere, anywhere],
+        functools.partial(attention_kernel, far_count),
+        [smem, smem, vmem, vmem, vmem],
         (
             jnp.stack([device, lax.axis_index("core")]),
             chosen_device,
             arrived,
             ready,
-            gates,
             own,
         ),
         (
@@ -333,12 +326,8 @@
             shape((2, tok_rows, head_count), f32),
         ),
         (
-            pltpu.VMEM(ready.shape, bf16),
-            pltpu.VMEM(gates.shape, f32),
-            pltpu.VMEM(own.shape, bf16),
             pltpu.VMEM((2, (chosen_device.shape[1] + 1) * packed, 128), bf16),
             pltpu.VMEM((y_count * z_count * (sent_rows - SEL), 128), bf16),
-            pltpu.SemaphoreType.DMA((3,)),
         ),
         4 * 10**9,
         ATTENTION_ROOM,
@@ -358,7 +347,7 @@
 
 
 def solution(mesh):
-    torus = Mesh(mesh.devices.reshape(32, 4, 4, 2), ("z", "y", "x", "core"))
+    torus = Mesh(mesh.devices.reshape(8, 4, 4, 4, 2), (*KV, *TP))
     return jax.shard_map(
         shards,
         mesh=torus,

time: 132 us -> 131 us (level)
  starting transfers between devices: 38.7 us -> 32.1 us
  waiting for transfers between devices: 8.58 us -> 12.4 us
  blocking collectives: 58.4 us -> 60.9 us
    ppermute x1, starting transfers between devices: 16.8 us -> 11.3 us  [shards(): other_weight = lax.ppermute(swap_weight, 'core', [(0, 1), (1, 0)])]
    all_to_all x1, waiting for transfers between devices: 0.01 us -> 3.87 us  [spread(): return lax.all_to_all(copies, axis, split_axis=0, concat_axis=0, tiled=True)]
    all_gather x1 -> x2, blocking collectives: 58.4 us -> 60.9 us  [the longest x1 47.6 us: shards(): far = lax.all_gather(sent, 'z_far', axis=0, tiled=True)]
  transfers between devices with their start and end apart: 4 -> 4, of which waited for: 1 -> 2; matrix products, arithmetic and copies ran while one was open for 2% -> 2% of each run, Pallas kernels for 8% -> 8%
where the time goes in v4:
time: 131 us; the launch traced here: 130 us
  blocking collectives  60.9 us (46%)
  starting transfers between devices  32.1 us (25%)
  Pallas kernels  13.4 us (10%)
  waiting for transfers between devices  12.4 us (9%)
  matrix products  3.87 us (3%)
  local copies, waits for them, and re-layouts  3.52 us (3%)
  other arithmetic  2.72 us (2%)
  between operations  1.36 us (1%)
    all_gather x1, blocking collectives, shards(): far = lax.all_gather(sent, 'z_far', axis=0, tiled=True)  47.6 us
    pallas_call x3, Pallas kernels, kernel_call(): pl.pallas_call(kernel, out_shape=outputs, in_specs=[pl.BlockSpec(memory_s...  13.4 us
    all_gather x1, blocking collectives, shards(): column = lax.all_gather(far, 'z_near', axis=0, tiled=True)  13.2 us
    ppermute x1, starting transfers between devices, shards(): taken = lax.ppermute(given, 'core', [(0, 1), (1, 0)])  12.4 us
    ppermute x1, starting transfers between devices, shards(): other_weight = lax.ppermute(swap_weight, 'core', [(0, 1), (1, 0)])  11.3 us
    all_to_all x1, waiting for transfers between devices, shards(): lax.all_to_all(pair_sum, 'x', split_axis=0, concat_axis=0, tiled=True)  8.57 us
    all_to_all x1, starting transfers between devices, shards(): lax.all_to_all(pair_sum, 'x', split_axis=0, concat_axis=0, tiled=True)  4.23 us
    all_to_all x1, starting transfers between devices, spread(): return lax.all_to_all(copies, axis, split_axis=0, concat_axis=0, tiled=True)  4.17 us
  transfers between devices with their start and end apart: 4, of which 2 were waited for; matrix products, arithmetic and copies ran while one was open for 2% of the time, Pallas kernels for 8%

profile of v4, /device:TPU:1, one launch (start us, length us, event | category | flops | bytes accessed | tf_op | source)
XLA Modules:
  0.0 130.4 jit_solution(7864089063786160439)
XLA Ops:
  1.3 1.2 multiply_sine_fusion
  2.5 3.0 %shard_map.113 = (bf16[72,128]{1,0:T(8,128)(2,1)}, bf16[2,4,32,128]{3,2,1,0:T(8,128)(2,1)}) custom-call(s32[1]{0:T(128)S(6)} %copy.13.pick, bf16[256,2048]{1,0:T(8,128)(2,1)} %tokens.2, bf16[64,2048]{1,0:T(8,128)(2,1)} %bitcast.20, bf16[64,2048]{1,0:T(8,128)(2,1)} %bitcast.21, f32[1,64]{1,0:T(1,128)} %bitcast.23, f32[256,32]{1,0:T(8,128)} %get-tuple-element.15.cosines, ...), custom_call_target="tpu_custom_call" | custom-call | flops 1000000000 | bytes 4194304 | tf_op jit(solution)/shard_map/pallas_call | solution.py:233
  5.6 47.6 %all_gather.6 = bf16[576,128]{1,0:T(8,128)(2,1)S(1)} all-gather(bf16[72,128]{1,0:T(8,128)(2,1)} %get-tuple-element.12), channel_id=1, replica_groups=mesh['z_far'=8,'z_near'=4,'y'=4,'x'=4,'core'=2] {'z_far'}, dimensions={0}, use_global_device_ids=true | all-gather | bytes 165888 | tf_op jit(solution)/shard_map/all_gather | solution.py:288
  53.2 13.2 %all_gather.7 = bf16[2304,128]{1,0:T(8,128)(2,1)S(1)} all-gather(bf16[576,128]{1,0:T(8,128)(2,1)S(1)} %all_gather.6), channel_id=1, replica_groups=mesh['z_far'=8,'z_near'=4,'y'=4,'x'=4,'core'=2] {'z_near'}, dimensions={0}, use_global_device_ids=true | all-gather | bytes 737280 | tf_op jit(solution)/shard_map/all_gather | solution.py:289
  66.4 1.7 %broadcast_in_dim.7 = bf16[4,2304,128]{2,1,0:T(8,128)(2,1)} broadcast(bf16[2304,128]{1,0:T(8,128)(2,1)S(1)} %all_gather.7), dimensions={1,2} | broadcast | bytes 2949120 | tf_op jit(solution)/shard_map/broadcast_in_dim | solution.py:27
  68.2 0.0 copy-start.3
  68.2 4.2 %all-to-all-start = ((bf16[4,2304,128]{2,1,0:T(8,128)(2,1)}), bf16[4,2304,128]{2,1,0:T(8,128)(2,1)S(1)}, u32[]{:S(2)}, u32[]{:S(2)}) async-start(bf16[4,2304,128]{2,1,0:T(8,128)(2,1)} %broadcast_in_dim.7), calls=%async_computation | async-start | bytes 4718592 | tf_op jit(solution)/shard_map/all_to_all | solution.py:28
  72.3 0.0 copy-start
  72.3 0.0 copy-start.2
  72.3 11.3 %collective-permute-start.1 = (bf16[256,2048]{1,0:T(8,128)(2,1)}, bf16[256,2048]{1,0:T(8,128)(2,1)}, u32[]{:S(2)}, u32[]{:S(2)}) collective-permute-start(bf16[256,2048]{1,0:T(8,128)(2,1)} %param.17), channel_id=1, source_target_pairs={{0,1},{1,0},{2,3},{3,2},{4,5},{5,4},{6,7},{7,6},{8,9},{9,8},{10,11... | collective-permute-start | bytes 3145736 | tf_op jit(solution)/shard_map/ppermute | solution.py:295
  83.7 0.0 copy-done.3
  83.7 0.7 maximum_bitcast_fusion.gain
  84.4 3.6 %shard_map.114.ready = f32[5,256,128]{2,1,0:T(8,128)} custom-call(s32[1]{0:T(128)} %bitcast.6.group, bf16[256,2048]{1,0:T(8,128)(2,1)} %tokens.2, bf16[2048,256]{1,0:T(8,128)(2,1)} %query_weight.1, bf16[64,2048]{1,0:T(8,128)(2,1)} %bitcast.22, f32[1,128]{1,0:T(1,128)} %maximum_bitcast_fusion.gain, f32[256,32]{1,0:T(8,128)} %get-tuple-element.15.cosines, ...), custom_call_target="tpu_custom_call" | custom-call | flops 1000000000 | bytes 4194304 | tf_op jit(solution)/shard_map/pallas_call | solution.py:233
  88.0 0.1 pad_add_fusion.place_of
  88.1 3.9 %all-to-all-done = bf16[4,2304,128]{2,1,0:T(8,128)(2,1)S(1)} async-done(((bf16[4,2304,128]{2,1,0:T(8,128)(2,1)}), bf16[4,2304,128]{2,1,0:T(8,128)(2,1)S(1)}, u32[]{:S(2)}, u32[]{:S(2)}) %all-to-all-start) | async-done | bytes 2359328 | tf_op jit(solution)/shard_map/all_to_all | solution.py:28
  92.0 0.0 copy-done
  92.0 0.0 copy-done.2
  92.0 0.0 copy-start.1
  92.0 1.1 copy-done.1
  93.0 6.8 %shard_map.115 = (bf16[4,32,256]{2,1,0:T(8,128)(2,1)S(1)}, bf16[4,32,256]{2,1,0:T(8,128)(2,1)S(1)}, f32[2,256,4]{2,1,0:T(8,128)S(1)}) custom-call(s32[2]{0:T(128)S(1)} %pad_add_fusion.place_of, s32[4,15]{1,0:T(4,128)S(1)} %copy-done, bf16[4,32,72,128]{3,2,1,0:T(8,128)(2,1)S(1)} %bitcast.17, f32[5,256,128]{2,1,0:T(8,128)S(1)} %copy-done.1, ...), custom_call_target="tpu_custom_call" | custom-call | flops 4000000000 | bytes 4194304 | tf_op jit(solution)/shard_map/pallas_call | solution.py:233
  99.8 12.4 %collective-permute-start = (bf16[4,32,256]{2,1,0:T(8,128)(2,1)S(1)}, bf16[4,32,256]{2,1,0:T(8,128)(2,1)S(1)}, u32[]{:S(2)}, u32[]{:S(2)}) collective-permute-start(bf16[4,32,256]{2,1,0:T(8,128)(2,1)S(1)} %get-tuple-element.19), channel_id=1, source_target_pairs={{0,1},{1,0},{2,3},{3,2},{4,5},{5,4},{6,7},{7,6},{8,9},{9,8},{10,11... | collective-permute-start | bytes 196616 | tf_op jit(solution)/shard_map/ppermute | solution.py:335
  112.2 1.5 %fusion.3 = f32[128,2048]{1,0:T(8,128)S(1)} fusion(bf16[128,256]{1,0:T(8,128)(2,1)S(1)} %bitcast.18, bf16[256,2048]{1,0:T(8,128)(2,1)} %param.17), kind=kOutput, calls=%fused_computation.5 | convolution fusion | flops 134742016 | bytes 2162688 | tf_op jit(solution)/shard_map/dot_general | solution.py:336
  113.8 0.0 collective-permute-done.1
  113.8 0.0 collective-permute-done
  113.8 2.3 %fusion.2 = bf16[128,2048]{1,0:T(8,128)(2,1)} fusion(f32[128,2048]{1,0:T(8,128)S(1)} %fusion.3, bf16[128,256]{1,0:T(8,128)(2,1)S(1)} %bitcast.19, bf16[256,2048]{1,0:T(8,128)(2,1)} %collective-permute-done.1), kind=kOutput, calls=%fused_computation.3 | convolution fusion | flops 135266304 | bytes 2686976 | tf_op jit(solution)/shard_map/dot_general | solution.py:339
  116.1 4.2 %all-to-all-start.1 = ((bf16[4,32,2048]{2,1,0:T(8,128)(2,1)}), bf16[4,32,2048]{2,1,0:T(8,128)(2,1)S(1)}, u32[]{:S(2)}, u32[]{:S(2)}) async-start(bf16[4,32,2048]{2,1,0:T(8,128)(2,1)} %bitcast.11), calls=%async_computation.1 | async-start | bytes 1048576 | tf_op jit(solution)/shard_map/all_to_all | solution.py:344
  120.3 0.7 copy.12
  121.1 8.6 %all-to-all-done.1 = bf16[4,32,2048]{2,1,0:T(8,128)(2,1)S(1)} async-done(((bf16[4,32,2048]{2,1,0:T(8,128)(2,1)}), bf16[4,32,2048]{2,1,0:T(8,128)(2,1)S(1)}, u32[]{:S(2)}, u32[]{:S(2)}) %all-to-all-start.1) | async-done | bytes 524320 | tf_op jit(solution)/shard_map/all_to_all | solution.py:344
  129.6 0.7 reduce_sum.12
  (2 shorter events, 0.0 us)
Async XLA Ops:
  68.2 15.5 %copy-start.3 = (f32[64]{0:T(128)S(1)}, f32[64]{0:T(128)}, u32[]{:S(2)}) copy-start(f32[64]{0:T(128)} %param.15) | copy-start | bytes 772
  68.2 23.8 %all-to-all-start = ((bf16[4,2304,128]{2,1,0:T(8,128)(2,1)}), bf16[4,2304,128]{2,1,0:T(8,128)(2,1)S(1)}, u32[]{:S(2)}, u32[]{:S(2)}) async-start(bf16[4,2304,128]{2,1,0:T(8,128)(2,1)} %broadcast_in_dim.7), calls=%async_computation | async-start | bytes 4718592 | tf_op jit(solution)/shard_map/all_to_all | solution.py:28
  72.3 19.6 %copy-start = (s32[4,15]{1,0:T(4,128)S(1)}, s32[4,15]{1,0:T(4,128)}, u32[]{:S(2)}) copy-start(s32[4,15]{1,0:T(4,128)} %chosen.1) | copy-start | bytes 724
  72.3 19.6 %copy-start.2 = (bf16[2,4,32,128]{3,2,1,0:T(8,128)(2,1)S(1)}, bf16[2,4,32,128]{3,2,1,0:T(8,128)(2,1)}, u32[]{:S(2)}) copy-start(bf16[2,4,32,128]{3,2,1,0:T(8,128)(2,1)} %get-tuple-element.17.own) | copy-start | bytes 196612
  72.3 41.4 %collective-permute-start.1 = (bf16[256,2048]{1,0:T(8,128)(2,1)}, bf16[256,2048]{1,0:T(8,128)(2,1)}, u32[]{:S(2)}, u32[]{:S(2)}) collective-permute-start(bf16[256,2048]{1,0:T(8,128)(2,1)} %param.17), channel_id=1, source_target_pairs={{0,1},{1,0},{2,3},{3,2},{4,5},{5,4},{6,7},{7,6},{8,9},{9,8},{10,11... | collective-permute-start | bytes 3145736 | tf_op jit(solution)/shard_map/ppermute | solution.py:295
  92.0 1.1 copy-start.1
  99.8 13.9 %collective-permute-start = (bf16[4,32,256]{2,1,0:T(8,128)(2,1)S(1)}, bf16[4,32,256]{2,1,0:T(8,128)(2,1)S(1)}, u32[]{:S(2)}, u32[]{:S(2)}) collective-permute-start(bf16[4,32,256]{2,1,0:T(8,128)(2,1)S(1)} %get-tuple-element.19), channel_id=1, source_target_pairs={{0,1},{1,0},{2,3},{3,2},{4,5},{5,4},{6,7},{7,6},{8,9},{9,8},{10,11... | collective-permute-start | bytes 196616 | tf_op jit(solution)/shard_map/ppermute | solution.py:335
  116.1 13.5 %all-to-all-start.1 = ((bf16[4,32,2048]{2,1,0:T(8,128)(2,1)}), bf16[4,32,2048]{2,1,0:T(8,128)(2,1)S(1)}, u32[]{:S(2)}, u32[]{:S(2)}) async-start(bf16[4,32,2048]{2,1,0:T(8,128)(2,1)} %bitcast.11), calls=%async_computation.1 | async-start | bytes 1048576 | tf_op jit(solution)/shard_map/all_to_all | solution.py:344

commit v5 on v4

--- a/solution.py
+++ b/solution.py
@@ -14,18 +14,12 @@
 TP = ("x", "core")
 KEY_ROOM = 60
 QUERY_ROOM = 60
-ATTENTION_ROOM = 12
+ATTENTION_ROOM = 60
 
 
 norm_eps = 1e-06
 rope_base = 500000.0
 big_negative = -1e30
-
-
-def spread(block, axis):
-    count = lax.axis_size(axis)
-    copies = lax.optimization_barrier(jnp.broadcast_to(block[None], (count, *block.shape)))
-    return lax.all_to_all(copies, axis, split_axis=0, concat_axis=0, tiled=True)
 
 
 def swapped(values_in):
@@ -120,16 +114,42 @@
     far_count,
     place_of,
     chosen,
+    column_far,
+    following,
+    previous,
+    opposite_first,
+    opposite_last,
+    ready_far,
+    own_far,
+    kept,
+    given,
+    logs,
     arrived,
     ready,
     own,
-    kept,
-    given,
-    logs,
     chosen_rows,
     spans,
+    semaphores,
 ):
     device, core = place_of[0], place_of[1]
+    half = opposite_first.shape[0]
+    loads = (
+        (ready_far, ready),
+        (own_far, own),
+        (column_far, arrived.at[0]),
+        (following, arrived.at[1]),
+        (opposite_first, arrived.at[2, :half]),
+        (opposite_last, arrived.at[2, half:]),
+        (previous, arrived.at[3]),
+    )
+    loads = [
+        pltpu.make_async_copy(source, target, semaphores.at[number])
+        for number, (source, target) in enumerate(loads)
+    ]
+    for load in loads:
+        load.start()
+    for load in loads:
+        load.wait()
     blocks, named = chosen.shape
     _, _, packed, _ = own.shape
     y_count, z_count, sent_rows, _ = arrived.shape
@@ -150,7 +170,7 @@
     slot = span_index % column_rows // span_rows
     near_count = z_count // far_count
     owner = (slot % far_count * near_count + slot // far_count) * y_count
-    owner = owner + span_index // column_rows
+    owner = owner + (device % y_count + span_index // column_rows) % y_count
     span_ends = owner * tok_rows + span_index % span_rows * CMP + CMP - 1
     rank = lax.broadcasted_iota(jnp.int32, (1, chosen_rows.shape[1]), 1) // packed
 
@@ -182,7 +202,7 @@
             chosen_rows[part, :packed] = own[part, block]
         for number in range(named):
             source = chosen[block, number]
-            z, y = source // y_count, source % y_count
+            z, y = source // y_count, (source + y_count - device % y_count) % y_count
             slot = z % near_count * far_count + z // near_count
             for part in range(2):
                 chosen_rows[part, (number + 1) * packed : (number + 2) * packed] = arrived[
@@ -287,12 +307,21 @@
     )
     far = lax.all_gather(sent, "z_far", axis=0, tiled=True)
     column = lax.all_gather(far, "z_near", axis=0, tiled=True)
-    arrived = spread(column, "y").reshape(y_count, z_count, sent_rows, 128)
-
-    tokens_later, own, cosines, sines, swap_weight, _ = lax.optimization_barrier(
-        (tokens, own, cosines, sines, out_weight, column)
-    )
-    other_weight = lax.ppermute(swap_weight, "core", [(0, 1), (1, 0)])
+    ahead = [(place, (place + 1) % y_count) for place in range(y_count)]
+    back = [(place, (place - 1) % y_count) for place in range(y_count)]
+    half_rows = column.shape[0] // 2
+    previous = lax.ppermute(column, "y", ahead)
+    following = lax.ppermute(column, "y", back)
+    opposite_first = lax.ppermute(previous[:half_rows], "y", ahead)
+    opposite_last = lax.ppermute(following[half_rows:], "y", back)
+    pieces = [
+        piece.reshape(-1, sent_rows, 128)
+        for piece in (column, following, previous, opposite_first, opposite_last)
+    ]
+
+    tokens_later, swap_weight, own, cosines, sines, _ = lax.optimization_barrier(
+        (tokens, out_weight, own, cosines, sines, column)
+    )
     ready = kernel_call(
         query_kernel,
         [smem] + [vmem] * 6,
@@ -310,13 +339,14 @@
         10**9,
         QUERY_ROOM,
     )
+    other_weight = lax.ppermute(swap_weight, "core", [(0, 1), (1, 0)])
     kept, given, log_weight = kernel_call(
         functools.partial(attention_kernel, far_count),
-        [smem, smem, vmem, vmem, vmem],
+        [smem, smem] + [pl.ANY] * 7,
         (
             jnp.stack([device, lax.axis_index("core")]),
             chosen_device,
-            arrived,
+            *pieces,
             ready,
             own,
         ),
@@ -326,8 +356,12 @@
             shape((2, tok_rows, head_count), f32),
         ),
         (
+            pltpu.VMEM((y_count, z_count, sent_rows, 128), bf16),
+            pltpu.VMEM(ready.shape, f32),
+            pltpu.VMEM(own.shape, bf16),
             pltpu.VMEM((2, (chosen_device.shape[1] + 1) * packed, 128), bf16),
             pltpu.VMEM((y_count * z_count * (sent_rows - SEL), 128), bf16),
+            pltpu.SemaphoreType.DMA((7,)),
         ),
         4 * 10**9,
         ATTENTION_ROOM,
@@ -341,8 +375,8 @@
     ).astype(bf16)
     pair_sum = (own_partial.astype(f32) + other_partial.astype(f32)).astype(bf16)
     pair_sum = pair_sum.reshape(local_blocks, packed, -1)
-    pieces = lax.all_to_all(pair_sum, "x", split_axis=0, concat_axis=0, tiled=True)
-    mixed_out = pieces.astype(f32).sum(axis=0).astype(bf16)
+    partials = lax.all_to_all(pair_sum, "x", split_axis=0, concat_axis=0, tiled=True)
+    mixed_out = partials.astype(f32).sum(axis=0).astype(bf16)
     return (mixed_out, log_weight)
 
 

time: 131 us -> 131 us (level)
  waiting for transfers between devices: 12.4 us -> 8.32 us
  starting transfers between devices: 32.1 us -> 35.1 us
  Pallas kernels: 13.4 us -> 16.4 us
  matrix products: 3.87 us -> 2.25 us
    ppermute x0 -> x4, starting transfers between devices: none -> 13.1 us  [the longest x1 4.54 us: shards(): opposite_last = lax.ppermute(following[half_rows:], 'y', back)]
    ppermute x1, starting transfers between devices: 12.4 us -> 6.43 us  [shards(): taken = lax.ppermute(given, 'core', [(0, 1), (1, 0)])]
    all_to_all x1 -> x0, starting transfers between devices: 4.17 us -> none  [spread(): return lax.all_to_all(copies, axis, split_axis=0, concat_axis=0, tiled=True)]
    all_to_all x1 -> x0, waiting for transfers between devices: 3.87 us -> none  [spread(): return lax.all_to_all(copies, axis, split_axis=0, concat_axis=0, tiled=True)]
    pallas_call x3, Pallas kernels: 13.4 us -> 16.4 us  [kernel_call(): pl.pallas_call(kernel, out_shape=outputs, in_specs=[pl.BlockSpec(memory_s...]
    broadcast_in_dim x1 -> x0, local copies, waits for them, and re-layouts: 1.71 us -> none  [spread(): jnp.broadcast_to(block[None], (count, *block.shape))]
  transfers between devices with their start and end apart: 4 -> 7, of which waited for: 2 -> 1; matrix products, arithmetic and copies ran while one was open for 2% -> 3% of each run, Pallas kernels for 8% -> 10%
where the time goes in v5:
time: 131 us; the launch traced here: 130 us
  blocking collectives  60.9 us (46%)
  starting transfers between devices  35.1 us (27%)
  Pallas kernels  16.4 us (13%)
  waiting for transfers between devices  8.32 us (6%)
  other arithmetic  3.31 us (3%)
  local copies, waits for them, and re-layouts  2.47 us (2%)
  matrix products  2.25 us (2%)
  between operations  1.47 us (1%)
    all_gather x1, blocking collectives, shards(): far = lax.all_gather(sent, 'z_far', axis=0, tiled=True)  47.6 us
    pallas_call x3, Pallas kernels, kernel_call(): pl.pallas_call(kernel, out_shape=outputs, in_specs=[pl.BlockSpec(memory_s...  16.4 us
    all_gather x1, blocking collectives, shards(): column = lax.all_gather(far, 'z_near', axis=0, tiled=True)  13.2 us
    ppermute x1, starting transfers between devices, shards(): other_weight = lax.ppermute(swap_weight, 'core', [(0, 1), (1, 0)])  11.4 us
    all_to_all x1, waiting for transfers between devices, shards(): lax.all_to_all(pair_sum, 'x', split_axis=0, concat_axis=0, tiled=True)  8.31 us
    ppermute x1, starting transfers between devices, shards(): taken = lax.ppermute(given, 'core', [(0, 1), (1, 0)])  6.43 us
    ppermute x1, starting transfers between devices, shards(): opposite_last = lax.ppermute(following[half_rows:], 'y', back)  4.54 us
    all_to_all x1, starting transfers between devices, shards(): lax.all_to_all(pair_sum, 'x', split_axis=0, concat_axis=0, tiled=True)  4.17 us
  transfers between devices with their start and end apart: 7, of which 1 were waited for; matrix products, arithmetic and copies ran while one was open for 3% of the time, Pallas kernels for 10%

profile of v5, /device:TPU:1, one launch (start us, length us, event | category | flops | bytes accessed | tf_op | source)
XLA Modules:
  0.0 130.2 jit_solution(9987121497974245737)
XLA Ops:
  1.3 1.2 multiply_sine_fusion
  2.5 0.0 copy-start
  2.6 3.1 %shard_map.113 = (bf16[72,128]{1,0:T(8,128)(2,1)}, bf16[2,4,32,128]{3,2,1,0:T(8,128)(2,1)}) custom-call(s32[1]{0:T(128)S(6)} %copy.13.pick, bf16[256,2048]{1,0:T(8,128)(2,1)} %tokens.2, bf16[64,2048]{1,0:T(8,128)(2,1)} %bitcast.26, bf16[64,2048]{1,0:T(8,128)(2,1)} %bitcast.27, f32[1,64]{1,0:T(1,128)} %bitcast.29, f32[256,32]{1,0:T(8,128)} %get-tuple-element.15.cosines, ...), custom_call_target="tpu_custom_call" | custom-call | flops 1000000000 | bytes 4194304 | tf_op jit(solution)/shard_map/pallas_call | solution.py:253
  5.7 47.6 %all_gather.6 = bf16[576,128]{1,0:T(8,128)(2,1)S(1)} all-gather(bf16[72,128]{1,0:T(8,128)(2,1)} %get-tuple-element.12), channel_id=1, replica_groups=mesh['z_far'=8,'z_near'=4,'y'=4,'x'=4,'core'=2] {'z_far'}, dimensions={0}, use_global_device_ids=true | all-gather | bytes 165888 | tf_op jit(solution)/shard_map/all_gather | solution.py:308
  53.3 13.2 %all_gather.7 = bf16[2304,128]{1,0:T(8,128)(2,1)S(1)} all-gather(bf16[576,128]{1,0:T(8,128)(2,1)S(1)} %all_gather.6), channel_id=1, replica_groups=mesh['z_far'=8,'z_near'=4,'y'=4,'x'=4,'core'=2] {'z_near'}, dimensions={0}, use_global_device_ids=true | all-gather | bytes 737280 | tf_op jit(solution)/shard_map/all_gather | solution.py:309
  66.5 0.0 copy-start.1
  66.6 3.0 %collective-permute-start.1 = (bf16[2304,128]{1,0:T(8,128)(2,1)S(1)}, bf16[2304,128]{1,0:T(8,128)(2,1)S(1)}, u32[]{:S(2)}, u32[]{:S(2)}) collective-permute-start(bf16[2304,128]{1,0:T(8,128)(2,1)S(1)} %all_gather.7), channel_id=1, source_target_pairs={{0,8},{8,16},{16,24},{24,0},{1,9},{9,17},{17,25},{25,1},{2,10},{10... | collective-permute-start | bytes 1769480 | tf_op jit(solution)/shard_map/ppermute | solution.py:313
  69.6 3.4 %collective-permute-start = (bf16[2304,128]{1,0:T(8,128)(2,1)S(1)}, bf16[2304,128]{1,0:T(8,128)(2,1)}, u32[]{:S(2)}, u32[]{:S(2)}) collective-permute-start(bf16[2304,128]{1,0:T(8,128)(2,1)S(1)} %all_gather.7), channel_id=1, source_target_pairs={{0,24},{8,0},{16,8},{24,16},{1,25},{9,1},{17,9},{25,17},{2,26},{10... | collective-permute-start | bytes 1769480 | tf_op jit(solution)/shard_map/ppermute | solution.py:314
  73.0 0.0 copy-done
  73.1 11.4 %collective-permute-start.5 = (bf16[256,2048]{1,0:T(8,128)(2,1)S(1)}, bf16[256,2048]{1,0:T(8,128)(2,1)S(1)}, u32[]{:S(2)}, u32[]{:S(2)}) collective-permute-start(bf16[256,2048]{1,0:T(8,128)(2,1)S(1)} %copy-done), channel_id=1, source_target_pairs={{0,1},{1,0},{2,3},{3,2},{4,5},{5,4},{6,7},{7,6},{8,9},{9,8},{10,11... | collective-permute-start | bytes 3145736 | tf_op jit(solution)/shard_map/ppermute | solution.py:342
  84.5 0.0 collective-permute-done.1
  84.5 0.0 copy-start.3
  84.5 0.0 copy-start.5
  84.5 2.1 %collective-permute-start.2 = (bf16[1152,128]{1,0:T(8,128)(2,1)S(1)}, bf16[1152,128]{1,0:T(8,128)(2,1)}, u32[]{:S(2)}, u32[]{:S(2)}) collective-permute-start(bf16[1152,128]{1,0:T(8,128)(2,1)S(1)} %slice.8), channel_id=1, source_target_pairs={{0,8},{8,16},{16,24},{24,0},{1,9},{9,17},{17,25},{25,1},{2,10},{10... | collective-permute-start | bytes 884744 | tf_op jit(solution)/shard_map/ppermute | solution.py:315
  86.6 0.0 copy-done.3
  86.6 0.0 collective-permute-done
  86.7 1.0 slice.9
  87.6 0.0 copy-done.1
  87.6 4.5 %collective-permute-start.3 = (bf16[1152,128]{1,0:T(8,128)(2,1)S(1)}, bf16[1152,128]{1,0:T(8,128)(2,1)S(1)}, u32[]{:S(2)}, u32[]{:S(2)}) collective-permute-start(bf16[1152,128]{1,0:T(8,128)(2,1)S(1)} %slice.9), channel_id=1, source_target_pairs={{0,24},{8,0},{16,8},{24,16},{1,25},{9,1},{17,9},{25,17},{2,26},{10... | collective-permute-start | bytes 884744 | tf_op jit(solution)/shard_map/ppermute | solution.py:316
  92.2 0.0 copy-done.5
  92.2 0.7 maximum_bitcast_fusion.gain
  92.9 3.6 %shard_map.114.ready_far = f32[5,256,128]{2,1,0:T(8,128)} custom-call(s32[1]{0:T(128)} %bitcast.10.group, bf16[256,2048]{1,0:T(8,128)(2,1)} %tokens.2, bf16[2048,256]{1,0:T(8,128)(2,1)} %query_weight.1, bf16[64,2048]{1,0:T(8,128)(2,1)} %bitcast.28, f32[1,128]{1,0:T(1,128)} %maximum_bitcast_fusion.gain, f32[256,32]{1,0:T(8,128)} %get-tuple-element.15.cosines, ...), custom_call_target="tpu_custom_call" | custom-call | flops 1000000000 | bytes 4194304 | tf_op jit(solution)/shard_map/pallas_call | solution.py:253
  96.5 0.7 pad_add_fusion.place_of
  97.2 0.0 collective-permute-done.2
  97.2 0.0 collective-permute-done.3
  97.2 0.0 copy-start.4
  97.2 0.7 copy-done.4
  97.9 9.6 %shard_map.115 = (bf16[4,32,256]{2,1,0:T(8,128)(2,1)}, bf16[4,32,256]{2,1,0:T(8,128)(2,1)}, f32[2,256,4]{2,1,0:T(8,128)}) custom-call(s32[2]{0:T(128)} %pad_add_fusion.place_of, s32[4,15]{1,0:T(4,128)} %chosen.1, bf16[32,72,128]{2,1,0:T(8,128)(2,1)} %bitcast.21, bf16[32,72,128]{2,1,0:T(8,128)(2,1)} %bitcast.6.following, bf16[32,72,128]{2,1,0:T(8,128)(2,1)} %bitcast.22, ...), custom_call_target="tpu_custom_call" | custom-call | flops 4000000000 | bytes 4194304 | tf_op jit(solution)/shard_map/pallas_call | solution.py:253
  107.5 6.4 %collective-permute-start.4 = (bf16[4,32,256]{2,1,0:T(8,128)(2,1)}, bf16[4,32,256]{2,1,0:T(8,128)(2,1)S(1)}, u32[]{:S(2)}, u32[]{:S(2)}) collective-permute-start(bf16[4,32,256]{2,1,0:T(8,128)(2,1)} %get-tuple-element.19), channel_id=1, source_target_pairs={{0,1},{1,0},{2,3},{3,2},{4,5},{5,4},{6,7},{7,6},{8,9},{9,8},{10,11... | collective-permute-start | bytes 196616 | tf_op jit(solution)/shard_map/ppermute | solution.py:369
  114.0 1.1 fusion.3
  115.1 0.0 collective-permute-done.4
  115.1 0.0 collective-permute-done.5
  115.2 1.1 fusion.2
  116.3 0.0 copy-start.2
  116.3 4.2 %all-to-all-start = ((bf16[4,32,2048]{2,1,0:T(8,128)(2,1)}), bf16[4,32,2048]{2,1,0:T(8,128)(2,1)S(1)}, u32[]{:S(2)}, u32[]{:S(2)}) async-start(bf16[4,32,2048]{2,1,0:T(8,128)(2,1)} %bitcast.15), calls=%async_computation | async-start | bytes 1048576 | tf_op jit(solution)/shard_map/all_to_all | solution.py:378
  120.4 0.0 copy-done.2
  120.4 0.7 copy.12
  121.1 8.3 %all-to-all-done = bf16[4,32,2048]{2,1,0:T(8,128)(2,1)S(1)} async-done(((bf16[4,32,2048]{2,1,0:T(8,128)(2,1)}), bf16[4,32,2048]{2,1,0:T(8,128)(2,1)S(1)}, u32[]{:S(2)}, u32[]{:S(2)}) %all-to-all-start) | async-done | bytes 524320 | tf_op jit(solution)/shard_map/all_to_all | solution.py:378
  129.5 0.7 reduce_sum.12
  (3 shorter events, 0.0 us)
Async XLA Ops:
  2.5 70.5 %copy-start = (bf16[256,2048]{1,0:T(8,128)(2,1)S(1)}, bf16[256,2048]{1,0:T(8,128)(2,1)}, u32[]{:S(2)}) copy-start(bf16[256,2048]{1,0:T(8,128)(2,1)} %param.17) | copy-start | bytes 3145732
  66.5 21.1 %copy-start.1 = (bf16[2304,128]{1,0:T(8,128)(2,1)}, bf16[2304,128]{1,0:T(8,128)(2,1)S(1)}, u32[]{:S(2)}) copy-start(bf16[2304,128]{1,0:T(8,128)(2,1)S(1)} %all_gather.7) | copy-start | bytes 1769476
  66.6 17.9 %collective-permute-start.1 = (bf16[2304,128]{1,0:T(8,128)(2,1)S(1)}, bf16[2304,128]{1,0:T(8,128)(2,1)S(1)}, u32[]{:S(2)}, u32[]{:S(2)}) collective-permute-start(bf16[2304,128]{1,0:T(8,128)(2,1)S(1)} %all_gather.7), channel_id=1, source_target_pairs={{0,8},{8,16},{16,24},{24,0},{1,9},{9,17},{17,25},{25,1},{2,10},{10... | collective-permute-start | bytes 1769480 | tf_op jit(solution)/shard_map/ppermute | solution.py:313
  69.6 17.0 %collective-permute-start = (bf16[2304,128]{1,0:T(8,128)(2,1)S(1)}, bf16[2304,128]{1,0:T(8,128)(2,1)}, u32[]{:S(2)}, u32[]{:S(2)}) collective-permute-start(bf16[2304,128]{1,0:T(8,128)(2,1)S(1)} %all_gather.7), channel_id=1, source_target_pairs={{0,24},{8,0},{16,8},{24,16},{1,25},{9,1},{17,9},{25,17},{2,26},{10... | collective-permute-start | bytes 1769480 | tf_op jit(solution)/shard_map/ppermute | solution.py:314
  73.1 42.1 %collective-permute-start.5 = (bf16[256,2048]{1,0:T(8,128)(2,1)S(1)}, bf16[256,2048]{1,0:T(8,128)(2,1)S(1)}, u32[]{:S(2)}, u32[]{:S(2)}) collective-permute-start(bf16[256,2048]{1,0:T(8,128)(2,1)S(1)} %copy-done), channel_id=1, source_target_pairs={{0,1},{1,0},{2,3},{3,2},{4,5},{5,4},{6,7},{7,6},{8,9},{9,8},{10,11... | collective-permute-start | bytes 3145736 | tf_op jit(solution)/shard_map/ppermute | solution.py:342
  84.5 2.2 %copy-start.3 = (bf16[2304,128]{1,0:T(8,128)(2,1)}, bf16[2304,128]{1,0:T(8,128)(2,1)S(1)}, u32[]{:S(2)}) copy-start(bf16[2304,128]{1,0:T(8,128)(2,1)S(1)} %collective-permute-done.1) | copy-start | bytes 1769476
  84.5 7.7 %copy-start.5 = (f32[64]{0:T(128)S(1)}, f32[64]{0:T(128)}, u32[]{:S(2)}) copy-start(f32[64]{0:T(128)} %param.15) | copy-start | bytes 772
  84.5 12.6 %collective-permute-start.2 = (bf16[1152,128]{1,0:T(8,128)(2,1)S(1)}, bf16[1152,128]{1,0:T(8,128)(2,1)}, u32[]{:S(2)}, u32[]{:S(2)}) collective-permute-start(bf16[1152,128]{1,0:T(8,128)(2,1)S(1)} %slice.8), channel_id=1, source_target_pairs={{0,8},{8,16},{16,24},{24,0},{1,9},{9,17},{17,25},{25,1},{2,10},{10... | collective-permute-start | bytes 884744 | tf_op jit(solution)/shard_map/ppermute | solution.py:315
  87.6 9.5 %collective-permute-start.3 = (bf16[1152,128]{1,0:T(8,128)(2,1)S(1)}, bf16[1152,128]{1,0:T(8,128)(2,1)S(1)}, u32[]{:S(2)}, u32[]{:S(2)}) collective-permute-start(bf16[1152,128]{1,0:T(8,128)(2,1)S(1)} %slice.9), channel_id=1, source_target_pairs={{0,24},{8,0},{16,8},{24,16},{1,25},{9,1},{17,9},{25,17},{2,26},{10... | collective-permute-start | bytes 884744 | tf_op jit(solution)/shard_map/ppermute | solution.py:316
  97.2 0.7 copy-start.4
  107.5 7.6 %collective-permute-start.4 = (bf16[4,32,256]{2,1,0:T(8,128)(2,1)}, bf16[4,32,256]{2,1,0:T(8,128)(2,1)S(1)}, u32[]{:S(2)}, u32[]{:S(2)}) collective-permute-start(bf16[4,32,256]{2,1,0:T(8,128)(2,1)} %get-tuple-element.19), channel_id=1, source_target_pairs={{0,1},{1,0},{2,3},{3,2},{4,5},{5,4},{6,7},{7,6},{8,9},{9,8},{10,11... | collective-permute-start | bytes 196616 | tf_op jit(solution)/shard_map/ppermute | solution.py:369
  116.3 4.2 %copy-start.2 = (f32[2,256,4]{2,1,0:T(8,128)S(1)}, f32[2,256,4]{2,1,0:T(8,128)}, u32[]{:S(2)}) copy-start(f32[2,256,4]{2,1,0:T(8,128)} %get-tuple-element.23) | copy-start | bytes 24580
  116.3 13.2 %all-to-all-start = ((bf16[4,32,2048]{2,1,0:T(8,128)(2,1)}), bf16[4,32,2048]{2,1,0:T(8,128)(2,1)S(1)}, u32[]{:S(2)}, u32[]{:S(2)}) async-start(bf16[4,32,2048]{2,1,0:T(8,128)(2,1)} %bitcast.15), calls=%async_computation | async-start | bytes 1048576 | tf_op jit(solution)/shard_map/all_to_all | solution.py:378

commit v6 on v4

--- a/solution.py
+++ b/solution.py
@@ -2,6 +2,7 @@
 
 import jax
 import jax.numpy as jnp
+import numpy as np
 from jax import lax
 from jax.experimental import pallas as pl
 from jax.experimental.pallas import tpu as pltpu
@@ -48,7 +49,13 @@
     )
 
 
-def key_kernel(pick, tokens, key_weight, value_weight, gain, cosines, sines, sent, own):
+def turns_of(start, within):
+    cosines = start[0:1] * within[0] - start[1:2] * within[1]
+    sines = start[1:2] * within[0] + start[0:1] * within[1]
+    return cosines, sines
+
+
+def key_kernel(pick, tokens, key_weight, value_weight, gain, start, within, sent, own):
     _, blocks, packed, _ = own.shape
     tok_rows = tokens.shape[0]
     block_len = 2 * packed
@@ -58,9 +65,8 @@
     square = jnp.mean(keys * keys, axis=-1, keepdims=True)
     plain = (keys * lax.rsqrt(square + norm_eps) * gain[...]).astype(jnp.bfloat16)
     plain = plain.astype(jnp.float32)
-    turned = plain * repeated(cosines[...], (1, 1)) + swapped(plain) * repeated(
-        sines[...], (-1, 1)
-    )
+    cosines, sines = turns_of(start[...], within[...])
+    turned = plain * repeated(cosines, (1, 1)) + swapped(plain) * repeated(sines, (-1, 1))
     turned = turned.astype(jnp.bfloat16)
     for block in range(blocks):
         rows = slice(block * block_len, (block + 1) * block_len)
@@ -73,7 +79,7 @@
     sent[block_len:] = spans.astype(jnp.bfloat16)
 
 
-def query_kernel(group, tokens, query_weight, gate_weight, gain, cosines, sines, ready):
+def query_kernel(group, tokens, query_weight, gate_weight, gain, turn_start, within, ready):
     tok_rows = tokens.shape[0]
     width = query_weight.shape[1]
     gate_count = 2 * (width // 64)
@@ -82,8 +88,9 @@
         dot_last(tokens[...], gate_weight[pl.ds(start, gate_count), :].astype(jnp.bfloat16))
     )
     lanes = lax.broadcasted_iota(jnp.int32, (tok_rows, 128), 1)
-    cos_lanes = repeated(cosines[...], (1, 1, 1, 1))
-    sin_lanes = repeated(sines[...], (-1, 1, -1, 1))
+    cosines, sines = turns_of(turn_start[...], within[...])
+    cos_lanes = repeated(cosines, (1, 1, 1, 1))
+    sin_lanes = repeated(sines, (-1, 1, -1, 1))
     for pair in range(width // 128):
         queries = jnp.dot(
             tokens[...],
@@ -128,6 +135,8 @@
     logs,
     chosen_rows,
     spans,
+    span_part,
+    span_log,
 ):
     device, core = place_of[0], place_of[1]
     blocks, named = chosen.shape
@@ -138,21 +147,35 @@
     heads = 2 * pairs
     tok_rows = blocks * block_len
     span_rows = sent_rows - block_len
+    near_count = z_count // far_count
     score_scale = 64 ** (-0.5)
-    column_rows = z_count * span_rows
-    for y in range(y_count):
-        column = arrived[y, :, block_len:, :].astype(jnp.float32)
-        spans[y * column_rows : (y + 1) * column_rows] = column.reshape(column_rows, 128).astype(
-            jnp.bfloat16
+    all_spans = spans.shape[0]
+    all_rows = chosen_rows.shape[1]
+
+    def slot_of(z):
+        return z % near_count * far_count + z // near_count
+
+    for z in range(z_count):
+        plane = jnp.concatenate(
+            [
+                arrived[y, slot_of(z), block_len:, :].astype(jnp.float32)
+                for y in range(y_count)
+            ],
+            axis=0,
         )
+        spans[z * y_count * span_rows : (z + 1) * y_count * span_rows] = plane.astype(jnp.bfloat16)
+    chosen_rows[...] = jnp.zeros_like(chosen_rows)
     row_place = lax.broadcasted_iota(jnp.int32, (heads * block_len, 1), 0) % block_len
-    span_index = lax.broadcasted_iota(jnp.int32, (1, y_count * column_rows), 1)
-    slot = span_index % column_rows // span_rows
-    near_count = z_count // far_count
-    owner = (slot % far_count * near_count + slot // far_count) * y_count
-    owner = owner + span_index // column_rows
-    span_ends = owner * tok_rows + span_index % span_rows * CMP + CMP - 1
-    rank = lax.broadcasted_iota(jnp.int32, (1, chosen_rows.shape[1]), 1) // packed
+
+    def in_width(count, widths, branch):
+        least = 0
+        for width, most in widths:
+
+            @pl.when((count >= least) & (count < most))
+            def _():
+                branch(width)
+
+            least = most
 
     @pl.loop(0, blocks)
     def _(block):
@@ -164,69 +187,100 @@
             )
             for b in range(2)
         ]
-        scores = dot_last(
-            one_sided([ready[pair, rows, :] for pair in range(pairs)], False), spans[...]
+
+        def span_branch(width):
+            scores = dot_last(
+                one_sided([ready[pair, rows, :] for pair in range(pairs)], False), spans[:width]
+            )
+            places = device * tok_rows + block * block_len + row_place
+            has_span = places >= CMP - 1
+            span_ends = lax.broadcasted_iota(jnp.int32, (1, width), 1) * CMP + CMP - 1
+            scores = jnp.where(span_ends <= places, scores * score_scale, big_negative)
+            peak = jnp.max(scores, axis=-1, keepdims=True)
+            raw = jnp.exp(scores - peak)
+            total = jnp.where(has_span, jnp.sum(raw, axis=-1, keepdims=True), 1.0)
+            summed = jnp.dot(
+                raw.astype(jnp.bfloat16), spans[:width], preferred_element_type=jnp.float32
+            )
+            span_part[...] = jnp.where(has_span, gate_of[0] * (summed[:, 64:] / total), 0.0)
+            span_log[...] = jnp.where(has_span, peak + jnp.log(total), 0.0)
+
+        in_width(
+            (device + 1) * span_rows - 1,
+            [(width, width) for width in (all_spans // 4, all_spans // 2, all_spans)],
+            span_branch,
         )
-        places = device * tok_rows + block * block_len + row_place
-        has_span = places >= CMP - 1
-        scores = jnp.where(span_ends <= places, scores * score_scale, big_negative)
-        peak = jnp.max(scores, axis=-1, keepdims=True)
-        raw = jnp.exp(scores - peak)
-        total = jnp.where(has_span, jnp.sum(raw, axis=-1, keepdims=True), 1.0)
-        summed = jnp.dot(raw.astype(jnp.bfloat16), spans[...], preferred_element_type=jnp.float32)
-        mixed_spans = jnp.where(has_span, gate_of[0] * (summed[:, 64:] / total), 0.0)
-        span_log = jnp.where(has_span, peak + jnp.log(total), 0.0)
-
-        blocked = jnp.zeros(rank.shape, jnp.float32)
+
         for part in range(2):
             chosen_rows[part, :packed] = own[part, block]
+        counted = jnp.int32(1)
         for number in range(named):
             source = chosen[block, number]
-            z, y = source // y_count, source % y_count
-            slot = z % near_count * far_count + z // near_count
-            for part in range(2):
-                chosen_rows[part, (number + 1) * packed : (number + 2) * packed] = arrived[
-                    y, slot, part * packed : (part + 1) * packed, :
-                ]
-            bias = jnp.where(source < device, 0.0, big_negative)
-            blocked = jnp.where(rank == number + 1, bias, blocked)
-        half_scores = []
-        lanes = lax.broadcasted_iota(jnp.int32, (heads * block_len, chosen_rows.shape[1]), 1)
+            start = pl.multiple_of(counted * packed, packed)
+
+            @pl.when(source < device)
+            def _():
+                for part in range(2):
+                    chosen_rows[part, pl.ds(start, packed)] = arrived[
+                        source % y_count,
+                        slot_of(source // y_count),
+                        part * packed : (part + 1) * packed,
+                        :,
+                    ]
+
+            counted = counted + jnp.where(source < device, 1, 0)
         queries = [ready[pairs + pair, rows, :] for pair in range(pairs)]
-        for upper in (False, True):
-            scores = dot_last(one_sided(queries, upper), chosen_rows[0])
-            scores = scores * score_scale + blocked
-            later = (lanes < packed) & (lanes + packed * upper > row_place)
-            half_scores.append(jnp.where(later, big_negative, scores))
-        peak = jnp.maximum(
-            jnp.max(half_scores[0], axis=-1, keepdims=True),
-            jnp.max(half_scores[1], axis=-1, keepdims=True),
+
+        def chosen_branch(width):
+            half_scores = []
+            lanes = lax.broadcasted_iota(jnp.int32, (heads * block_len, width), 1)
+            blocked = jnp.where(lanes[:1] < counted * packed, 0.0, big_negative)
+            for upper in (False, True):
+                scores = dot_last(one_sided(queries, upper), chosen_rows[0, :width])
+                scores = scores * score_scale + blocked
+                later = (lanes < packed) & (lanes + packed * upper > row_place)
+                half_scores.append(jnp.where(later, big_negative, scores))
+            peak = jnp.maximum(
+                jnp.max(half_scores[0], axis=-1, keepdims=True),
+                jnp.max(half_scores[1], axis=-1, keepdims=True),
+            )
+            total = 0.0
+            products = []
+            for upper in range(2):
+                raw = jnp.exp(half_scores[upper] - peak)
+                total = total + jnp.sum(raw, axis=-1, keepdims=True)
+                products.append(
+                    jnp.dot(
+                        raw.astype(jnp.bfloat16),
+                        chosen_rows[1, :width],
+                        preferred_element_type=jnp.float32,
+                    )
+                )
+            summed = products[0][:, :64] + products[1][:, 64:]
+            mixed = span_part[...] + gate_of[1] * (summed / total)
+            chosen_log = peak + jnp.log(total)
+            for pair in range(pairs):
+                first = mixed[2 * pair * block_len : (2 * pair + 1) * block_len]
+                second = mixed[(2 * pair + 1) * block_len : (2 * pair + 2) * block_len]
+                both = jnp.concatenate([first, second], axis=1)
+                lower, upper = both[:packed], both[packed:]
+                lane_range = slice(pair * 128, (pair + 1) * 128)
+                kept[block, :, lane_range] = jnp.where(core == 0, lower, upper).astype(
+                    jnp.bfloat16
+                )
+                given[block, :, lane_range] = jnp.where(core == 0, upper, lower).astype(
+                    jnp.bfloat16
+                )
+            for head in range(heads):
+                piece = slice(head * block_len, (head + 1) * block_len)
+                logs[0, rows, head : head + 1] = span_log[piece]
+                logs[1, rows, head : head + 1] = chosen_log[piece]
+
+        in_width(
+            counted - 1,
+            [(width, width // packed) for width in (all_rows // 4, all_rows // 2, all_rows)],
+            chosen_branch,
         )
-        total = 0.0
-        products = []
-        for upper in range(2):
-            raw = jnp.exp(half_scores[upper] - peak)
-            total = total + jnp.sum(raw, axis=-1, keepdims=True)
-            products.append(
-                jnp.dot(
-                    raw.astype(jnp.bfloat16), chosen_rows[1], preferred_element_type=jnp.float32
-                )
-            )
-        summed = products[0][:, :64] + products[1][:, 64:]
-        mixed = mixed_spans + gate_of[1] * (summed / total)
-        chosen_log = peak + jnp.log(total)
-        for pair in range(pairs):
-            first = mixed[2 * pair * block_len : (2 * pair + 1) * block_len]
-            second = mixed[(2 * pair + 1) * block_len : (2 * pair + 2) * block_len]
-            both = jnp.concatenate([first, second], axis=1)
-            lower, upper = both[:packed], both[packed:]
-            lane_range = slice(pair * 128, (pair + 1) * 128)
-            kept[block, :, lane_range] = jnp.where(core == 0, lower, upper).astype(jnp.bfloat16)
-            given[block, :, lane_range] = jnp.where(core == 0, upper, lower).astype(jnp.bfloat16)
-        for head in range(heads):
-            piece = slice(head * block_len, (head + 1) * block_len)
-            logs[0, rows, head : head + 1] = span_log[piece]
-            logs[1, rows, head : head + 1] = chosen_log[piece]
 
 
 def kernel_call(kernel, specs, operands, outputs, scratch, flops, room):
@@ -241,11 +295,15 @@
     )(*operands)
 
 
-def turns(places, head_size):
+def turns(first_place, tok_rows, head_size):
     half_size = head_size // 2
-    inverse = jnp.power(rope_base, -jnp.arange(half_size, dtype=jnp.float32) * 2.0 / head_size)
-    angles = places.astype(jnp.float32)[:, None] * inverse[None, :]
-    return jnp.cos(angles), jnp.sin(angles)
+    exact = rope_base ** (-np.arange(half_size) * 2.0 / head_size)
+    within = np.arange(tok_rows)[:, None] * exact[None, :]
+    start = first_place.astype(jnp.float32) * exact.astype(np.float32)
+    return (
+        jnp.stack([jnp.cos(start), jnp.sin(start)]),
+        jnp.asarray(np.stack([np.cos(within), np.sin(within)]).astype(np.float32)),
+    )
 
 
 def shards(
@@ -270,8 +328,7 @@
     far_count, near_count, y_count = (lax.axis_size(axis) for axis in KV)
     z_count = far_count * near_count
     sent_rows = SEL + tok_rows // CMP
-    places = device * tok_rows + jnp.arange(tok_rows, dtype=jnp.int32)
-    cosines, sines = turns(places, head_size)
+    turn_start, within = turns(device * tok_rows, tok_rows, head_size)
     bf16, f32 = jnp.bfloat16, jnp.float32
     shape = jax.ShapeDtypeStruct
     vmem, smem = pltpu.VMEM, pltpu.SMEM
@@ -279,7 +336,7 @@
     sent, own = kernel_call(
         key_kernel,
         [smem] + [vmem] * 6,
-        (shared_block, tokens, key_weight.T, value_weight.T, key_gain[None], cosines, sines),
+        (shared_block, tokens, key_weight.T, value_weight.T, key_gain[None], turn_start, within),
         (shape((sent_rows, 128), bf16), shape((2, local_blocks, packed, 128), bf16)),
         (),
         10**9,
@@ -289,8 +346,8 @@
     column = lax.all_gather(far, "z_near", axis=0, tiled=True)
     arrived = spread(column, "y").reshape(y_count, z_count, sent_rows, 128)
 
-    tokens_later, own, cosines, sines, swap_weight, _ = lax.optimization_barrier(
-        (tokens, own, cosines, sines, out_weight, column)
+    tokens_later, own, turn_start, swap_weight, _ = lax.optimization_barrier(
+        (tokens, own, turn_start, out_weight, column)
     )
     other_weight = lax.ppermute(swap_weight, "core", [(0, 1), (1, 0)])
     ready = kernel_call(
@@ -302,8 +359,8 @@
             query_weight,
             gate_weight.T,
             jnp.concatenate([query_gain, query_gain])[None],
-            cosines,
-            sines,
+            turn_start,
+            within,
         ),
         shape((2 * (width // 128) + 1, tok_rows, 128), f32),
         (),
@@ -328,6 +385,8 @@
         (
             pltpu.VMEM((2, (chosen_device.shape[1] + 1) * packed, 128), bf16),
             pltpu.VMEM((y_count * z_count * (sent_rows - SEL), 128), bf16),
+            pltpu.VMEM((head_count * SEL, head_size), f32),
+            pltpu.VMEM((head_count * SEL, 1), f32),
         ),
         4 * 10**9,
         ATTENTION_ROOM,

time: 131 us -> 130 us (level)
  no operation moved by 1% of the time
where the time goes in v6:
time: 130 us
  blocking collectives  60.7 us (47%)
  starting transfers between devices  32 us (25%)
  Pallas kernels  12.9 us (10%)
  waiting for transfers between devices  12.7 us (10%)
  matrix products  3.87 us (3%)
  local copies, waits for them, and re-layouts  3.52 us (3%)
  other arithmetic  2.71 us (2%)
  between operations  1.35 us (1%)
    all_gather x1, blocking collectives, shards(): far = lax.all_gather(sent, 'z_far', axis=0, tiled=True)  47.6 us
    all_gather x1, blocking collectives, shards(): column = lax.all_gather(far, 'z_near', axis=0, tiled=True)  13.1 us
    pallas_call x3, Pallas kernels, kernel_call(): pl.pallas_call(kernel, out_shape=outputs, in_specs=[pl.BlockSpec(memory_s...  12.9 us
    ppermute x1, starting transfers between devices, shards(): taken = lax.ppermute(given, 'core', [(0, 1), (1, 0)])  12.3 us
    ppermute x1, starting transfers between devices, shards(): other_weight = lax.ppermute(swap_weight, 'core', [(0, 1), (1, 0)])  11.2 us
    all_to_all x1, waiting for transfers between devices, shards(): lax.all_to_all(pair_sum, 'x', split_axis=0, concat_axis=0, tiled=True)  8.57 us
    all_to_all x1, starting transfers between devices, spread(): return lax.all_to_all(copies, axis, split_axis=0, concat_axis=0, tiled=True)  4.51 us
    all_to_all x1, waiting for transfers between devices, spread(): return lax.all_to_all(copies, axis, split_axis=0, concat_axis=0, tiled=True)  4.14 us
  transfers between devices with their start and end apart: 4, of which 2 were waited for; matrix products, arithmetic and copies ran while one was open for 2% of the time, Pallas kernels for 8%

profile of v6, /device:TPU:1, one launch (start us, length us, event | category | flops | bytes accessed | tf_op | source)
XLA Modules:
  0.0 129.8 jit_solution(17870962011942639986)
XLA Ops:
  1.3 0.7 fusion.4
  2.0 0.6 pad_maximum_fusion.start.turn_start
  2.6 3.0 %shard_map.131 = (bf16[72,128]{1,0:T(8,128)(2,1)}, bf16[2,4,32,128]{3,2,1,0:T(8,128)(2,1)}) custom-call(s32[1]{0:T(128)S(6)} %copy.15.pick, bf16[256,2048]{1,0:T(8,128)(2,1)} %tokens.2, bf16[64,2048]{1,0:T(8,128)(2,1)} %bitcast.24, bf16[64,2048]{1,0:T(8,128)(2,1)} %bitcast.25, f32[1,64]{1,0:T(1,128)} %bitcast.27, f32[2,32]{1,0:T(2,128)} %pad_maximum_fusion.start.turn_start, ...), custom_call_target="tpu_custom_call" | custom-call | flops 1000000000 | bytes 4194304 | tf_op jit(solution)/shard_map/pallas_call | solution.py:287
  5.6 47.6 %all_gather.6 = bf16[576,128]{1,0:T(8,128)(2,1)S(1)} all-gather(bf16[72,128]{1,0:T(8,128)(2,1)} %get-tuple-element.11), channel_id=1, replica_groups=mesh['z_far'=8,'z_near'=4,'y'=4,'x'=4,'core'=2] {'z_far'}, dimensions={0}, use_global_device_ids=true | all-gather | bytes 165888 | tf_op jit(solution)/shard_map/all_gather | solution.py:345
  53.2 13.1 %all_gather.7 = bf16[2304,128]{1,0:T(8,128)(2,1)S(1)} all-gather(bf16[576,128]{1,0:T(8,128)(2,1)S(1)} %all_gather.6), channel_id=1, replica_groups=mesh['z_far'=8,'z_near'=4,'y'=4,'x'=4,'core'=2] {'z_near'}, dimensions={0}, use_global_device_ids=true | all-gather | bytes 737280 | tf_op jit(solution)/shard_map/all_gather | solution.py:346
  66.3 1.7 %broadcast_in_dim.13 = bf16[4,2304,128]{2,1,0:T(8,128)(2,1)} broadcast(bf16[2304,128]{1,0:T(8,128)(2,1)S(1)} %all_gather.7), dimensions={1,2} | broadcast | bytes 2949120 | tf_op jit(solution)/shard_map/broadcast_in_dim | solution.py:28
  68.0 0.0 copy-start.3
  68.0 4.5 %all-to-all-start = ((bf16[4,2304,128]{2,1,0:T(8,128)(2,1)}), bf16[4,2304,128]{2,1,0:T(8,128)(2,1)S(1)}, u32[]{:S(2)}, u32[]{:S(2)}) async-start(bf16[4,2304,128]{2,1,0:T(8,128)(2,1)} %broadcast_in_dim.13), calls=%async_computation | async-start | bytes 4718592 | tf_op jit(solution)/shard_map/all_to_all | solution.py:29
  72.6 0.0 copy-start
  72.6 0.0 copy-start.2
  72.6 11.2 %collective-permute-start.1 = (bf16[256,2048]{1,0:T(8,128)(2,1)}, bf16[256,2048]{1,0:T(8,128)(2,1)}, u32[]{:S(2)}, u32[]{:S(2)}) collective-permute-start(bf16[256,2048]{1,0:T(8,128)(2,1)} %param.19), channel_id=1, source_target_pairs={{0,1},{1,0},{2,3},{3,2},{4,5},{5,4},{6,7},{7,6},{8,9},{9,8},{10,11... | collective-permute-start | bytes 3145736 | tf_op jit(solution)/shard_map/ppermute | solution.py:352
  83.8 0.0 copy-done.3
  83.8 0.6 maximum_bitcast_fusion.gain
  84.4 3.7 %shard_map.132.ready = f32[5,256,128]{2,1,0:T(8,128)} custom-call(s32[1]{0:T(128)} %bitcast.8.group, bf16[256,2048]{1,0:T(8,128)(2,1)} %tokens.2, bf16[2048,256]{1,0:T(8,128)(2,1)} %query_weight.1, bf16[64,2048]{1,0:T(8,128)(2,1)} %bitcast.26, f32[1,128]{1,0:T(1,128)} %maximum_bitcast_fusion.gain, f32[2,32]{1,0:T(2,128)} %pad_maximum_fusion.start.turn_start, ...), custom_call_target="tpu_custom_call" | custom-call | flops 1000000000 | bytes 4194304 | tf_op jit(solution)/shard_map/pallas_call | solution.py:287
  88.1 0.1 pad_add_fusion.place_of
  88.2 4.1 %all-to-all-done = bf16[4,2304,128]{2,1,0:T(8,128)(2,1)S(1)} async-done(((bf16[4,2304,128]{2,1,0:T(8,128)(2,1)}), bf16[4,2304,128]{2,1,0:T(8,128)(2,1)S(1)}, u32[]{:S(2)}, u32[]{:S(2)}) %all-to-all-start) | async-done | bytes 2359328 | tf_op jit(solution)/shard_map/all_to_all | solution.py:29
  92.3 0.0 copy-done
  92.3 0.0 copy-done.2
  92.3 0.0 copy-start.1
  92.3 1.1 copy-done.1
  93.4 6.2 %shard_map.133 = (bf16[4,32,256]{2,1,0:T(8,128)(2,1)S(1)}, bf16[4,32,256]{2,1,0:T(8,128)(2,1)S(1)}, f32[2,256,4]{2,1,0:T(8,128)S(1)}) custom-call(s32[2]{0:T(128)S(1)} %pad_add_fusion.place_of, s32[4,15]{1,0:T(4,128)S(1)} %copy-done, bf16[4,32,72,128]{3,2,1,0:T(8,128)(2,1)S(1)} %bitcast.21, f32[5,256,128]{2,1,0:T(8,128)S(1)} %copy-done.1, ...), custom_call_target="tpu_custom_call" | custom-call | flops 4000000000 | bytes 4194304 | tf_op jit(solution)/shard_map/pallas_call | solution.py:287
  99.6 12.3 %collective-permute-start = (bf16[4,32,256]{2,1,0:T(8,128)(2,1)S(1)}, bf16[4,32,256]{2,1,0:T(8,128)(2,1)S(1)}, u32[]{:S(2)}, u32[]{:S(2)}) collective-permute-start(bf16[4,32,256]{2,1,0:T(8,128)(2,1)S(1)} %get-tuple-element.17), channel_id=1, source_target_pairs={{0,1},{1,0},{2,3},{3,2},{4,5},{5,4},{6,7},{7,6},{8,9},{9,8},{10,11... | collective-permute-start | bytes 196616 | tf_op jit(solution)/shard_map/ppermute | solution.py:394
  111.9 1.5 %fusion.3 = f32[128,2048]{1,0:T(8,128)S(1)} fusion(bf16[128,256]{1,0:T(8,128)(2,1)S(1)} %bitcast.22, bf16[256,2048]{1,0:T(8,128)(2,1)} %param.19), kind=kOutput, calls=%fused_computation.5 | convolution fusion | flops 134742016 | bytes 2162688 | tf_op jit(solution)/shard_map/dot_general | solution.py:395
  113.4 0.0 collective-permute-done.1
  113.4 0.0 collective-permute-done
  113.4 2.3 %fusion.2 = bf16[128,2048]{1,0:T(8,128)(2,1)} fusion(f32[128,2048]{1,0:T(8,128)S(1)} %fusion.3, bf16[128,256]{1,0:T(8,128)(2,1)S(1)} %bitcast.23, bf16[256,2048]{1,0:T(8,128)(2,1)} %collective-permute-done.1), kind=kOutput, calls=%fused_computation.3 | convolution fusion | flops 135266304 | bytes 2686976 | tf_op jit(solution)/shard_map/dot_general | solution.py:398
  115.8 4.0 %all-to-all-start.1 = ((bf16[4,32,2048]{2,1,0:T(8,128)(2,1)}), bf16[4,32,2048]{2,1,0:T(8,128)(2,1)S(1)}, u32[]{:S(2)}, u32[]{:S(2)}) async-start(bf16[4,32,2048]{2,1,0:T(8,128)(2,1)} %bitcast.13), calls=%async_computation.1 | async-start | bytes 1048576 | tf_op jit(solution)/shard_map/all_to_all | solution.py:403
  119.7 0.7 copy.14
  120.4 8.6 %all-to-all-done.1 = bf16[4,32,2048]{2,1,0:T(8,128)(2,1)S(1)} async-done(((bf16[4,32,2048]{2,1,0:T(8,128)(2,1)}), bf16[4,32,2048]{2,1,0:T(8,128)(2,1)S(1)}, u32[]{:S(2)}, u32[]{:S(2)}) %all-to-all-start.1) | async-done | bytes 524320 | tf_op jit(solution)/shard_map/all_to_all | solution.py:403
  129.0 0.7 reduce_sum.12
Async XLA Ops:
  68.0 15.8 %copy-start.3 = (f32[64]{0:T(128)S(1)}, f32[64]{0:T(128)}, u32[]{:S(2)}) copy-start(f32[64]{0:T(128)} %param.17) | copy-start | bytes 772
  68.0 24.3 %all-to-all-start = ((bf16[4,2304,128]{2,1,0:T(8,128)(2,1)}), bf16[4,2304,128]{2,1,0:T(8,128)(2,1)S(1)}, u32[]{:S(2)}, u32[]{:S(2)}) async-start(bf16[4,2304,128]{2,1,0:T(8,128)(2,1)} %broadcast_in_dim.13), calls=%async_computation | async-start | bytes 4718592 | tf_op jit(solution)/shard_map/all_to_all | solution.py:29
  72.6 19.7 %copy-start = (s32[4,15]{1,0:T(4,128)S(1)}, s32[4,15]{1,0:T(4,128)}, u32[]{:S(2)}) copy-start(s32[4,15]{1,0:T(4,128)} %chosen.1) | copy-start | bytes 724
  72.6 19.7 %copy-start.2 = (bf16[2,4,32,128]{3,2,1,0:T(8,128)(2,1)S(1)}, bf16[2,4,32,128]{3,2,1,0:T(8,128)(2,1)}, u32[]{:S(2)}) copy-start(bf16[2,4,32,128]{3,2,1,0:T(8,128)(2,1)} %get-tuple-element.15.own) | copy-start | bytes 196612
  72.6 40.9 %collective-permute-start.1 = (bf16[256,2048]{1,0:T(8,128)(2,1)}, bf16[256,2048]{1,0:T(8,128)(2,1)}, u32[]{:S(2)}, u32[]{:S(2)}) collective-permute-start(bf16[256,2048]{1,0:T(8,128)(2,1)} %param.19), channel_id=1, source_target_pairs={{0,1},{1,0},{2,3},{3,2},{4,5},{5,4},{6,7},{7,6},{8,9},{9,8},{10,11... | collective-permute-start | bytes 3145736 | tf_op jit(solution)/shard_map/ppermute | solution.py:352
  92.3 1.1 copy-start.1
  99.6 13.8 %collective-permute-start = (bf16[4,32,256]{2,1,0:T(8,128)(2,1)S(1)}, bf16[4,32,256]{2,1,0:T(8,128)(2,1)S(1)}, u32[]{:S(2)}, u32[]{:S(2)}) collective-permute-start(bf16[4,32,256]{2,1,0:T(8,128)(2,1)S(1)} %get-tuple-element.17), channel_id=1, source_target_pairs={{0,1},{1,0},{2,3},{3,2},{4,5},{5,4},{6,7},{7,6},{8,9},{9,8},{10,11... | collective-permute-start | bytes 196616 | tf_op jit(solution)/shard_map/ppermute | solution.py:394
  115.8 13.3 %all-to-all-start.1 = ((bf16[4,32,2048]{2,1,0:T(8,128)(2,1)}), bf16[4,32,2048]{2,1,0:T(8,128)(2,1)S(1)}, u32[]{:S(2)}, u32[]{:S(2)}) async-start(bf16[4,32,2048]{2,1,0:T(8,128)(2,1)} %bitcast.13), calls=%async_computation.1 | async-start | bytes 1048576 | tf_op jit(solution)/shard_map/all_to_all | solution.py:403

commit v7 on v6

--- a/solution.py
+++ b/solution.py
@@ -49,13 +49,13 @@
     )
 
 
-def turns_of(start, within):
-    cosines = start[0:1] * within[0] - start[1:2] * within[1]
-    sines = start[1:2] * within[0] + start[0:1] * within[1]
+def turns_of(start_cosines, start_sines, within):
+    cosines = start_cosines * within[0] - start_sines * within[1]
+    sines = start_sines * within[0] + start_cosines * within[1]
     return cosines, sines
 
 
-def key_kernel(pick, tokens, key_weight, value_weight, gain, start, within, sent, own):
+def key_kernel(pick, tokens, key_weight, value_weight, gain, start_cosines, start_sines, within, sent, own):
     _, blocks, packed, _ = own.shape
     tok_rows = tokens.shape[0]
     block_len = 2 * packed
@@ -65,7 +65,7 @@
     square = jnp.mean(keys * keys, axis=-1, keepdims=True)
     plain = (keys * lax.rsqrt(square + norm_eps) * gain[...]).astype(jnp.bfloat16)
     plain = plain.astype(jnp.float32)
-    cosines, sines = turns_of(start[...], within[...])
+    cosines, sines = turns_of(start_cosines[...], start_sines[...], within[...])
     turned = plain * repeated(cosines, (1, 1)) + swapped(plain) * repeated(sines, (-1, 1))
     turned = turned.astype(jnp.bfloat16)
     for block in range(blocks):
@@ -79,7 +79,7 @@
     sent[block_len:] = spans.astype(jnp.bfloat16)
 
 
-def query_kernel(group, tokens, query_weight, gate_weight, gain, turn_start, within, ready):
+def query_kernel(group, tokens, query_weight, gate_weight, gain, start_cosines, start_sines, within, ready):
     tok_rows = tokens.shape[0]
     width = query_weight.shape[1]
     gate_count = 2 * (width // 64)
@@ -88,7 +88,7 @@
         dot_last(tokens[...], gate_weight[pl.ds(start, gate_count), :].astype(jnp.bfloat16))
     )
     lanes = lax.broadcasted_iota(jnp.int32, (tok_rows, 128), 1)
-    cosines, sines = turns_of(turn_start[...], within[...])
+    cosines, sines = turns_of(start_cosines[...], start_sines[...], within[...])
     cos_lanes = repeated(cosines, (1, 1, 1, 1))
     sin_lanes = repeated(sines, (-1, 1, -1, 1))
     for pair in range(width // 128):
@@ -152,18 +152,31 @@
     all_spans = spans.shape[0]
     all_rows = chosen_rows.shape[1]
 
+    near_bits, y_bits = near_count.bit_length() - 1, y_count.bit_length() - 1
+
     def slot_of(z):
-        return z % near_count * far_count + z // near_count
-
-    for z in range(z_count):
-        plane = jnp.concatenate(
-            [
-                arrived[y, slot_of(z), block_len:, :].astype(jnp.float32)
-                for y in range(y_count)
-            ],
-            axis=0,
-        )
-        spans[z * y_count * span_rows : (z + 1) * y_count * span_rows] = plane.astype(jnp.bfloat16)
+        return (z & (near_count - 1)) * far_count + (z >> near_bits)
+
+    plane_rows = y_count * span_rows
+    for first in range(0, z_count, far_count):
+
+        @pl.when(first << y_bits <= device)
+        def _():
+            for z in range(first, first + far_count):
+                plane = jnp.concatenate(
+                    [
+                        arrived[y, slot_of(z), block_len:, :].astype(jnp.float32)
+                        for y in range(y_count)
+                    ],
+                    axis=0,
+                )
+                spans[z * plane_rows : (z + 1) * plane_rows] = plane.astype(jnp.bfloat16)
+
+        @pl.when(first << y_bits > device)
+        def _():
+            rows = slice(first * plane_rows, (first + far_count) * plane_rows)
+            spans[rows] = jnp.zeros((far_count * plane_rows, 128), jnp.bfloat16)
+
     chosen_rows[...] = jnp.zeros_like(chosen_rows)
     row_place = lax.broadcasted_iota(jnp.int32, (heads * block_len, 1), 0) % block_len
 
@@ -217,17 +230,11 @@
         for number in range(named):
             source = chosen[block, number]
             start = pl.multiple_of(counted * packed, packed)
-
-            @pl.when(source < device)
-            def _():
-                for part in range(2):
-                    chosen_rows[part, pl.ds(start, packed)] = arrived[
-                        source % y_count,
-                        slot_of(source // y_count),
-                        part * packed : (part + 1) * packed,
-                        :,
-                    ]
-
+            y, slot = source & (y_count - 1), slot_of(source >> y_bits)
+            for part in range(2):
+                chosen_rows[part, pl.ds(start, packed)] = arrived[
+                    y, slot, part * packed : (part + 1) * packed, :
+                ]
             counted = counted + jnp.where(source < device, 1, 0)
         queries = [ready[pairs + pair, rows, :] for pair in range(pairs)]
 
@@ -301,7 +308,8 @@
     within = np.arange(tok_rows)[:, None] * exact[None, :]
     start = first_place.astype(jnp.float32) * exact.astype(np.float32)
     return (
-        jnp.stack([jnp.cos(start), jnp.sin(start)]),
+        jnp.cos(start)[None],
+        jnp.sin(start)[None],
         jnp.asarray(np.stack([np.cos(within), np.sin(within)]).astype(np.float32)),
     )
 
@@ -328,15 +336,15 @@
     far_count, near_count, y_count = (lax.axis_size(axis) for axis in KV)
     z_count = far_count * near_count
     sent_rows = SEL + tok_rows // CMP
-    turn_start, within = turns(device * tok_rows, tok_rows, head_size)
+    start_cosines, start_sines, within = turns(device * tok_rows, tok_rows, head_size)
     bf16, f32 = jnp.bfloat16, jnp.float32
     shape = jax.ShapeDtypeStruct
     vmem, smem = pltpu.VMEM, pltpu.SMEM
 
     sent, own = kernel_call(
         key_kernel,
-        [smem] + [vmem] * 6,
-        (shared_block, tokens, key_weight.T, value_weight.T, key_gain[None], turn_start, within),
+        [smem] + [vmem] * 7,
+        (shared_block, tokens, key_weight.T, value_weight.T, key_gain[None], start_cosines, start_sines, within),
         (shape((sent_rows, 128), bf16), shape((2, local_blocks, packed, 128), bf16)),
         (),
         10**9,
@@ -346,20 +354,21 @@
     column = lax.all_gather(far, "z_near", axis=0, tiled=True)
     arrived = spread(column, "y").reshape(y_count, z_count, sent_rows, 128)
 
-    tokens_later, own, turn_start, swap_weight, _ = lax.optimization_barrier(
-        (tokens, own, turn_start, out_weight, column)
+    tokens_later, own, start_cosines, start_sines, swap_weight, _ = lax.optimization_barrier(
+        (tokens, own, start_cosines, start_sines, out_weight, column)
     )
     other_weight = lax.ppermute(swap_weight, "core", [(0, 1), (1, 0)])
     ready = kernel_call(
         query_kernel,
-        [smem] + [vmem] * 6,
+        [smem] + [vmem] * 7,
         (
             lax.axis_index(TP).reshape(1),
             tokens_later,
             query_weight,
             gate_weight.T,
             jnp.concatenate([query_gain, query_gain])[None],
-            turn_start,
+            start_cosines,
+            start_sines,
             within,
         ),
         shape((2 * (width // 128) + 1, tok_rows, 128), f32),
@@ -367,6 +376,7 @@
         10**9,
         QUERY_ROOM,
     )
+    ready, other_weight = lax.optimization_barrier((ready, other_weight))
     kept, given, log_weight = kernel_call(
         functools.partial(attention_kernel, far_count),
         [smem, smem, vmem, vmem, vmem],

time: 130 us -> 130 us (level)
  transfers between devices with their start and end apart: 4 -> 4, of which waited for: 2 -> 2; matrix products, arithmetic and copies ran while one was open for 2% -> 2% of each run, Pallas kernels for 8% -> 3%
where the time goes in v7:
time: 130 us
  blocking collectives  60.7 us (47%)
  starting transfers between devices  32 us (25%)
  Pallas kernels  12.7 us (10%)
  waiting for transfers between devices  12.7 us (10%)
  matrix products  3.87 us (3%)
  local copies, waits for them, and re-layouts  3.52 us (3%)
  other arithmetic  2.69 us (2%)
  between operations  1.34 us (1%)
    all_gather x1, blocking collectives, shards(): far = lax.all_gather(sent, 'z_far', axis=0, tiled=True)  47.6 us
    all_gather x1, blocking collectives, shards(): column = lax.all_gather(far, 'z_near', axis=0, tiled=True)  13.1 us
    pallas_call x3, Pallas kernels, kernel_call(): pl.pallas_call(kernel, out_shape=outputs, in_specs=[pl.BlockSpec(memory_s...  12.7 us
    ppermute x1, starting transfers between devices, shards(): taken = lax.ppermute(given, 'core', [(0, 1), (1, 0)])  12.3 us
    ppermute x1, starting transfers between devices, shards(): other_weight = lax.ppermute(swap_weight, 'core', [(0, 1), (1, 0)])  11.2 us
    all_to_all x1, waiting for transfers between devices, shards(): lax.all_to_all(pair_sum, 'x', split_axis=0, concat_axis=0, tiled=True)  8.57 us
    all_to_all x1, starting transfers between devices, spread(): return lax.all_to_all(copies, axis, split_axis=0, concat_axis=0, tiled=True)  4.51 us
    all_to_all x1, waiting for transfers between devices, spread(): return lax.all_to_all(copies, axis, split_axis=0, concat_axis=0, tiled=True)  4.17 us
  transfers between devices with their start and end apart: 4, of which 2 were waited for; matrix products, arithmetic and copies ran while one was open for 2% of the time, Pallas kernels for 3%

profile of v7, /device:TPU:1, one launch (start us, length us, event | category | flops | bytes accessed | tf_op | source)
XLA Modules:
  0.0 129.5 jit_solution(8144307876608993584)
XLA Ops:
  1.3 1.3 fusion.5
  2.6 3.0 %shard_map.131 = (bf16[72,128]{1,0:T(8,128)(2,1)}, bf16[2,4,32,128]{3,2,1,0:T(8,128)(2,1)}) custom-call(s32[1]{0:T(128)S(6)} %copy.15.pick, bf16[256,2048]{1,0:T(8,128)(2,1)} %tokens.2, bf16[64,2048]{1,0:T(8,128)(2,1)} %bitcast.24, bf16[64,2048]{1,0:T(8,128)(2,1)} %bitcast.25, f32[1,64]{1,0:T(1,128)} %bitcast.27, f32[1,32]{1,0:T(1,128)} %get-tuple-element.17.start_cosines, ...), custom_call_target="tpu_custom_call" | custom-call | flops 1000000000 | bytes 4194304 | tf_op jit(solution)/shard_map/pallas_call | solution.py:294
  5.6 47.6 %all_gather.6 = bf16[576,128]{1,0:T(8,128)(2,1)S(1)} all-gather(bf16[72,128]{1,0:T(8,128)(2,1)} %get-tuple-element.14), channel_id=1, replica_groups=mesh['z_far'=8,'z_near'=4,'y'=4,'x'=4,'core'=2] {'z_far'}, dimensions={0}, use_global_device_ids=true | all-gather | bytes 165888 | tf_op jit(solution)/shard_map/all_gather | solution.py:353
  53.2 13.1 %all_gather.7 = bf16[2304,128]{1,0:T(8,128)(2,1)S(1)} all-gather(bf16[576,128]{1,0:T(8,128)(2,1)S(1)} %all_gather.6), channel_id=1, replica_groups=mesh['z_far'=8,'z_near'=4,'y'=4,'x'=4,'core'=2] {'z_near'}, dimensions={0}, use_global_device_ids=true | all-gather | bytes 737280 | tf_op jit(solution)/shard_map/all_gather | solution.py:354
  66.3 1.7 %broadcast_in_dim.21 = bf16[4,2304,128]{2,1,0:T(8,128)(2,1)} broadcast(bf16[2304,128]{1,0:T(8,128)(2,1)S(1)} %all_gather.7), dimensions={1,2} | broadcast | bytes 2949120 | tf_op jit(solution)/shard_map/broadcast_in_dim | solution.py:28
  68.0 0.0 copy-start.3
  68.0 4.5 %all-to-all-start = ((bf16[4,2304,128]{2,1,0:T(8,128)(2,1)}), bf16[4,2304,128]{2,1,0:T(8,128)(2,1)S(1)}, u32[]{:S(2)}, u32[]{:S(2)}) async-start(bf16[4,2304,128]{2,1,0:T(8,128)(2,1)} %broadcast_in_dim.21), calls=%async_computation | async-start | bytes 4718592 | tf_op jit(solution)/shard_map/all_to_all | solution.py:29
  72.6 0.0 copy-start
  72.6 0.0 copy-start.2
  72.6 11.2 %collective-permute-start = (bf16[256,2048]{1,0:T(8,128)(2,1)}, bf16[256,2048]{1,0:T(8,128)(2,1)}, u32[]{:S(2)}, u32[]{:S(2)}) collective-permute-start(bf16[256,2048]{1,0:T(8,128)(2,1)} %param.19), channel_id=1, source_target_pairs={{0,1},{1,0},{2,3},{3,2},{4,5},{5,4},{6,7},{7,6},{8,9},{9,8},{10,11... | collective-permute-start | bytes 3145736 | tf_op jit(solution)/shard_map/ppermute | solution.py:360
  83.8 0.0 copy-done.3
  83.8 0.6 maximum_bitcast_fusion.gain
  84.4 3.7 %shard_map.132.ready = f32[5,256,128]{2,1,0:T(8,128)} custom-call(s32[1]{0:T(128)} %bitcast.8.group, bf16[256,2048]{1,0:T(8,128)(2,1)} %tokens.2, bf16[2048,256]{1,0:T(8,128)(2,1)} %query_weight.1, bf16[64,2048]{1,0:T(8,128)(2,1)} %bitcast.26, f32[1,128]{1,0:T(1,128)} %maximum_bitcast_fusion.gain, f32[1,32]{1,0:T(1,128)} %get-tuple-element.17.start_cosines, ...), custom_call_target="tpu_custom_call" | custom-call | flops 1000000000 | bytes 4194304 | tf_op jit(solution)/shard_map/pallas_call | solution.py:294
  88.1 0.1 pad_add_fusion.place_of
  88.1 0.0 collective-permute-done
  88.1 4.2 %all-to-all-done = bf16[4,2304,128]{2,1,0:T(8,128)(2,1)S(1)} async-done(((bf16[4,2304,128]{2,1,0:T(8,128)(2,1)}), bf16[4,2304,128]{2,1,0:T(8,128)(2,1)S(1)}, u32[]{:S(2)}, u32[]{:S(2)}) %all-to-all-start) | async-done | bytes 2359328 | tf_op jit(solution)/shard_map/all_to_all | solution.py:29
  92.3 0.0 copy-done
  92.3 0.0 copy-done.2
  92.3 0.0 copy-start.1
  92.3 1.1 copy-done.1
  93.4 6.0 %shard_map.133 = (bf16[4,32,256]{2,1,0:T(8,128)(2,1)S(1)}, bf16[4,32,256]{2,1,0:T(8,128)(2,1)S(1)}, f32[2,256,4]{2,1,0:T(8,128)S(1)}) custom-call(s32[2]{0:T(128)S(1)} %pad_add_fusion.place_of, s32[4,15]{1,0:T(4,128)S(1)} %copy-done, bf16[4,32,72,128]{3,2,1,0:T(8,128)(2,1)S(1)} %bitcast.21, f32[5,256,128]{2,1,0:T(8,128)S(1)} %copy-done.1, ...), custom_call_target="tpu_custom_call" | custom-call | flops 4000000000 | bytes 4194304 | tf_op jit(solution)/shard_map/pallas_call | solution.py:294
  99.4 12.3 %collective-permute-start.1 = (bf16[4,32,256]{2,1,0:T(8,128)(2,1)S(1)}, bf16[4,32,256]{2,1,0:T(8,128)(2,1)S(1)}, u32[]{:S(2)}, u32[]{:S(2)}) collective-permute-start(bf16[4,32,256]{2,1,0:T(8,128)(2,1)S(1)} %get-tuple-element.23), channel_id=1, source_target_pairs={{0,1},{1,0},{2,3},{3,2},{4,5},{5,4},{6,7},{7,6},{8,9},{9,8},{10,11... | collective-permute-start | bytes 196616 | tf_op jit(solution)/shard_map/ppermute | solution.py:404
  111.7 1.5 %fusion.3 = f32[128,2048]{1,0:T(8,128)S(1)} fusion(bf16[128,256]{1,0:T(8,128)(2,1)S(1)} %bitcast.22, bf16[256,2048]{1,0:T(8,128)(2,1)} %param.19), kind=kOutput, calls=%fused_computation.5 | convolution fusion | flops 134742016 | bytes 2162688 | tf_op jit(solution)/shard_map/dot_general | solution.py:405
  113.2 0.0 collective-permute-done.1
  113.2 2.3 %fusion.2 = bf16[128,2048]{1,0:T(8,128)(2,1)} fusion(f32[128,2048]{1,0:T(8,128)S(1)} %fusion.3, bf16[128,256]{1,0:T(8,128)(2,1)S(1)} %bitcast.23, bf16[256,2048]{1,0:T(8,128)(2,1)} %collective-permute-done), kind=kOutput, calls=%fused_computation.3 | convolution fusion | flops 135266304 | bytes 2686976 | tf_op jit(solution)/shard_map/dot_general | solution.py:408
  115.5 4.0 %all-to-all-start.1 = ((bf16[4,32,2048]{2,1,0:T(8,128)(2,1)}), bf16[4,32,2048]{2,1,0:T(8,128)(2,1)S(1)}, u32[]{:S(2)}, u32[]{:S(2)}) async-start(bf16[4,32,2048]{2,1,0:T(8,128)(2,1)} %bitcast.13), calls=%async_computation.1 | async-start | bytes 1048576 | tf_op jit(solution)/shard_map/all_to_all | solution.py:413
  119.5 0.7 copy.14
  120.2 8.6 %all-to-all-done.1 = bf16[4,32,2048]{2,1,0:T(8,128)(2,1)S(1)} async-done(((bf16[4,32,2048]{2,1,0:T(8,128)(2,1)}), bf16[4,32,2048]{2,1,0:T(8,128)(2,1)S(1)}, u32[]{:S(2)}, u32[]{:S(2)}) %all-to-all-start.1) | async-done | bytes 524320 | tf_op jit(solution)/shard_map/all_to_all | solution.py:413
  128.8 0.7 reduce_sum.12
Async XLA Ops:
  68.0 15.8 %copy-start.3 = (f32[64]{0:T(128)S(1)}, f32[64]{0:T(128)}, u32[]{:S(2)}) copy-start(f32[64]{0:T(128)} %param.17) | copy-start | bytes 772
  68.0 24.3 %all-to-all-start = ((bf16[4,2304,128]{2,1,0:T(8,128)(2,1)}), bf16[4,2304,128]{2,1,0:T(8,128)(2,1)S(1)}, u32[]{:S(2)}, u32[]{:S(2)}) async-start(bf16[4,2304,128]{2,1,0:T(8,128)(2,1)} %broadcast_in_dim.21), calls=%async_computation | async-start | bytes 4718592 | tf_op jit(solution)/shard_map/all_to_all | solution.py:29
  72.6 19.7 %copy-start = (s32[4,15]{1,0:T(4,128)S(1)}, s32[4,15]{1,0:T(4,128)}, u32[]{:S(2)}) copy-start(s32[4,15]{1,0:T(4,128)} %chosen.1) | copy-start | bytes 724
  72.6 19.7 %copy-start.2 = (bf16[2,4,32,128]{3,2,1,0:T(8,128)(2,1)S(1)}, bf16[2,4,32,128]{3,2,1,0:T(8,128)(2,1)}, u32[]{:S(2)}) copy-start(bf16[2,4,32,128]{3,2,1,0:T(8,128)(2,1)} %get-tuple-element.21.own) | copy-start | bytes 196612
  72.6 15.6 %collective-permute-start = (bf16[256,2048]{1,0:T(8,128)(2,1)}, bf16[256,2048]{1,0:T(8,128)(2,1)}, u32[]{:S(2)}, u32[]{:S(2)}) collective-permute-start(bf16[256,2048]{1,0:T(8,128)(2,1)} %param.19), channel_id=1, source_target_pairs={{0,1},{1,0},{2,3},{3,2},{4,5},{5,4},{6,7},{7,6},{8,9},{9,8},{10,11... | collective-permute-start | bytes 3145736 | tf_op jit(solution)/shard_map/ppermute | solution.py:360
  92.3 1.1 copy-start.1
  99.4 13.8 %collective-permute-start.1 = (bf16[4,32,256]{2,1,0:T(8,128)(2,1)S(1)}, bf16[4,32,256]{2,1,0:T(8,128)(2,1)S(1)}, u32[]{:S(2)}, u32[]{:S(2)}) collective-permute-start(bf16[4,32,256]{2,1,0:T(8,128)(2,1)S(1)} %get-tuple-element.23), channel_id=1, source_target_pairs={{0,1},{1,0},{2,3},{3,2},{4,5},{5,4},{6,7},{7,6},{8,9},{9,8},{10,11... | collective-permute-start | bytes 196616 | tf_op jit(solution)/shard_map/ppermute | solution.py:404
  115.5 13.3 %all-to-all-start.1 = ((bf16[4,32,2048]{2,1,0:T(8,128)(2,1)}), bf16[4,32,2048]{2,1,0:T(8,128)(2,1)S(1)}, u32[]{:S(2)}, u32[]{:S(2)}) async-start(bf16[4,32,2048]{2,1,0:T(8,128)(2,1)} %bitcast.13), calls=%async_computation.1 | async-start | bytes 1048576 | tf_op jit(solution)/shard_map/all_to_all | solution.py:413

commit v8 on v7

--- a/solution.py
+++ b/solution.py
@@ -136,7 +136,6 @@
     chosen_rows,
     spans,
     span_part,
-    span_log,
 ):
     device, core = place_of[0], place_of[1]
     blocks, named = chosen.shape
@@ -150,7 +149,7 @@
     near_count = z_count // far_count
     score_scale = 64 ** (-0.5)
     all_spans = spans.shape[0]
-    all_rows = chosen_rows.shape[1]
+    all_rows = chosen_rows.shape[2]
 
     near_bits, y_bits = near_count.bit_length() - 1, y_count.bit_length() - 1
 
@@ -178,116 +177,109 @@
             spans[rows] = jnp.zeros((far_count * plane_rows, 128), jnp.bfloat16)
 
     chosen_rows[...] = jnp.zeros_like(chosen_rows)
+
+    def gate_columns(rows, branch):
+        gate_rows = ready[2 * pairs, rows, :]
+        return jnp.concatenate(
+            [gate_rows[:, 2 * head + branch : 2 * head + branch + 1] for head in range(heads)],
+            axis=0,
+        )
+
+    def span_branch(first_row, length, width):
+        rows = pl.ds(first_row, length)
+        scores = dot_last(
+            one_sided([ready[pair, rows, :] for pair in range(pairs)], False), spans[:width]
+        )
+        row_place = lax.broadcasted_iota(jnp.int32, (heads * length, 1), 0) % length
+        places = device * tok_rows + first_row + row_place
+        has_span = places >= CMP - 1
+        span_ends = lax.broadcasted_iota(jnp.int32, (1, width), 1) * CMP + CMP - 1
+        scores = jnp.where(span_ends <= places, scores * score_scale, big_negative)
+        peak = jnp.max(scores, axis=-1, keepdims=True)
+        raw = jnp.exp(scores - peak)
+        total = jnp.where(has_span, jnp.sum(raw, axis=-1, keepdims=True), 1.0)
+        summed = jnp.dot(
+            raw.astype(jnp.bfloat16), spans[:width], preferred_element_type=jnp.float32
+        )
+        summed = jnp.where(has_span, gate_columns(rows, 0) * (summed[:, 64:] / total), 0.0)
+        span_log = jnp.where(has_span, peak + jnp.log(total), 0.0)
+        for head in range(heads):
+            piece = slice(head * length, (head + 1) * length)
+            span_part[head, rows, :] = summed[piece]
+            logs[0, rows, head : head + 1] = span_log[piece]
+
+    few_spans = all_spans // 4
+    few = (device + 1) * span_rows <= few_spans
+
+    @pl.when(few)
+    def _():
+        for part in range(2):
+            span_branch(part * (tok_rows // 2), tok_rows // 2, few_spans)
+
+    @pl.when(jnp.logical_not(few))
+    def _():
+        @pl.loop(0, blocks)
+        def _(block):
+            span_branch(pl.multiple_of(block * block_len, block_len), block_len, all_spans)
+
     row_place = lax.broadcasted_iota(jnp.int32, (heads * block_len, 1), 0) % block_len
-
-    def in_width(count, widths, branch):
-        least = 0
-        for width, most in widths:
-
-            @pl.when((count >= least) & (count < most))
-            def _():
-                branch(width)
-
-            least = most
-
-    @pl.loop(0, blocks)
-    def _(block):
+    lanes = lax.broadcasted_iota(jnp.int32, (heads * block_len, all_rows), 1)
+
+    def chosen_branch(block, keys, values):
         rows = pl.ds(pl.multiple_of(block * block_len, block_len), block_len)
-        gate_rows = ready[2 * pairs, rows, :]
-        gate_of = [
-            jnp.concatenate(
-                [gate_rows[:, 2 * head + b : 2 * head + b + 1] for head in range(heads)], axis=0
-            )
-            for b in range(2)
-        ]
-
-        def span_branch(width):
-            scores = dot_last(
-                one_sided([ready[pair, rows, :] for pair in range(pairs)], False), spans[:width]
-            )
-            places = device * tok_rows + block * block_len + row_place
-            has_span = places >= CMP - 1
-            span_ends = lax.broadcasted_iota(jnp.int32, (1, width), 1) * CMP + CMP - 1
-            scores = jnp.where(span_ends <= places, scores * score_scale, big_negative)
-            peak = jnp.max(scores, axis=-1, keepdims=True)
-            raw = jnp.exp(scores - peak)
-            total = jnp.where(has_span, jnp.sum(raw, axis=-1, keepdims=True), 1.0)
-            summed = jnp.dot(
-                raw.astype(jnp.bfloat16), spans[:width], preferred_element_type=jnp.float32
-            )
-            span_part[...] = jnp.where(has_span, gate_of[0] * (summed[:, 64:] / total), 0.0)
-            span_log[...] = jnp.where(has_span, peak + jnp.log(total), 0.0)
-
-        in_width(
-            (device + 1) * span_rows - 1,
-            [(width, width) for width in (all_spans // 4, all_spans // 2, all_spans)],
-            span_branch,
-        )
-
-        for part in range(2):
-            chosen_rows[part, :packed] = own[part, block]
+        keys[:packed] = own[0, block]
+        values[:packed] = own[1, block]
         counted = jnp.int32(1)
         for number in range(named):
             source = chosen[block, number]
             start = pl.multiple_of(counted * packed, packed)
             y, slot = source & (y_count - 1), slot_of(source >> y_bits)
-            for part in range(2):
-                chosen_rows[part, pl.ds(start, packed)] = arrived[
-                    y, slot, part * packed : (part + 1) * packed, :
-                ]
+            keys[pl.ds(start, packed)] = arrived[y, slot, :packed, :]
+            values[pl.ds(start, packed)] = arrived[y, slot, packed:block_len, :]
             counted = counted + jnp.where(source < device, 1, 0)
         queries = [ready[pairs + pair, rows, :] for pair in range(pairs)]
-
-        def chosen_branch(width):
-            half_scores = []
-            lanes = lax.broadcasted_iota(jnp.int32, (heads * block_len, width), 1)
-            blocked = jnp.where(lanes[:1] < counted * packed, 0.0, big_negative)
-            for upper in (False, True):
-                scores = dot_last(one_sided(queries, upper), chosen_rows[0, :width])
-                scores = scores * score_scale + blocked
-                later = (lanes < packed) & (lanes + packed * upper > row_place)
-                half_scores.append(jnp.where(later, big_negative, scores))
-            peak = jnp.maximum(
-                jnp.max(half_scores[0], axis=-1, keepdims=True),
-                jnp.max(half_scores[1], axis=-1, keepdims=True),
+        half_scores = []
+        blocked = jnp.where(lanes[:1] < counted * packed, 0.0, big_negative)
+        for upper in (False, True):
+            scores = dot_last(one_sided(queries, upper), keys[...])
+            scores = scores * score_scale + blocked
+            later = (lanes < packed) & (lanes + packed * upper > row_place)
+            half_scores.append(jnp.where(later, big_negative, scores))
+        peak = jnp.maximum(
+            jnp.max(half_scores[0], axis=-1, keepdims=True),
+            jnp.max(half_scores[1], axis=-1, keepdims=True),
+        )
+        total = 0.0
+        products = []
+        for upper in range(2):
+            raw = jnp.exp(half_scores[upper] - peak)
+            total = total + jnp.sum(raw, axis=-1, keepdims=True)
+            products.append(
+                jnp.dot(raw.astype(jnp.bfloat16), values[...], preferred_element_type=jnp.float32)
             )
-            total = 0.0
-            products = []
-            for upper in range(2):
-                raw = jnp.exp(half_scores[upper] - peak)
-                total = total + jnp.sum(raw, axis=-1, keepdims=True)
-                products.append(
-                    jnp.dot(
-                        raw.astype(jnp.bfloat16),
-                        chosen_rows[1, :width],
-                        preferred_element_type=jnp.float32,
-                    )
-                )
-            summed = products[0][:, :64] + products[1][:, 64:]
-            mixed = span_part[...] + gate_of[1] * (summed / total)
-            chosen_log = peak + jnp.log(total)
-            for pair in range(pairs):
-                first = mixed[2 * pair * block_len : (2 * pair + 1) * block_len]
-                second = mixed[(2 * pair + 1) * block_len : (2 * pair + 2) * block_len]
-                both = jnp.concatenate([first, second], axis=1)
-                lower, upper = both[:packed], both[packed:]
-                lane_range = slice(pair * 128, (pair + 1) * 128)
-                kept[block, :, lane_range] = jnp.where(core == 0, lower, upper).astype(
-                    jnp.bfloat16
-                )
-                given[block, :, lane_range] = jnp.where(core == 0, upper, lower).astype(
-                    jnp.bfloat16
-                )
-            for head in range(heads):
-                piece = slice(head * block_len, (head + 1) * block_len)
-                logs[0, rows, head : head + 1] = span_log[piece]
-                logs[1, rows, head : head + 1] = chosen_log[piece]
-
-        in_width(
-            counted - 1,
-            [(width, width // packed) for width in (all_rows // 4, all_rows // 2, all_rows)],
-            chosen_branch,
-        )
+        summed = products[0][:, :64] + products[1][:, 64:]
+        scaled = gate_columns(rows, 1) * (summed / total)
+        chosen_log = peak + jnp.log(total)
+        pieces = []
+        for head in range(heads):
+            piece = slice(head * block_len, (head + 1) * block_len)
+            logs[1, rows, head : head + 1] = chosen_log[piece]
+            pieces.append(span_part[head, rows, :] + scaled[piece])
+        for pair in range(pairs):
+            both = jnp.concatenate([pieces[2 * pair], pieces[2 * pair + 1]], axis=1)
+            lower, upper = both[:packed], both[packed:]
+            lane_range = slice(pair * 128, (pair + 1) * 128)
+            kept[block, :, lane_range] = jnp.where(core == 0, lower, upper).astype(jnp.bfloat16)
+            given[block, :, lane_range] = jnp.where(core == 0, upper, lower).astype(jnp.bfloat16)
+
+    side = chosen_rows.shape[0]
+
+    @pl.loop(0, blocks // side)
+    def _(step):
+        for number in range(side):
+            chosen_branch(
+                step * side + number, chosen_rows.at[number, 0], chosen_rows.at[number, 1]
+            )
 
 
 def kernel_call(kernel, specs, operands, outputs, scratch, flops, room):
@@ -393,10 +385,9 @@
             shape((2, tok_rows, head_count), f32),
         ),
         (
-            pltpu.VMEM((2, (chosen_device.shape[1] + 1) * packed, 128), bf16),
+            pltpu.VMEM((2, 2, (chosen_device.shape[1] + 1) * packed, 128), bf16),
             pltpu.VMEM((y_count * z_count * (sent_rows - SEL), 128), bf16),
-            pltpu.VMEM((head_count * SEL, head_size), f32),
-            pltpu.VMEM((head_count * SEL, 1), f32),
+            pltpu.VMEM((head_count, tok_rows, head_size), f32),
         ),
         4 * 10**9,
         ATTENTION_ROOM,

time: 130 us -> 130 us (level)
  no operation moved by 1% of the time
where the time goes in v8:
time: 130 us; the launch traced here: 129 us
  blocking collectives  60.7 us (47%)
  starting transfers between devices  32 us (25%)
  waiting for transfers between devices  12.7 us (10%)
  Pallas kernels  12.1 us (9%)
  matrix products  3.87 us (3%)
  local copies, waits for them, and re-layouts  3.52 us (3%)
  other arithmetic  2.69 us (2%)
  between operations  1.35 us (1%)
    all_gather x1, blocking collectives, shards(): far = lax.all_gather(sent, 'z_far', axis=0, tiled=True)  47.6 us
    all_gather x1, blocking collectives, shards(): column = lax.all_gather(far, 'z_near', axis=0, tiled=True)  13.1 us
    ppermute x1, starting transfers between devices, shards(): taken = lax.ppermute(given, 'core', [(0, 1), (1, 0)])  12.3 us
    pallas_call x3, Pallas kernels, kernel_call(): pl.pallas_call(kernel, out_shape=outputs, in_specs=[pl.BlockSpec(memory_s...  12.1 us
    ppermute x1, starting transfers between devices, shards(): other_weight = lax.ppermute(swap_weight, 'core', [(0, 1), (1, 0)])  11.2 us
    all_to_all x1, waiting for transfers between devices, shards(): lax.all_to_all(pair_sum, 'x', split_axis=0, concat_axis=0, tiled=True)  8.57 us
    all_to_all x1, starting transfers between devices, spread(): return lax.all_to_all(copies, axis, split_axis=0, concat_axis=0, tiled=True)  4.51 us
    all_to_all x1, waiting for transfers between devices, spread(): return lax.all_to_all(copies, axis, split_axis=0, concat_axis=0, tiled=True)  4.17 us
  transfers between devices with their start and end apart: 4, of which 2 were waited for; matrix products, arithmetic and copies ran while one was open for 2% of the time, Pallas kernels for 3%

profile of v8, /device:TPU:1, one launch (start us, length us, event | category | flops | bytes accessed | tf_op | source)
XLA Modules:
  0.0 129.0 jit_solution(1096237638278849135)
XLA Ops:
  1.3 1.3 fusion.5
  2.6 3.0 %shard_map.131 = (bf16[72,128]{1,0:T(8,128)(2,1)}, bf16[2,4,32,128]{3,2,1,0:T(8,128)(2,1)}) custom-call(s32[1]{0:T(128)S(6)} %copy.15.pick, bf16[256,2048]{1,0:T(8,128)(2,1)} %tokens.2, bf16[64,2048]{1,0:T(8,128)(2,1)} %bitcast.24, bf16[64,2048]{1,0:T(8,128)(2,1)} %bitcast.25, f32[1,64]{1,0:T(1,128)} %bitcast.27, f32[1,32]{1,0:T(1,128)} %get-tuple-element.17.start_cosines, ...), custom_call_target="tpu_custom_call" | custom-call | flops 1000000000 | bytes 4194304 | tf_op jit(solution)/shard_map/pallas_call | solution.py:286
  5.6 47.6 %all_gather.6 = bf16[576,128]{1,0:T(8,128)(2,1)S(1)} all-gather(bf16[72,128]{1,0:T(8,128)(2,1)} %get-tuple-element.14), channel_id=1, replica_groups=mesh['z_far'=8,'z_near'=4,'y'=4,'x'=4,'core'=2] {'z_far'}, dimensions={0}, use_global_device_ids=true | all-gather | bytes 165888 | tf_op jit(solution)/shard_map/all_gather | solution.py:345
  53.2 13.1 %all_gather.7 = bf16[2304,128]{1,0:T(8,128)(2,1)S(1)} all-gather(bf16[576,128]{1,0:T(8,128)(2,1)S(1)} %all_gather.6), channel_id=1, replica_groups=mesh['z_far'=8,'z_near'=4,'y'=4,'x'=4,'core'=2] {'z_near'}, dimensions={0}, use_global_device_ids=true | all-gather | bytes 737280 | tf_op jit(solution)/shard_map/all_gather | solution.py:346
  66.3 1.7 %broadcast_in_dim.21 = bf16[4,2304,128]{2,1,0:T(8,128)(2,1)} broadcast(bf16[2304,128]{1,0:T(8,128)(2,1)S(1)} %all_gather.7), dimensions={1,2} | broadcast | bytes 2949120 | tf_op jit(solution)/shard_map/broadcast_in_dim | solution.py:28
  68.0 0.0 copy-start.3
  68.0 4.5 %all-to-all-start = ((bf16[4,2304,128]{2,1,0:T(8,128)(2,1)}), bf16[4,2304,128]{2,1,0:T(8,128)(2,1)S(1)}, u32[]{:S(2)}, u32[]{:S(2)}) async-start(bf16[4,2304,128]{2,1,0:T(8,128)(2,1)} %broadcast_in_dim.21), calls=%async_computation | async-start | bytes 4718592 | tf_op jit(solution)/shard_map/all_to_all | solution.py:29
  72.6 0.0 copy-start
  72.6 0.0 copy-start.2
  72.6 11.2 %collective-permute-start = (bf16[256,2048]{1,0:T(8,128)(2,1)}, bf16[256,2048]{1,0:T(8,128)(2,1)}, u32[]{:S(2)}, u32[]{:S(2)}) collective-permute-start(bf16[256,2048]{1,0:T(8,128)(2,1)} %param.19), channel_id=1, source_target_pairs={{0,1},{1,0},{2,3},{3,2},{4,5},{5,4},{6,7},{7,6},{8,9},{9,8},{10,11... | collective-permute-start | bytes 3145736 | tf_op jit(solution)/shard_map/ppermute | solution.py:352
  83.8 0.0 copy-done.3
  83.8 0.6 maximum_bitcast_fusion.gain
  84.4 3.7 %shard_map.132.ready = f32[5,256,128]{2,1,0:T(8,128)} custom-call(s32[1]{0:T(128)} %bitcast.8.group, bf16[256,2048]{1,0:T(8,128)(2,1)} %tokens.2, bf16[2048,256]{1,0:T(8,128)(2,1)} %query_weight.1, bf16[64,2048]{1,0:T(8,128)(2,1)} %bitcast.26, f32[1,128]{1,0:T(1,128)} %maximum_bitcast_fusion.gain, f32[1,32]{1,0:T(1,128)} %get-tuple-element.17.start_cosines, ...), custom_call_target="tpu_custom_call" | custom-call | flops 1000000000 | bytes 4194304 | tf_op jit(solution)/shard_map/pallas_call | solution.py:286
  88.1 0.1 pad_add_fusion.place_of
  88.1 0.0 collective-permute-done
  88.1 4.2 %all-to-all-done = bf16[4,2304,128]{2,1,0:T(8,128)(2,1)S(1)} async-done(((bf16[4,2304,128]{2,1,0:T(8,128)(2,1)}), bf16[4,2304,128]{2,1,0:T(8,128)(2,1)S(1)}, u32[]{:S(2)}, u32[]{:S(2)}) %all-to-all-start) | async-done | bytes 2359328 | tf_op jit(solution)/shard_map/all_to_all | solution.py:29
  92.3 0.0 copy-done
  92.3 0.0 copy-done.2
  92.3 0.0 copy-start.1
  92.3 1.1 copy-done.1
  93.4 5.5 %shard_map.133 = (bf16[4,32,256]{2,1,0:T(8,128)(2,1)S(1)}, bf16[4,32,256]{2,1,0:T(8,128)(2,1)S(1)}, f32[2,256,4]{2,1,0:T(8,128)S(1)}) custom-call(s32[2]{0:T(128)S(1)} %pad_add_fusion.place_of, s32[4,15]{1,0:T(4,128)S(1)} %copy-done, bf16[4,32,72,128]{3,2,1,0:T(8,128)(2,1)S(1)} %bitcast.21, f32[5,256,128]{2,1,0:T(8,128)S(1)} %copy-done.1, ...), custom_call_target="tpu_custom_call" | custom-call | flops 4000000000 | bytes 4194304 | tf_op jit(solution)/shard_map/pallas_call | solution.py:286
  98.9 12.3 %collective-permute-start.1 = (bf16[4,32,256]{2,1,0:T(8,128)(2,1)S(1)}, bf16[4,32,256]{2,1,0:T(8,128)(2,1)S(1)}, u32[]{:S(2)}, u32[]{:S(2)}) collective-permute-start(bf16[4,32,256]{2,1,0:T(8,128)(2,1)S(1)} %get-tuple-element.23), channel_id=1, source_target_pairs={{0,1},{1,0},{2,3},{3,2},{4,5},{5,4},{6,7},{7,6},{8,9},{9,8},{10,11... | collective-permute-start | bytes 196616 | tf_op jit(solution)/shard_map/ppermute | solution.py:395
  111.1 1.5 %fusion.3 = f32[128,2048]{1,0:T(8,128)S(1)} fusion(bf16[128,256]{1,0:T(8,128)(2,1)S(1)} %bitcast.22, bf16[256,2048]{1,0:T(8,128)(2,1)} %param.19), kind=kOutput, calls=%fused_computation.5 | convolution fusion | flops 134742016 | bytes 2162688 | tf_op jit(solution)/shard_map/dot_general | solution.py:396
  112.7 0.0 collective-permute-done.1
  112.7 2.3 %fusion.2 = bf16[128,2048]{1,0:T(8,128)(2,1)} fusion(f32[128,2048]{1,0:T(8,128)S(1)} %fusion.3, bf16[128,256]{1,0:T(8,128)(2,1)S(1)} %bitcast.23, bf16[256,2048]{1,0:T(8,128)(2,1)} %collective-permute-done), kind=kOutput, calls=%fused_computation.3 | convolution fusion | flops 135266304 | bytes 2686976 | tf_op jit(solution)/shard_map/dot_general | solution.py:399
  115.0 4.0 %all-to-all-start.1 = ((bf16[4,32,2048]{2,1,0:T(8,128)(2,1)}), bf16[4,32,2048]{2,1,0:T(8,128)(2,1)S(1)}, u32[]{:S(2)}, u32[]{:S(2)}) async-start(bf16[4,32,2048]{2,1,0:T(8,128)(2,1)} %bitcast.13), calls=%async_computation.1 | async-start | bytes 1048576 | tf_op jit(solution)/shard_map/all_to_all | solution.py:404
  119.0 0.7 copy.14
  119.7 8.6 %all-to-all-done.1 = bf16[4,32,2048]{2,1,0:T(8,128)(2,1)S(1)} async-done(((bf16[4,32,2048]{2,1,0:T(8,128)(2,1)}), bf16[4,32,2048]{2,1,0:T(8,128)(2,1)S(1)}, u32[]{:S(2)}, u32[]{:S(2)}) %all-to-all-start.1) | async-done | bytes 524320 | tf_op jit(solution)/shard_map/all_to_all | solution.py:404
  128.3 0.7 reduce_sum.12
Async XLA Ops:
  68.0 15.8 %copy-start.3 = (f32[64]{0:T(128)S(1)}, f32[64]{0:T(128)}, u32[]{:S(2)}) copy-start(f32[64]{0:T(128)} %param.17) | copy-start | bytes 772
  68.0 24.3 %all-to-all-start = ((bf16[4,2304,128]{2,1,0:T(8,128)(2,1)}), bf16[4,2304,128]{2,1,0:T(8,128)(2,1)S(1)}, u32[]{:S(2)}, u32[]{:S(2)}) async-start(bf16[4,2304,128]{2,1,0:T(8,128)(2,1)} %broadcast_in_dim.21), calls=%async_computation | async-start | bytes 4718592 | tf_op jit(solution)/shard_map/all_to_all | solution.py:29
  72.6 19.7 %copy-start = (s32[4,15]{1,0:T(4,128)S(1)}, s32[4,15]{1,0:T(4,128)}, u32[]{:S(2)}) copy-start(s32[4,15]{1,0:T(4,128)} %chosen.1) | copy-start | bytes 724
  72.6 19.7 %copy-start.2 = (bf16[2,4,32,128]{3,2,1,0:T(8,128)(2,1)S(1)}, bf16[2,4,32,128]{3,2,1,0:T(8,128)(2,1)}, u32[]{:S(2)}) copy-start(bf16[2,4,32,128]{3,2,1,0:T(8,128)(2,1)} %get-tuple-element.21.own) | copy-start | bytes 196612
  72.6 15.6 %collective-permute-start = (bf16[256,2048]{1,0:T(8,128)(2,1)}, bf16[256,2048]{1,0:T(8,128)(2,1)}, u32[]{:S(2)}, u32[]{:S(2)}) collective-permute-start(bf16[256,2048]{1,0:T(8,128)(2,1)} %param.19), channel_id=1, source_target_pairs={{0,1},{1,0},{2,3},{3,2},{4,5},{5,4},{6,7},{7,6},{8,9},{9,8},{10,11... | collective-permute-start | bytes 3145736 | tf_op jit(solution)/shard_map/ppermute | solution.py:352
  92.3 1.1 copy-start.1
  98.9 13.8 %collective-permute-start.1 = (bf16[4,32,256]{2,1,0:T(8,128)(2,1)S(1)}, bf16[4,32,256]{2,1,0:T(8,128)(2,1)S(1)}, u32[]{:S(2)}, u32[]{:S(2)}) collective-permute-start(bf16[4,32,256]{2,1,0:T(8,128)(2,1)S(1)} %get-tuple-element.23), channel_id=1, source_target_pairs={{0,1},{1,0},{2,3},{3,2},{4,5},{5,4},{6,7},{7,6},{8,9},{9,8},{10,11... | collective-permute-start | bytes 196616 | tf_op jit(solution)/shard_map/ppermute | solution.py:395
  115.0 13.2 %all-to-all-start.1 = ((bf16[4,32,2048]{2,1,0:T(8,128)(2,1)}), bf16[4,32,2048]{2,1,0:T(8,128)(2,1)S(1)}, u32[]{:S(2)}, u32[]{:S(2)}) async-start(bf16[4,32,2048]{2,1,0:T(8,128)(2,1)} %bitcast.13), calls=%async_computation.1 | async-start | bytes 1048576 | tf_op jit(solution)/shard_map/all_to_all | solution.py:404

commit v9 on v8

--- a/solution.py
+++ b/solution.py
@@ -49,13 +49,15 @@
     )
 
 
-def turns_of(start_cosines, start_sines, within):
+def turns_of(device, starts, within):
+    start_cosines = starts[0, pl.ds(device, 1), :]
+    start_sines = starts[1, pl.ds(device, 1), :]
     cosines = start_cosines * within[0] - start_sines * within[1]
     sines = start_sines * within[0] + start_cosines * within[1]
     return cosines, sines
 
 
-def key_kernel(pick, tokens, key_weight, value_weight, gain, start_cosines, start_sines, within, sent, own):
+def key_kernel(device, pick, tokens, key_weight, value_weight, gain, starts, within, sent, own):
     _, blocks, packed, _ = own.shape
     tok_rows = tokens.shape[0]
     block_len = 2 * packed
@@ -65,7 +67,7 @@
     square = jnp.mean(keys * keys, axis=-1, keepdims=True)
     plain = (keys * lax.rsqrt(square + norm_eps) * gain[...]).astype(jnp.bfloat16)
     plain = plain.astype(jnp.float32)
-    cosines, sines = turns_of(start_cosines[...], start_sines[...], within[...])
+    cosines, sines = turns_of(device[0], starts, within)
     turned = plain * repeated(cosines, (1, 1)) + swapped(plain) * repeated(sines, (-1, 1))
     turned = turned.astype(jnp.bfloat16)
     for block in range(blocks):
@@ -79,7 +81,7 @@
     sent[block_len:] = spans.astype(jnp.bfloat16)
 
 
-def query_kernel(group, tokens, query_weight, gate_weight, gain, start_cosines, start_sines, within, ready):
+def query_kernel(device, group, tokens, query_weight, gate_weight, gain, starts, within, ready):
     tok_rows = tokens.shape[0]
     width = query_weight.shape[1]
     gate_count = 2 * (width // 64)
@@ -88,7 +90,7 @@
         dot_last(tokens[...], gate_weight[pl.ds(start, gate_count), :].astype(jnp.bfloat16))
     )
     lanes = lax.broadcasted_iota(jnp.int32, (tok_rows, 128), 1)
-    cosines, sines = turns_of(start_cosines[...], start_sines[...], within[...])
+    cosines, sines = turns_of(device[0], starts, within)
     cos_lanes = repeated(cosines, (1, 1, 1, 1))
     sin_lanes = repeated(sines, (-1, 1, -1, 1))
     for pair in range(width // 128):
@@ -294,16 +296,15 @@
     )(*operands)
 
 
-def turns(first_place, tok_rows, head_size):
+def turns(devices, tok_rows, head_size):
     half_size = head_size // 2
-    exact = rope_base ** (-np.arange(half_size) * 2.0 / head_size)
-    within = np.arange(tok_rows)[:, None] * exact[None, :]
-    start = first_place.astype(jnp.float32) * exact.astype(np.float32)
-    return (
-        jnp.cos(start)[None],
-        jnp.sin(start)[None],
-        jnp.asarray(np.stack([np.cos(within), np.sin(within)]).astype(np.float32)),
-    )
+    inverse = rope_base ** (-np.arange(half_size) * 2.0 / head_size)
+
+    def table(places):
+        angles = places[:, None] * inverse[None, :]
+        return jnp.asarray(np.stack([np.cos(angles), np.sin(angles)]).astype(np.float32))
+
+    return table(np.arange(devices) * tok_rows), table(np.arange(tok_rows))
 
 
 def shards(
@@ -328,15 +329,24 @@
     far_count, near_count, y_count = (lax.axis_size(axis) for axis in KV)
     z_count = far_count * near_count
     sent_rows = SEL + tok_rows // CMP
-    start_cosines, start_sines, within = turns(device * tok_rows, tok_rows, head_size)
+    starts, within = turns(z_count * y_count, tok_rows, head_size)
     bf16, f32 = jnp.bfloat16, jnp.float32
     shape = jax.ShapeDtypeStruct
     vmem, smem = pltpu.VMEM, pltpu.SMEM
 
     sent, own = kernel_call(
         key_kernel,
-        [smem] + [vmem] * 7,
-        (shared_block, tokens, key_weight.T, value_weight.T, key_gain[None], start_cosines, start_sines, within),
+        [smem] * 2 + [vmem] * 6,
+        (
+            device.reshape(1),
+            shared_block,
+            tokens,
+            key_weight.T,
+            value_weight.T,
+            key_gain[None],
+            starts,
+            within,
+        ),
         (shape((sent_rows, 128), bf16), shape((2, local_blocks, packed, 128), bf16)),
         (),
         10**9,
@@ -346,21 +356,21 @@
     column = lax.all_gather(far, "z_near", axis=0, tiled=True)
     arrived = spread(column, "y").reshape(y_count, z_count, sent_rows, 128)
 
-    tokens_later, own, start_cosines, start_sines, swap_weight, _ = lax.optimization_barrier(
-        (tokens, own, start_cosines, start_sines, out_weight, column)
+    tokens_later, own, swap_weight, _ = lax.optimization_barrier(
+        (tokens, own, out_weight, column)
     )
     other_weight = lax.ppermute(swap_weight, "core", [(0, 1), (1, 0)])
     ready = kernel_call(
         query_kernel,
-        [smem] + [vmem] * 7,
+        [smem] * 2 + [vmem] * 6,
         (
+            device.reshape(1),
             lax.axis_index(TP).reshape(1),
             tokens_later,
             query_weight,
             gate_weight.T,
             jnp.concatenate([query_gain, query_gain])[None],
-            start_cosines,
-            start_sines,
+            starts,
             within,
         ),
         shape((2 * (width // 128) + 1, tok_rows, 128), f32),

time: 130 us -> 128 us (0.985)
  other arithmetic: 2.69 us -> 1.39 us
where the time goes in v9:
time: 128 us
  blocking collectives  60.9 us (48%)
  starting transfers between devices  31.6 us (25%)
  waiting for transfers between devices  12.7 us (10%)
  Pallas kernels  12.2 us (10%)
  matrix products  3.87 us (3%)
  local copies, waits for them, and re-layouts  3.53 us (3%)
  other arithmetic  1.39 us (1%)
  between operations  1.35 us (1%)
    all_gather x1, blocking collectives, shards(): far = lax.all_gather(sent, 'z_far', axis=0, tiled=True)  47.7 us
    all_gather x1, blocking collectives, shards(): column = lax.all_gather(far, 'z_near', axis=0, tiled=True)  13.2 us
    ppermute x1, starting transfers between devices, shards(): taken = lax.ppermute(given, 'core', [(0, 1), (1, 0)])  12.3 us
    pallas_call x3, Pallas kernels, kernel_call(): pl.pallas_call(kernel, out_shape=outputs, in_specs=[pl.BlockSpec(memory_s...  12.2 us
    ppermute x1, starting transfers between devices, shards(): other_weight = lax.ppermute(swap_weight, 'core', [(0, 1), (1, 0)])  11.2 us
    all_to_all x1, waiting for transfers between devices, shards(): lax.all_to_all(pair_sum, 'x', split_axis=0, concat_axis=0, tiled=True)  8.57 us
    all_to_all x1, starting transfers between devices, spread(): return lax.all_to_all(copies, axis, split_axis=0, concat_axis=0, tiled=True)  4.34 us
    all_to_all x1, waiting for transfers between devices, spread(): return lax.all_to_all(copies, axis, split_axis=0, concat_axis=0, tiled=True)  4.13 us
  transfers between devices with their start and end apart: 4, of which 2 were waited for; matrix products, arithmetic and copies ran while one was open for 2% of the time, Pallas kernels for 3%

profile of v9, /device:TPU:1, one launch (start us, length us, event | category | flops | bytes accessed | tf_op | source)
XLA Modules:
  0.0 127.6 jit_solution(16240072299263302864)
XLA Ops:
  1.3 3.1 %shard_map.131 = (bf16[72,128]{1,0:T(8,128)(2,1)}, bf16[2,4,32,128]{3,2,1,0:T(8,128)(2,1)}) custom-call(s32[1]{0:T(128)} %bitcast.device, s32[1]{0:T(128)S(6)} %copy.15.pick, bf16[256,2048]{1,0:T(8,128)(2,1)} %tokens.2, bf16[64,2048]{1,0:T(8,128)(2,1)} %bitcast.20, bf16[64,2048]{1,0:T(8,128)(2,1)} %bitcast.21, f32[1,64]{1,0:T(1,128)} %bitcast.23, ...), custom_call_target="tpu_custom_call" | custom-call | flops 1000000000 | bytes 4194304 | tf_op jit(solution)/shard_map/pallas_call | solution.py:288
  4.3 47.7 %all_gather.6 = bf16[576,128]{1,0:T(8,128)(2,1)S(1)} all-gather(bf16[72,128]{1,0:T(8,128)(2,1)} %get-tuple-element.12), channel_id=1, replica_groups=mesh['z_far'=8,'z_near'=4,'y'=4,'x'=4,'core'=2] {'z_far'}, dimensions={0}, use_global_device_ids=true | all-gather | bytes 165888 | tf_op jit(solution)/shard_map/all_gather | solution.py:355
  52.1 13.2 %all_gather.7 = bf16[2304,128]{1,0:T(8,128)(2,1)S(1)} all-gather(bf16[576,128]{1,0:T(8,128)(2,1)S(1)} %all_gather.6), channel_id=1, replica_groups=mesh['z_far'=8,'z_near'=4,'y'=4,'x'=4,'core'=2] {'z_near'}, dimensions={0}, use_global_device_ids=true | all-gather | bytes 737280 | tf_op jit(solution)/shard_map/all_gather | solution.py:356
  65.3 1.7 %broadcast_in_dim.13 = bf16[4,2304,128]{2,1,0:T(8,128)(2,1)} broadcast(bf16[2304,128]{1,0:T(8,128)(2,1)S(1)} %all_gather.7), dimensions={1,2} | broadcast | bytes 2949120 | tf_op jit(solution)/shard_map/broadcast_in_dim | solution.py:28
  67.0 0.0 copy-start.3
  67.0 4.3 %all-to-all-start = ((bf16[4,2304,128]{2,1,0:T(8,128)(2,1)}), bf16[4,2304,128]{2,1,0:T(8,128)(2,1)S(1)}, u32[]{:S(2)}, u32[]{:S(2)}) async-start(bf16[4,2304,128]{2,1,0:T(8,128)(2,1)} %broadcast_in_dim.13), calls=%async_computation | async-start | bytes 4718592 | tf_op jit(solution)/shard_map/all_to_all | solution.py:29
  71.3 0.0 copy-start
  71.3 0.0 copy-start.2
  71.3 11.2 %collective-permute-start = (bf16[256,2048]{1,0:T(8,128)(2,1)}, bf16[256,2048]{1,0:T(8,128)(2,1)}, u32[]{:S(2)}, u32[]{:S(2)}) collective-permute-start(bf16[256,2048]{1,0:T(8,128)(2,1)} %param.19), channel_id=1, source_target_pairs={{0,1},{1,0},{2,3},{3,2},{4,5},{5,4},{6,7},{7,6},{8,9},{9,8},{10,11... | collective-permute-start | bytes 3145736 | tf_op jit(solution)/shard_map/ppermute | solution.py:362
  82.6 0.0 copy-done.3
  82.6 0.6 maximum_bitcast_fusion.gain
  83.2 3.7 %shard_map.132.ready = f32[5,256,128]{2,1,0:T(8,128)} custom-call(s32[1]{0:T(128)} %bitcast.device, s32[1]{0:T(128)} %bitcast.6.group, bf16[256,2048]{1,0:T(8,128)(2,1)} %tokens.2, bf16[2048,256]{1,0:T(8,128)(2,1)} %query_weight.1, bf16[64,2048]{1,0:T(8,128)(2,1)} %bitcast.22, f32[1,128]{1,0:T(1,128)} %maximum_bitcast_fusion.gain, ...), custom_call_target="tpu_custom_call" | custom-call | flops 1000000000 | bytes 4194304 | tf_op jit(solution)/shard_map/pallas_call | solution.py:288
  86.9 0.1 pad_add_fusion.place_of
  86.9 0.0 collective-permute-done
  86.9 4.1 %all-to-all-done = bf16[4,2304,128]{2,1,0:T(8,128)(2,1)S(1)} async-done(((bf16[4,2304,128]{2,1,0:T(8,128)(2,1)}), bf16[4,2304,128]{2,1,0:T(8,128)(2,1)S(1)}, u32[]{:S(2)}, u32[]{:S(2)}) %all-to-all-start) | async-done | bytes 2359328 | tf_op jit(solution)/shard_map/all_to_all | solution.py:29
  91.1 0.0 copy-done
  91.1 0.0 copy-done.2
  91.1 0.0 copy-start.1
  91.1 1.1 copy-done.1
  92.2 5.5 %shard_map.133 = (bf16[4,32,256]{2,1,0:T(8,128)(2,1)S(1)}, bf16[4,32,256]{2,1,0:T(8,128)(2,1)S(1)}, f32[2,256,4]{2,1,0:T(8,128)S(1)}) custom-call(s32[2]{0:T(128)S(1)} %pad_add_fusion.place_of, s32[4,15]{1,0:T(4,128)S(1)} %copy-done, bf16[4,32,72,128]{3,2,1,0:T(8,128)(2,1)S(1)} %bitcast.17, f32[5,256,128]{2,1,0:T(8,128)S(1)} %copy-done.1, ...), custom_call_target="tpu_custom_call" | custom-call | flops 4000000000 | bytes 4194304 | tf_op jit(solution)/shard_map/pallas_call | solution.py:288
  97.6 12.3 %collective-permute-start.1 = (bf16[4,32,256]{2,1,0:T(8,128)(2,1)S(1)}, bf16[4,32,256]{2,1,0:T(8,128)(2,1)S(1)}, u32[]{:S(2)}, u32[]{:S(2)}) collective-permute-start(bf16[4,32,256]{2,1,0:T(8,128)(2,1)S(1)} %get-tuple-element.19), channel_id=1, source_target_pairs={{0,1},{1,0},{2,3},{3,2},{4,5},{5,4},{6,7},{7,6},{8,9},{9,8},{10,11... | collective-permute-start | bytes 196616 | tf_op jit(solution)/shard_map/ppermute | solution.py:405
  109.9 1.5 %fusion.3 = f32[128,2048]{1,0:T(8,128)S(1)} fusion(bf16[128,256]{1,0:T(8,128)(2,1)S(1)} %bitcast.18, bf16[256,2048]{1,0:T(8,128)(2,1)} %param.19), kind=kOutput, calls=%fused_computation.5 | convolution fusion | flops 134742016 | bytes 2162688 | tf_op jit(solution)/shard_map/dot_general | solution.py:406
  111.5 0.0 collective-permute-done.1
  111.5 2.3 %fusion.2 = bf16[128,2048]{1,0:T(8,128)(2,1)} fusion(f32[128,2048]{1,0:T(8,128)S(1)} %fusion.3, bf16[128,256]{1,0:T(8,128)(2,1)S(1)} %bitcast.19, bf16[256,2048]{1,0:T(8,128)(2,1)} %collective-permute-done), kind=kOutput, calls=%fused_computation.3 | convolution fusion | flops 135266304 | bytes 2686976 | tf_op jit(solution)/shard_map/dot_general | solution.py:409
  113.8 3.8 %all-to-all-start.1 = ((bf16[4,32,2048]{2,1,0:T(8,128)(2,1)}), bf16[4,32,2048]{2,1,0:T(8,128)(2,1)S(1)}, u32[]{:S(2)}, u32[]{:S(2)}) async-start(bf16[4,32,2048]{2,1,0:T(8,128)(2,1)} %bitcast.11), calls=%async_computation.1 | async-start | bytes 1048576 | tf_op jit(solution)/shard_map/all_to_all | solution.py:414
  117.6 0.7 copy.14
  118.3 8.6 %all-to-all-done.1 = bf16[4,32,2048]{2,1,0:T(8,128)(2,1)S(1)} async-done(((bf16[4,32,2048]{2,1,0:T(8,128)(2,1)}), bf16[4,32,2048]{2,1,0:T(8,128)(2,1)S(1)}, u32[]{:S(2)}, u32[]{:S(2)}) %all-to-all-start.1) | async-done | bytes 524320 | tf_op jit(solution)/shard_map/all_to_all | solution.py:414
  126.9 0.7 reduce_sum.12
Async XLA Ops:
  67.0 15.6 %copy-start.3 = (f32[64]{0:T(128)S(1)}, f32[64]{0:T(128)}, u32[]{:S(2)}) copy-start(f32[64]{0:T(128)} %param.17) | copy-start | bytes 772
  67.0 24.1 %all-to-all-start = ((bf16[4,2304,128]{2,1,0:T(8,128)(2,1)}), bf16[4,2304,128]{2,1,0:T(8,128)(2,1)S(1)}, u32[]{:S(2)}, u32[]{:S(2)}) async-start(bf16[4,2304,128]{2,1,0:T(8,128)(2,1)} %broadcast_in_dim.13), calls=%async_computation | async-start | bytes 4718592 | tf_op jit(solution)/shard_map/all_to_all | solution.py:29
  71.3 19.7 %copy-start = (s32[4,15]{1,0:T(4,128)S(1)}, s32[4,15]{1,0:T(4,128)}, u32[]{:S(2)}) copy-start(s32[4,15]{1,0:T(4,128)} %chosen.1) | copy-start | bytes 724
  71.3 19.7 %copy-start.2 = (bf16[2,4,32,128]{3,2,1,0:T(8,128)(2,1)S(1)}, bf16[2,4,32,128]{3,2,1,0:T(8,128)(2,1)}, u32[]{:S(2)}) copy-start(bf16[2,4,32,128]{3,2,1,0:T(8,128)(2,1)} %get-tuple-element.17.own) | copy-start | bytes 196612
  71.3 15.6 %collective-permute-start = (bf16[256,2048]{1,0:T(8,128)(2,1)}, bf16[256,2048]{1,0:T(8,128)(2,1)}, u32[]{:S(2)}, u32[]{:S(2)}) collective-permute-start(bf16[256,2048]{1,0:T(8,128)(2,1)} %param.19), channel_id=1, source_target_pairs={{0,1},{1,0},{2,3},{3,2},{4,5},{5,4},{6,7},{7,6},{8,9},{9,8},{10,11... | collective-permute-start | bytes 3145736 | tf_op jit(solution)/shard_map/ppermute | solution.py:362
  91.1 1.1 copy-start.1
  97.6 13.8 %collective-permute-start.1 = (bf16[4,32,256]{2,1,0:T(8,128)(2,1)S(1)}, bf16[4,32,256]{2,1,0:T(8,128)(2,1)S(1)}, u32[]{:S(2)}, u32[]{:S(2)}) collective-permute-start(bf16[4,32,256]{2,1,0:T(8,128)(2,1)S(1)} %get-tuple-element.19), channel_id=1, source_target_pairs={{0,1},{1,0},{2,3},{3,2},{4,5},{5,4},{6,7},{7,6},{8,9},{9,8},{10,11... | collective-permute-start | bytes 196616 | tf_op jit(solution)/shard_map/ppermute | solution.py:405
  113.8 13.1 %all-to-all-start.1 = ((bf16[4,32,2048]{2,1,0:T(8,128)(2,1)}), bf16[4,32,2048]{2,1,0:T(8,128)(2,1)S(1)}, u32[]{:S(2)}, u32[]{:S(2)}) async-start(bf16[4,32,2048]{2,1,0:T(8,128)(2,1)} %bitcast.11), calls=%async_computation.1 | async-start | bytes 1048576 | tf_op jit(solution)/shard_map/all_to_all | solution.py:414

commit v10 on v9

--- a/solution.py
+++ b/solution.py
@@ -395,7 +395,7 @@
             shape((2, tok_rows, head_count), f32),
         ),
         (
-            pltpu.VMEM((2, 2, (chosen_device.shape[1] + 1) * packed, 128), bf16),
+            pltpu.VMEM((4, 2, (chosen_device.shape[1] + 1) * packed, 128), bf16),
             pltpu.VMEM((y_count * z_count * (sent_rows - SEL), 128), bf16),
             pltpu.VMEM((head_count, tok_rows, head_size), f32),
         ),

time: 128 us -> 128 us (level)
  no operation moved by 1% of the time
where the time goes in v10:
time: 128 us; the launch traced here: 127 us
  blocking collectives  60.9 us (48%)
  starting transfers between devices  31.6 us (25%)
  waiting for transfers between devices  12.7 us (10%)
  Pallas kernels  11.8 us (9%)
  matrix products  3.88 us (3%)
  local copies, waits for them, and re-layouts  3.53 us (3%)
  other arithmetic  1.39 us (1%)
  between operations  1.35 us (1%)
    all_gather x1, blocking collectives, shards(): far = lax.all_gather(sent, 'z_far', axis=0, tiled=True)  47.7 us
    all_gather x1, blocking collectives, shards(): column = lax.all_gather(far, 'z_near', axis=0, tiled=True)  13.2 us
    ppermute x1, starting transfers between devices, shards(): taken = lax.ppermute(given, 'core', [(0, 1), (1, 0)])  12.3 us
    pallas_call x3, Pallas kernels, kernel_call(): pl.pallas_call(kernel, out_shape=outputs, in_specs=[pl.BlockSpec(memory_s...  11.8 us
    ppermute x1, starting transfers between devices, shards(): other_weight = lax.ppermute(swap_weight, 'core', [(0, 1), (1, 0)])  11.2 us
    all_to_all x1, waiting for transfers between devices, shards(): lax.all_to_all(pair_sum, 'x', split_axis=0, concat_axis=0, tiled=True)  8.57 us
    all_to_all x1, starting transfers between devices, spread(): return lax.all_to_all(copies, axis, split_axis=0, concat_axis=0, tiled=True)  4.34 us
    all_to_all x1, waiting for transfers between devices, spread(): return lax.all_to_all(copies, axis, split_axis=0, concat_axis=0, tiled=True)  4.13 us
  transfers between devices with their start and end apart: 4, of which 2 were waited for; matrix products, arithmetic and copies ran while one was open for 2% of the time, Pallas kernels for 3%

profile of v10, /device:TPU:1, one launch (start us, length us, event | category | flops | bytes accessed | tf_op | source)
XLA Modules:
  0.0 127.2 jit_solution(3770529225559647190)
XLA Ops:
  1.3 3.1 %shard_map.131 = (bf16[72,128]{1,0:T(8,128)(2,1)}, bf16[2,4,32,128]{3,2,1,0:T(8,128)(2,1)}) custom-call(s32[1]{0:T(128)} %bitcast.device, s32[1]{0:T(128)S(6)} %copy.15.pick, bf16[256,2048]{1,0:T(8,128)(2,1)} %tokens.2, bf16[64,2048]{1,0:T(8,128)(2,1)} %bitcast.20, bf16[64,2048]{1,0:T(8,128)(2,1)} %bitcast.21, f32[1,64]{1,0:T(1,128)} %bitcast.23, ...), custom_call_target="tpu_custom_call" | custom-call | flops 1000000000 | bytes 4194304 | tf_op jit(solution)/shard_map/pallas_call | solution.py:288
  4.3 47.7 %all_gather.6 = bf16[576,128]{1,0:T(8,128)(2,1)S(1)} all-gather(bf16[72,128]{1,0:T(8,128)(2,1)} %get-tuple-element.12), channel_id=1, replica_groups=mesh['z_far'=8,'z_near'=4,'y'=4,'x'=4,'core'=2] {'z_far'}, dimensions={0}, use_global_device_ids=true | all-gather | bytes 165888 | tf_op jit(solution)/shard_map/all_gather | solution.py:355
  52.1 13.2 %all_gather.7 = bf16[2304,128]{1,0:T(8,128)(2,1)S(1)} all-gather(bf16[576,128]{1,0:T(8,128)(2,1)S(1)} %all_gather.6), channel_id=1, replica_groups=mesh['z_far'=8,'z_near'=4,'y'=4,'x'=4,'core'=2] {'z_near'}, dimensions={0}, use_global_device_ids=true | all-gather | bytes 737280 | tf_op jit(solution)/shard_map/all_gather | solution.py:356
  65.3 1.7 %broadcast_in_dim.13 = bf16[4,2304,128]{2,1,0:T(8,128)(2,1)} broadcast(bf16[2304,128]{1,0:T(8,128)(2,1)S(1)} %all_gather.7), dimensions={1,2} | broadcast | bytes 2949120 | tf_op jit(solution)/shard_map/broadcast_in_dim | solution.py:28
  67.0 0.0 copy-start.3
  67.0 4.3 %all-to-all-start = ((bf16[4,2304,128]{2,1,0:T(8,128)(2,1)}), bf16[4,2304,128]{2,1,0:T(8,128)(2,1)S(1)}, u32[]{:S(2)}, u32[]{:S(2)}) async-start(bf16[4,2304,128]{2,1,0:T(8,128)(2,1)} %broadcast_in_dim.13), calls=%async_computation | async-start | bytes 4718592 | tf_op jit(solution)/shard_map/all_to_all | solution.py:29
  71.3 0.0 copy-start
  71.3 0.0 copy-start.2
  71.3 11.2 %collective-permute-start = (bf16[256,2048]{1,0:T(8,128)(2,1)}, bf16[256,2048]{1,0:T(8,128)(2,1)}, u32[]{:S(2)}, u32[]{:S(2)}) collective-permute-start(bf16[256,2048]{1,0:T(8,128)(2,1)} %param.19), channel_id=1, source_target_pairs={{0,1},{1,0},{2,3},{3,2},{4,5},{5,4},{6,7},{7,6},{8,9},{9,8},{10,11... | collective-permute-start | bytes 3145736 | tf_op jit(solution)/shard_map/ppermute | solution.py:362
  82.6 0.0 copy-done.3
  82.6 0.6 maximum_bitcast_fusion.gain
  83.2 3.7 %shard_map.132.ready = f32[5,256,128]{2,1,0:T(8,128)} custom-call(s32[1]{0:T(128)} %bitcast.device, s32[1]{0:T(128)} %bitcast.6.group, bf16[256,2048]{1,0:T(8,128)(2,1)} %tokens.2, bf16[2048,256]{1,0:T(8,128)(2,1)} %query_weight.1, bf16[64,2048]{1,0:T(8,128)(2,1)} %bitcast.22, f32[1,128]{1,0:T(1,128)} %maximum_bitcast_fusion.gain, ...), custom_call_target="tpu_custom_call" | custom-call | flops 1000000000 | bytes 4194304 | tf_op jit(solution)/shard_map/pallas_call | solution.py:288
  86.9 0.1 pad_add_fusion.place_of
  86.9 0.0 collective-permute-done
  86.9 4.1 %all-to-all-done = bf16[4,2304,128]{2,1,0:T(8,128)(2,1)S(1)} async-done(((bf16[4,2304,128]{2,1,0:T(8,128)(2,1)}), bf16[4,2304,128]{2,1,0:T(8,128)(2,1)S(1)}, u32[]{:S(2)}, u32[]{:S(2)}) %all-to-all-start) | async-done | bytes 2359328 | tf_op jit(solution)/shard_map/all_to_all | solution.py:29
  91.1 0.0 copy-done
  91.1 0.0 copy-done.2
  91.1 0.0 copy-start.1
  91.1 1.1 copy-done.1
  92.2 5.0 %shard_map.133 = (bf16[4,32,256]{2,1,0:T(8,128)(2,1)S(1)}, bf16[4,32,256]{2,1,0:T(8,128)(2,1)S(1)}, f32[2,256,4]{2,1,0:T(8,128)S(1)}) custom-call(s32[2]{0:T(128)S(1)} %pad_add_fusion.place_of, s32[4,15]{1,0:T(4,128)S(1)} %copy-done, bf16[4,32,72,128]{3,2,1,0:T(8,128)(2,1)S(1)} %bitcast.17, f32[5,256,128]{2,1,0:T(8,128)S(1)} %copy-done.1, ...), custom_call_target="tpu_custom_call" | custom-call | flops 4000000000 | bytes 4194304 | tf_op jit(solution)/shard_map/pallas_call | solution.py:288
  97.2 12.3 %collective-permute-start.1 = (bf16[4,32,256]{2,1,0:T(8,128)(2,1)S(1)}, bf16[4,32,256]{2,1,0:T(8,128)(2,1)S(1)}, u32[]{:S(2)}, u32[]{:S(2)}) collective-permute-start(bf16[4,32,256]{2,1,0:T(8,128)(2,1)S(1)} %get-tuple-element.19), channel_id=1, source_target_pairs={{0,1},{1,0},{2,3},{3,2},{4,5},{5,4},{6,7},{7,6},{8,9},{9,8},{10,11... | collective-permute-start | bytes 196616 | tf_op jit(solution)/shard_map/ppermute | solution.py:405
  109.5 1.5 %fusion.3 = f32[128,2048]{1,0:T(8,128)S(1)} fusion(bf16[128,256]{1,0:T(8,128)(2,1)S(1)} %bitcast.18, bf16[256,2048]{1,0:T(8,128)(2,1)} %param.19), kind=kOutput, calls=%fused_computation.5 | convolution fusion | flops 134742016 | bytes 2162688 | tf_op jit(solution)/shard_map/dot_general | solution.py:406
  111.0 0.0 collective-permute-done.1
  111.0 2.3 %fusion.2 = bf16[128,2048]{1,0:T(8,128)(2,1)} fusion(f32[128,2048]{1,0:T(8,128)S(1)} %fusion.3, bf16[128,256]{1,0:T(8,128)(2,1)S(1)} %bitcast.19, bf16[256,2048]{1,0:T(8,128)(2,1)} %collective-permute-done), kind=kOutput, calls=%fused_computation.3 | convolution fusion | flops 135266304 | bytes 2686976 | tf_op jit(solution)/shard_map/dot_general | solution.py:409
  113.4 3.8 %all-to-all-start.1 = ((bf16[4,32,2048]{2,1,0:T(8,128)(2,1)}), bf16[4,32,2048]{2,1,0:T(8,128)(2,1)S(1)}, u32[]{:S(2)}, u32[]{:S(2)}) async-start(bf16[4,32,2048]{2,1,0:T(8,128)(2,1)} %bitcast.11), calls=%async_computation.1 | async-start | bytes 1048576 | tf_op jit(solution)/shard_map/all_to_all | solution.py:414
  117.2 0.7 copy.14
  117.9 8.6 %all-to-all-done.1 = bf16[4,32,2048]{2,1,0:T(8,128)(2,1)S(1)} async-done(((bf16[4,32,2048]{2,1,0:T(8,128)(2,1)}), bf16[4,32,2048]{2,1,0:T(8,128)(2,1)S(1)}, u32[]{:S(2)}, u32[]{:S(2)}) %all-to-all-start.1) | async-done | bytes 524320 | tf_op jit(solution)/shard_map/all_to_all | solution.py:414
  126.5 0.7 reduce_sum.12
Async XLA Ops:
  67.0 15.6 %copy-start.3 = (f32[64]{0:T(128)S(1)}, f32[64]{0:T(128)}, u32[]{:S(2)}) copy-start(f32[64]{0:T(128)} %param.17) | copy-start | bytes 772
  67.0 24.1 %all-to-all-start = ((bf16[4,2304,128]{2,1,0:T(8,128)(2,1)}), bf16[4,2304,128]{2,1,0:T(8,128)(2,1)S(1)}, u32[]{:S(2)}, u32[]{:S(2)}) async-start(bf16[4,2304,128]{2,1,0:T(8,128)(2,1)} %broadcast_in_dim.13), calls=%async_computation | async-start | bytes 4718592 | tf_op jit(solution)/shard_map/all_to_all | solution.py:29
  71.3 19.7 %copy-start = (s32[4,15]{1,0:T(4,128)S(1)}, s32[4,15]{1,0:T(4,128)}, u32[]{:S(2)}) copy-start(s32[4,15]{1,0:T(4,128)} %chosen.1) | copy-start | bytes 724
  71.3 19.7 %copy-start.2 = (bf16[2,4,32,128]{3,2,1,0:T(8,128)(2,1)S(1)}, bf16[2,4,32,128]{3,2,1,0:T(8,128)(2,1)}, u32[]{:S(2)}) copy-start(bf16[2,4,32,128]{3,2,1,0:T(8,128)(2,1)} %get-tuple-element.17.own) | copy-start | bytes 196612
  71.3 15.6 %collective-permute-start = (bf16[256,2048]{1,0:T(8,128)(2,1)}, bf16[256,2048]{1,0:T(8,128)(2,1)}, u32[]{:S(2)}, u32[]{:S(2)}) collective-permute-start(bf16[256,2048]{1,0:T(8,128)(2,1)} %param.19), channel_id=1, source_target_pairs={{0,1},{1,0},{2,3},{3,2},{4,5},{5,4},{6,7},{7,6},{8,9},{9,8},{10,11... | collective-permute-start | bytes 3145736 | tf_op jit(solution)/shard_map/ppermute | solution.py:362
  91.1 1.1 copy-start.1
  97.2 13.8 %collective-permute-start.1 = (bf16[4,32,256]{2,1,0:T(8,128)(2,1)S(1)}, bf16[4,32,256]{2,1,0:T(8,128)(2,1)S(1)}, u32[]{:S(2)}, u32[]{:S(2)}) collective-permute-start(bf16[4,32,256]{2,1,0:T(8,128)(2,1)S(1)} %get-tuple-element.19), channel_id=1, source_target_pairs={{0,1},{1,0},{2,3},{3,2},{4,5},{5,4},{6,7},{7,6},{8,9},{9,8},{10,11... | collective-permute-start | bytes 196616 | tf_op jit(solution)/shard_map/ppermute | solution.py:405
  113.4 13.1 %all-to-all-start.1 = ((bf16[4,32,2048]{2,1,0:T(8,128)(2,1)}), bf16[4,32,2048]{2,1,0:T(8,128)(2,1)S(1)}, u32[]{:S(2)}, u32[]{:S(2)}) async-start(bf16[4,32,2048]{2,1,0:T(8,128)(2,1)} %bitcast.11), calls=%async_computation.1 | async-start | bytes 1048576 | tf_op jit(solution)/shard_map/all_to_all | solution.py:414
